TPU v7x, 256 devices: a 4x2x16 block of a 4x16x16 slice. The times are simulated.
256 devices in a mesh: grp: 2 (over y), sp: 16 (over z), tp: 8 (over x, core).
Axes of the slice: x: 4, y: 2, z: 16, core: 2. Of those that a mesh axis runs over, the one named last changes fastest.
The devices are a block of a 4x16x16 slice.
Arguments:
- hidden_in: bfloat16 [12288, 4096], P(('grp', 'sp'), 'tp'), parts along dimension 0, may hold values from -30 to 30
- in_gain: float32 [2, 4096], P(None, 'tp'), may hold values from 0.1 to 1.9
- w_value: bfloat16 [2, 4096, 2048], P(None, 'sp', 'tp'), may hold values from -0.09375 to 0.09375
- w_gate: bfloat16 [2, 4096, 2048], P(None, 'sp', 'tp'), may hold values from -0.09375 to 0.09375
- conv_taps: float32 [2, 31, 2048], P(None, None, 'tp'), may hold values from -9 to 9
- norm_gain: float32 [2, 2048], P(None, 'tp'), may hold values from 0.1 to 1.9
- norm_shift: float32 [2, 2048], P(None, 'tp'), may hold values from -3 to 3
- w_out: bfloat16 [2, 2048, 4096], P(None, 'tp', 'sp'), may hold values from -0.125 to 0.125
Outputs:
- hidden_out: bfloat16 [12288, 4096], P(('grp', 'sp'), 'tp'), parts along dimension 0
There are 2 independent parts, one for each index of `grp`. A program takes and returns all parts, laid end to end along the dimension named above; an argument that names none is the same for every part. Nothing has to cross between parts.
All inputs are finite; a program needn't handle non-finite values.
Results may differ from a plain program's by a relative error of at most 0.013.
Values may be sent and summed in bfloat16 or wider, within the bound.
No kernel may reach another device: no remote copies, remote signals or barrier semaphores. Data moves between devices by JAX's collectives and lax.ppermute only.
A program may use at most 64 MiB of HBM per device.

v0:
```python
import jax
import jax.numpy as jnp
from jax import lax
from jax.experimental import pallas as pl
from jax.experimental.pallas import tpu as pltpu
from jax.sharding import PartitionSpec as P

epsilon = 1e-06


def shifted(value, axis, steps):
    count = lax.axis_size(axis)
    return lax.ppermute(value, axis, [(i, (i + steps) % count) for i in range(count)])


def swapped(value):
    return lax.ppermute(value, "tp", [(i, i ^ 1) for i in range(lax.axis_size("tp"))])


def passed_along(value, axis, steps):
    count = lax.axis_size(axis)
    initial, last = (max(0, -steps), min(count, count - steps))
    return lax.ppermute(value, axis, [(source, source + steps) for source in range(initial, last)])


def offsets_of(count):
    half = count // 2
    apart = [d if d <= half else d - count for d in range(0, count, 2)]
    return sorted(apart, key=lambda d: -abs(d))


def project(pieces, inv_rms, rows, width):
    tokens, size = pieces[0].shape
    count = len(pieces)
    offsets = offsets_of(count)[::-1]

    def kernel(*refs):
        blocks, (inv_ref, w_ref, out_ref, held, arrived) = refs[:count], refs[count:]
        lane = lax.axis_index("tp")
        other = lane + 1 - 2 * (lane % 2)
        copies = []
        for i in range(count):
            base = lane if i < len(offsets) else other
            at = (base + offsets[i % len(offsets)] + count) % count
            copies.append(
                pltpu.make_async_copy(
                    w_ref.at[pl.ds(pl.multiple_of(at * size, size), size), pl.ds(0, 2 * width)],
                    held.at[i],
                    arrived.at[i],
                )
            )
            copies[-1].start()
        total = None
        for i in range(count):
            copies[i].wait()
            part = jnp.dot(blocks[i][...], held[i], preferred_element_type=jnp.float32)
            total = part if total is None else total + part
        inv = inv_ref[...]
        value, gate = total[:, :width] * inv, total[:, width:] * inv
        out_ref[...] = (value * jax.nn.sigmoid(gate)).astype(out_ref.dtype)

    whole = pl.BlockSpec(memory_space=pltpu.VMEM)
    return pl.pallas_call(
        kernel,
        out_shape=jax.ShapeDtypeStruct((tokens, width), jnp.bfloat16),
        in_specs=[whole] * (count + 1) + [pl.BlockSpec(memory_space=pl.ANY)],
        out_specs=whole,
        scratch_shapes=[
            pltpu.VMEM((count, size, 2 * width), jnp.bfloat16),
            pltpu.SemaphoreType.DMA((count,)),
        ],
        compiler_params=pltpu.CompilerParams(vmem_limit_bytes=24 << 20),
        cost_estimate=pl.CostEstimate(
            flops=4 * tokens * size * count * width,
            bytes_accessed=4 * size * count * width,
            transcendentals=tokens * width,
        ),
        name="project",
    )(*pieces, inv_rms, rows)


def depthwise(gated, taps, lead):
    total_rows, width = gated.shape
    tokens = total_rows - lead
    reach = taps.shape[0] - 1
    tile = 32
    lanes = 128

    def kernel(gated_ref, taps_ref, out_ref, wide):
        wide[...] = gated_ref[...].astype(jnp.float32)

        @pl.loop(0, tokens // tile)
        def _(index):
            start = pl.multiple_of(index * tile, tile)
            for lane in range(0, width, lanes):
                rows = wide[pl.ds(start, tile + lead), pl.ds(lane, lanes)]
                total = None
                for k in range(reach + 1):
                    first = lead - reach + k
                    window = lax.slice_in_dim(rows, first, first + tile, axis=0)
                    part = taps_ref[pl.ds(k, 1), pl.ds(lane, lanes)] * window
                    total = part if total is None else total + part
                out_ref[pl.ds(start, tile), pl.ds(lane, lanes)] = total

    whole = pl.BlockSpec(memory_space=pltpu.VMEM)
    return pl.pallas_call(
        kernel,
        out_shape=jax.ShapeDtypeStruct((tokens, width), jnp.float32),
        in_specs=[whole] * 2,
        out_specs=whole,
        scratch_shapes=[pltpu.VMEM((total_rows, width), jnp.float32)],
        compiler_params=pltpu.CompilerParams(vmem_limit_bytes=8 << 20),
        cost_estimate=pl.CostEstimate(
            flops=2 * tokens * width * (reach + 1),
            bytes_accessed=6 * tokens * width,
            transcendentals=0,
        ),
        name="depthwise",
    )(gated, taps)


def shares(mixed, held, fetched, across=None):
    tokens, width = mixed.shape
    tp = lax.axis_size("tp")
    offsets = offsets_of(tp)
    count = len(offsets)
    size = held.shape[0] // tp
    last = [] if across is None else [jax.ShapeDtypeStruct((tokens, size), jnp.float32)]
    outs = [jax.ShapeDtypeStruct((count - len(last), tokens, size), jnp.bfloat16)] + last

    def kernel(mixed_ref, held_ref, fetched_ref, *refs):
        arrived, (pairs_ref, *own_ref) = refs[: len(refs) - len(outs)], refs[len(refs) - len(outs) :]
        lane = lax.axis_index("tp")
        base = lane if arrived else lane + 1 - 2 * (lane % 2)
        odd = lax.axis_index("grp") % 2 == 1
        for i, d in enumerate(offsets):
            for j in range(0, size, width):
                at = pl.multiple_of((base + d + tp) % tp * size + j, width)
                block = held_ref[pl.ds(at, width), :]
                pair = fetched_ref[pl.ds(at, width), :]
                block = jnp.concatenate(
                    [jnp.where(odd, pair, block), jnp.where(odd, block, pair)], axis=1
                )
                part = jnp.dot(mixed_ref[...], block, preferred_element_type=jnp.float32)
                if arrived:
                    part += arrived[0][i, :, pl.ds(j, width)].astype(jnp.float32)
                if arrived and d == 0:
                    own_ref[0][:, pl.ds(j, width)] = part
                else:
                    pairs_ref[i, :, pl.ds(j, width)] = part.astype(jnp.bfloat16)

    whole = pl.BlockSpec(memory_space=pltpu.VMEM)
    given = [] if across is None else [across]
    return pl.pallas_call(
        kernel,
        out_shape=outs,
        in_specs=[whole] * (3 + len(given)),
        out_specs=[whole] * len(outs),
        compiler_params=pltpu.CompilerParams(vmem_limit_bytes=16 << 20),
        cost_estimate=pl.CostEstimate(
            flops=2 * tokens * width * size * count,
            bytes_accessed=4 * tokens * size * count,
            transcendentals=0,
        ),
        name="shares",
    )(mixed, held, fetched, *given)


def over_lanes(part):
    everyone = jnp.broadcast_to(part[None], (lax.axis_size("tp"), *part.shape))
    return lax.all_to_all(everyone, "tp", 0, 0, tiled=True).sum(axis=0)


def fetched_rows(held):
    return lax.ppermute(held, "grp", [(i, i ^ 1) for i in range(lax.axis_size("grp"))])


def shards(hidden_in, in_gain, w_value, w_gate, conv_taps, norm_gain, norm_shift, w_out):
    layer_count = w_value.shape[0]
    reach_rows = conv_taps.shape[1] - 1
    tp = lax.axis_size("tp")
    tokens = hidden_in.shape[0]
    features = hidden_in.shape[1] * tp
    width = w_value.shape[2]
    channels = width * tp
    offsets = offsets_of(tp)

    half = w_out.shape[2] // 2
    mine = lax.axis_index("grp") % 2 * half
    taken = []
    for layer in range(layer_count):
        part = lax.dynamic_slice_in_dim(w_out[layer], mine, half, 1)
        rows = jnp.concatenate([w_value[layer], w_gate[layer], part], axis=1)
        taken.append(lax.all_gather(rows, "sp", axis=0, tiled=True))

    lead = -(-reach_rows // 32) * 32

    def run(layer, current):
        held = taken[layer][:, 2 * width :]
        fetched = fetched_rows(held)
        widened = current.astype(jnp.float32)
        scaled = (widened * in_gain[layer]).astype(jnp.bfloat16)
        near = [scaled if d == 0 else shifted(scaled, "tp", -d) for d in offsets]
        squares = over_lanes(jnp.sum(widened * widened, axis=1))
        inv_rms = lax.rsqrt(squares / features + epsilon)[:, None]
        far = [swapped(piece) for piece in near]
        gated = project(near[::-1] + far[::-1], inv_rms, taken[layer], width)
        conved = depthwise(gated, conv_taps[layer], lead)
        sums = jnp.stack([jnp.sum(conved, axis=1), jnp.sum(conved * conved, axis=1)])
        totals = over_lanes(sums)
        row_mean = totals[0] / channels
        spread = totals[1] / channels - row_mean * row_mean
        normed = (conved - row_mean[:, None]) * lax.rsqrt(spread + epsilon)[:, None] * norm_gain[
            layer
        ] + norm_shift[layer]
        mixed_out = jax.nn.silu(normed).astype(jnp.bfloat16)
        across = swapped(shares(mixed_out, held, fetched)[0])
        pairs, own = shares(mixed_out, held, fetched, across)
        summed = widened[lead:] + own
        for piece, d in zip(pairs, offsets):
            summed += shifted(piece, "tp", d).astype(jnp.float32)
        return summed.astype(jnp.bfloat16)

    ahead = lead * layer_count
    before = passed_along(hidden_in[tokens - ahead :], "sp", 1)
    current = jnp.concatenate([before, hidden_in], axis=0)
    for layer in range(layer_count):
        current = run(layer, current)
        ahead -= lead
        if ahead:
            absent = (jnp.arange(current.shape[0]) < ahead) & (lax.axis_index("sp") == 0)
            current = jnp.where(absent[:, None], 0, current)
    return current


def solution(mesh):
    placed = (
        P(("grp", "sp"), "tp"),
        P(None, "tp"),
        P(None, "sp", "tp"),
        P(None, "sp", "tp"),
        P(None, None, "tp"),
        P(None, "tp"),
        P(None, "tp"),
        P(None, "tp", "sp"),
    )
    return jax.shard_map(
        shards, mesh=mesh, in_specs=placed, out_specs=P(("grp", "sp"), "tp"), check_vma=False
    )
```

profile of v0, /device:TPU:40, one launch (start us, length us, event | category | flops | bytes accessed | tf_op | source)
XLA Modules:
  0.0 242.4 jit_solution(2017709700234798667)
XLA Ops:
  6.6 1.0 fusion.16
  7.6 1.2 slice_bitcast_fusion.6
  8.8 0.8 pad_maximum_fusion
  9.7 0.7 pad_maximum_fusion.1
  10.5 4.7 %collective-permute-start = (bf16[64,512]{1,0:T(8,128)(2,1)S(1)}, bf16[64,512]{1,0:T(8,128)(2,1)S(1)}, u32[]{:S(2)}, u32[]{:S(2)}) collective-permute-start(bf16[64,512]{1,0:T(8,128)(2,1)S(1)} %slice.69), channel_id=1, source_target_pairs={{0,8},{8,16},{16,24},{24,32},{32,40},{40,48},{48,56},{56,64},{64,7... | collective-permute-start | bytes 196616 | tf_op jit(solution)/shard_map/ppermute | solution.py:23
  15.3 1.9 collective-permute-done
  17.1 0.2 multiply_reduce_fusion
  17.4 1.7 collective-permute-start.1
  19.1 1.7 collective-permute-start.2
  20.8 2.0 collective-permute-start.3
  22.8 8.3 %collective-permute-done.1.refs_1_ = bf16[448,512]{1,0:T(8,128)(2,1)S(1)} collective-permute-done((bf16[448,512]{1,0:T(8,128)(2,1)S(1)}, bf16[448,512]{1,0:T(8,128)(2,1)S(1)}, u32[]{:S(2)}, u32[]{:S(2)}) %collective-permute-start.1) | collective-permute-done | bytes 458784 | tf_op jit(solution)/shard_map/ppermute | solution.py:13
  31.1 8.5 %collective-permute-done.2.refs_2_ = bf16[448,512]{1,0:T(8,128)(2,1)} collective-permute-done((bf16[448,512]{1,0:T(8,128)(2,1)S(1)}, bf16[448,512]{1,0:T(8,128)(2,1)}, u32[]{:S(2)}, u32[]{:S(2)}) %collective-permute-start.2) | collective-permute-done | bytes 458784 | tf_op jit(solution)/shard_map/ppermute | solution.py:13
  39.6 1.8 collective-permute-done.3.refs_3_
  41.5 0.6 broadcast_in_dim.22
  42.1 3.7 %all-to-all-start = ((f32[8,1,448]{2,1,0:T(1,128)}), f32[8,1,448]{2,1,0:T(1,128)S(1)}, u32[]{:S(2)}, u32[]{:S(2)}) async-start(f32[8,1,448]{2,1,0:T(1,128)} %broadcast_in_dim.22), calls=%async_computation | async-start | bytes 32768 | tf_op jit(solution)/shard_map/all_to_all | solution.py:171
  45.9 5.3 %all-to-all-done = f32[8,1,448]{2,1,0:T(1,128)S(1)} async-done(((f32[8,1,448]{2,1,0:T(1,128)}), f32[8,1,448]{2,1,0:T(1,128)S(1)}, u32[]{:S(2)}, u32[]{:S(2)}) %all-to-all-start) | async-done | bytes 14368 | tf_op jit(solution)/shard_map/all_to_all | solution.py:171
  51.3 0.1 copy.20.refs_8_
  51.4 50.4 %all-gather.3.cloned.1.call-done.refs_9_ = bf16[4096,640]{1,0:T(8,128)(2,1)} async-done(((bf16[256,640]{1,0:T(8,128)(2,1)}), bf16[4096,640]{1,0:T(8,128)(2,1)}) %all-gather.3.cloned.1.call-update) | async-done | bytes 5242896 | tf_op jit(solution)/shard_map/all_gather | solution.py:194
  101.8 1.3 slice.95.held_ref
  103.2 0.6 collective-permute-start.8
  103.8 2.5 %copy-done.1 = bf16[4096,640]{1,0:T(8,128)(2,1)S(1)} copy-done((bf16[4096,640]{1,0:T(8,128)(2,1)S(1)}, bf16[4096,640]{1,0:T(8,128)(2,1)}, u32[]{:S(2)}) %copy-start.1) | copy-done | bytes 5242904
  106.3 4.6 %project.2.gated_ref = bf16[448,256]{1,0:T(8,128)(2,1)S(1)} custom-call(bf16[448,512]{1,0:T(8,128)(2,1)S(1)} %get-tuple-element.28.refs_0_, bf16[448,512]{1,0:T(8,128)(2,1)S(1)} %collective-permute-done.1.refs_1_, bf16[448,512]{1,0:T(8,128)(2,1)} %collective-permute-done.2.refs_2_, bf16[448,512]{1,0:T(8,128)(2,1)} %collective-permute-done.3.refs_3_, ...), custom_call_target="tpu_custom_call" | custom-call | flops 1879048192 | bytes 4194304 | tf_op jit(solution)/shard_map/project/pallas_call | solution.py:63
  110.9 2.5 %depthwise.2 = f32[416,256]{1,0:T(8,128)S(1)} custom-call(bf16[448,256]{1,0:T(8,128)(2,1)S(1)} %project.2.gated_ref, f32[31,256]{1,0:T(8,128)S(1)} %bitcast.43), custom_call_target="tpu_custom_call" | custom-call | flops 6602752 | bytes 638976 | tf_op jit(solution)/shard_map/depthwise/pallas_call | solution.py:106
  113.3 0.2 fusion.13
  113.6 0.6 broadcast_in_dim.23
  114.2 4.5 %all-to-all-start.1 = ((f32[8,2,416]{2,1,0:T(2,128)}), f32[8,2,416]{2,1,0:T(2,128)S(1)}, u32[]{:S(2)}, u32[]{:S(2)}) async-start(f32[8,2,416]{2,1,0:T(2,128)} %broadcast_in_dim.23), calls=%async_computation.1 | async-start | bytes 65536 | tf_op jit(solution)/shard_map/all_to_all | solution.py:171
  118.7 5.4 %all-to-all-done.1 = f32[8,2,416]{2,1,0:T(2,128)S(1)} async-done(((f32[8,2,416]{2,1,0:T(2,128)}), f32[8,2,416]{2,1,0:T(2,128)S(1)}, u32[]{:S(2)}, u32[]{:S(2)}) %all-to-all-start.1) | async-done | bytes 26656 | tf_op jit(solution)/shard_map/all_to_all | solution.py:171
  124.2 0.2 multiply_convert_fusion.2.mixed_ref
  124.4 0.6 shares.4
  125.2 3.6 %collective-permute-done.9.refs_0_ = bf16[4,416,512]{2,1,0:T(8,128)(2,1)S(1)} collective-permute-done((bf16[4,416,512]{2,1,0:T(8,128)(2,1)S(1)}, bf16[4,416,512]{2,1,0:T(8,128)(2,1)S(1)}, u32[]{:S(2)}, u32[]{:S(2)}) %collective-permute-start.9) | collective-permute-done | bytes 1703968 | tf_op jit(solution)/shard_map/ppermute | solution.py:17
  128.8 0.6 shares.5
  129.4 0.8 slice_bitcast_fusion.2
  130.2 1.1 collective-permute-start.10
  131.3 0.9 collective-permute-start.11
  132.3 2.3 collective-permute-start.12
  134.7 10.0 %collective-permute-done.10 = bf16[416,512]{1,0:T(8,128)(2,1)S(1)} collective-permute-done((bf16[416,512]{1,0:T(8,128)(2,1)}, bf16[416,512]{1,0:T(8,128)(2,1)S(1)}, u32[]{:S(2)}, u32[]{:S(2)}) %collective-permute-start.10) | collective-permute-done | bytes 426016 | tf_op jit(solution)/shard_map/ppermute | solution.py:13
  144.7 8.3 %collective-permute-done.11 = bf16[416,512]{1,0:T(8,128)(2,1)S(1)} collective-permute-done((bf16[416,512]{1,0:T(8,128)(2,1)S(1)}, bf16[416,512]{1,0:T(8,128)(2,1)S(1)}, u32[]{:S(2)}, u32[]{:S(2)}) %collective-permute-start.11) | collective-permute-done | bytes 426016 | tf_op jit(solution)/shard_map/ppermute | solution.py:13
  152.9 0.4 multiply_reduce_fusion.1
  153.5 0.7 collective-permute-start.13
  154.1 2.7 %collective-permute-start.14 = (bf16[416,512]{1,0:T(8,128)(2,1)S(1)}, bf16[416,512]{1,0:T(8,128)(2,1)}, u32[]{:S(2)}, u32[]{:S(2)}) collective-permute-start(bf16[416,512]{1,0:T(8,128)(2,1)S(1)} %multiply_convert_fusion.1.refs_0_), channel_id=1, source_target_pairs={{0,6},{1,7},{2,0},{3,1},{4,2},{5,3},{6,4},{7,5},{8,14},{9,15},{10,... | collective-permute-start | bytes 1277960 | tf_op jit(solution)/shard_map/ppermute | solution.py:13
  156.8 18.9 %collective-permute-done.13.refs_1_ = bf16[416,512]{1,0:T(8,128)(2,1)S(1)} collective-permute-done((bf16[416,512]{1,0:T(8,128)(2,1)S(1)}, bf16[416,512]{1,0:T(8,128)(2,1)S(1)}, u32[]{:S(2)}, u32[]{:S(2)}) %collective-permute-start.13) | collective-permute-done | bytes 426016 | tf_op jit(solution)/shard_map/ppermute | solution.py:13
  175.8 0.5 collective-permute-start.18
  176.4 0.6 broadcast_in_dim.24
  177.0 4.2 %all-to-all-start.2 = ((f32[8,1,416]{2,1,0:T(1,128)}), f32[8,1,416]{2,1,0:T(1,128)S(1)}, u32[]{:S(2)}, u32[]{:S(2)}) async-start(f32[8,1,416]{2,1,0:T(1,128)} %broadcast_in_dim.24), calls=%async_computation.2 | async-start | bytes 32768 | tf_op jit(solution)/shard_map/all_to_all | solution.py:171
  181.3 1.3 slice.99.held_ref
  182.6 1.5 collective-permute-start.20
  184.1 2.5 %all-to-all-done.2 = f32[8,1,416]{2,1,0:T(1,128)S(1)} async-done(((f32[8,1,416]{2,1,0:T(1,128)}), f32[8,1,416]{2,1,0:T(1,128)S(1)}, u32[]{:S(2)}, u32[]{:S(2)}) %all-to-all-start.2) | async-done | bytes 13344 | tf_op jit(solution)/shard_map/all_to_all | solution.py:171
  186.9 2.5 %copy-done = bf16[4096,640]{1,0:T(8,128)(2,1)S(1)} copy-done((bf16[4096,640]{1,0:T(8,128)(2,1)S(1)}, bf16[4096,640]{1,0:T(8,128)(2,1)}, u32[]{:S(2)}) %copy-start) | copy-done | bytes 5242904
  189.3 4.4 %project.3.gated_ref = bf16[416,256]{1,0:T(8,128)(2,1)S(1)} custom-call(bf16[416,512]{1,0:T(8,128)(2,1)S(1)} %multiply_convert_fusion.1.refs_0_, bf16[416,512]{1,0:T(8,128)(2,1)S(1)} %collective-permute-done.13.refs_1_, bf16[416,512]{1,0:T(8,128)(2,1)} %collective-permute-done.14.refs_2_, bf16[416,512]{1,0:T(8,128)(2,1)} %collective-permute-done.15.refs_3_, ...), custom_call_target="tpu_custom_call" | custom-call | flops 1744830464 | bytes 4194304 | tf_op jit(solution)/shard_map/project/pallas_call | solution.py:63
  193.7 2.3 depthwise.3
  196.0 0.2 fusion.14
  196.2 7.8 %all_to_all.22 = f32[8,2,384]{2,1,0:T(2,128)S(1)} all-to-all(f32[8,2,384]{2,1,0:T(2,128)S(1)} %broadcast_in_dim.25), channel_id=1, replica_groups=mesh['grp'=2,'sp'=16,'tp'=8] {'tp'}, dimensions={0} | all-to-all | bytes 49152 | tf_op jit(solution)/shard_map/all_to_all | solution.py:171
  204.1 0.2 multiply_convert_fusion.3.mixed_ref
  204.3 3.9 %collective-permute-done.20.fetched_ref = bf16[4096,128]{1,0:T(8,128)(2,1)S(1)} collective-permute-done((bf16[4096,128]{1,0:T(8,128)(2,1)S(1)}, bf16[4096,128]{1,0:T(8,128)(2,1)S(1)}, u32[]{:S(2)}, u32[]{:S(2)}) %collective-permute-start.20) | collective-permute-done | bytes 1048608 | tf_op jit(solution)/shard_map/ppermute | solution.py:175
  208.3 0.6 shares.6
  209.0 3.4 %collective-permute-done.21.refs_0_ = bf16[4,384,512]{2,1,0:T(8,128)(2,1)S(1)} collective-permute-done((bf16[4,384,512]{2,1,0:T(8,128)(2,1)S(1)}, bf16[4,384,512]{2,1,0:T(8,128)(2,1)S(1)}, u32[]{:S(2)}, u32[]{:S(2)}) %collective-permute-start.21) | collective-permute-done | bytes 1572896 | tf_op jit(solution)/shard_map/ppermute | solution.py:17
  212.4 0.6 shares.7
  213.1 3.3 %collective-permute-start.22 = (bf16[384,512]{1,0:T(8,128)(2,1)S(1)}, bf16[384,512]{1,0:T(8,128)(2,1)S(1)}, u32[]{:S(2)}, u32[]{:S(2)}) collective-permute-start(bf16[384,512]{1,0:T(8,128)(2,1)S(1)} %get-tuple-element.24), channel_id=1, source_target_pairs={{0,4},{1,5},{2,6},{3,7},{4,0},{5,1},{6,2},{7,3},{8,12},{9,13},{10,... | collective-permute-start | bytes 1179656 | tf_op jit(solution)/shard_map/ppermute | solution.py:13
  216.3 0.6 collective-permute-start.23
  216.9 2.7 %collective-permute-start.24 = (bf16[384,512]{1,0:T(8,128)(2,1)S(1)}, bf16[384,512]{1,0:T(8,128)(2,1)S(1)}, u32[]{:S(2)}, u32[]{:S(2)}) collective-permute-start(bf16[384,512]{1,0:T(8,128)(2,1)S(1)} %get-tuple-element.25), channel_id=1, source_target_pairs={{0,6},{1,7},{2,0},{3,1},{4,2},{5,3},{6,4},{7,5},{8,14},{9,15},{10,... | collective-permute-start | bytes 1179656 | tf_op jit(solution)/shard_map/ppermute | solution.py:13
  219.6 7.2 %collective-permute-done.22 = bf16[384,512]{1,0:T(8,128)(2,1)S(1)} collective-permute-done((bf16[384,512]{1,0:T(8,128)(2,1)S(1)}, bf16[384,512]{1,0:T(8,128)(2,1)S(1)}, u32[]{:S(2)}, u32[]{:S(2)}) %collective-permute-start.22) | collective-permute-done | bytes 393248 | tf_op jit(solution)/shard_map/ppermute | solution.py:13
  226.7 7.6 %collective-permute-done.23 = bf16[384,512]{1,0:T(8,128)(2,1)S(1)} collective-permute-done((bf16[384,512]{1,0:T(8,128)(2,1)S(1)}, bf16[384,512]{1,0:T(8,128)(2,1)S(1)}, u32[]{:S(2)}, u32[]{:S(2)}) %collective-permute-start.23) | collective-permute-done | bytes 393248 | tf_op jit(solution)/shard_map/ppermute | solution.py:13
  234.3 0.2 collective-permute-done.24
  234.5 1.0 fusion.7
  (74 shorter events, 1.4 us)
Async XLA Ops:
  6.5 95.3 %all-gather.3.cloned.1.call-start = ((), (), s32[]{:S(2)}) async-start(), calls=%async_computation.4 | async-start | bytes 5570560 | tf_op jit(solution)/shard_map/all_gather | solution.py:194
  7.6 3.0 %copy-start.4 = (bf16[384,512]{1,0:T(8,128)(2,1)S(1)}, bf16[384,512]{1,0:T(8,128)(2,1)}, u32[]{:S(2)}) copy-start(bf16[384,512]{1,0:T(8,128)(2,1)} %param.8) | copy-start | bytes 1179652
  7.6 7.7 %copy-start.7 = (f32[2,512]{1,0:T(2,128)S(1)}, f32[2,512]{1,0:T(2,128)}, u32[]{:S(2)}) copy-start(f32[2,512]{1,0:T(2,128)} %param.9) | copy-start | bytes 12292
  8.8 32.7 %copy-start.6 = (f32[2,31,256]{2,0,1:T(2,128)S(1)}, f32[2,31,256]{2,0,1:T(2,128)}, u32[]{:S(2)}) copy-start(f32[2,31,256]{2,0,1:T(2,128)} %param.12) | copy-start | bytes 190468
  8.8 37.1 %copy-start.8 = (f32[2,256]{1,0:T(2,128)S(1)}, f32[2,256]{1,0:T(2,128)}, u32[]{:S(2)}) copy-start(f32[2,256]{1,0:T(2,128)} %param.13) | copy-start | bytes 6148
  9.6 171.7 %all-gather.5.cloned.1.call-start = ((), (), s32[]{:S(2)}) async-start(), calls=%async_computation.5 | async-start | bytes 5570560 | tf_op jit(solution)/shard_map/all_gather | solution.py:194
  10.5 6.6 %collective-permute-start = (bf16[64,512]{1,0:T(8,128)(2,1)S(1)}, bf16[64,512]{1,0:T(8,128)(2,1)S(1)}, u32[]{:S(2)}, u32[]{:S(2)}) collective-permute-start(bf16[64,512]{1,0:T(8,128)(2,1)S(1)} %slice.69), channel_id=1, source_target_pairs={{0,8},{8,16},{16,24},{24,32},{32,40},{40,48},{48,56},{56,64},{64,7... | collective-permute-start | bytes 196616 | tf_op jit(solution)/shard_map/ppermute | solution.py:23
  17.4 13.8 %collective-permute-start.1 = (bf16[448,512]{1,0:T(8,128)(2,1)S(1)}, bf16[448,512]{1,0:T(8,128)(2,1)S(1)}, u32[]{:S(2)}, u32[]{:S(2)}) collective-permute-start(bf16[448,512]{1,0:T(8,128)(2,1)S(1)} %get-tuple-element.28.refs_0_), channel_id=1, source_target_pairs={{0,2},{1,3},{2,4},{3,5},{4,6},{5,7},{6,0},{7,1},{8,10},{9,11},{10,... | collective-permute-start | bytes 1376264 | tf_op jit(solution)/shard_map/ppermute | solution.py:13
  19.1 20.5 %collective-permute-start.2 = (bf16[448,512]{1,0:T(8,128)(2,1)S(1)}, bf16[448,512]{1,0:T(8,128)(2,1)}, u32[]{:S(2)}, u32[]{:S(2)}) collective-permute-start(bf16[448,512]{1,0:T(8,128)(2,1)S(1)} %get-tuple-element.28.refs_0_), channel_id=1, source_target_pairs={{0,6},{1,7},{2,0},{3,1},{4,2},{5,3},{6,4},{7,5},{8,14},{9,15},{10,... | collective-permute-start | bytes 1376264 | tf_op jit(solution)/shard_map/ppermute | solution.py:13
  20.8 20.7 %collective-permute-start.3 = (bf16[448,512]{1,0:T(8,128)(2,1)S(1)}, bf16[448,512]{1,0:T(8,128)(2,1)}, u32[]{:S(2)}, u32[]{:S(2)}) collective-permute-start(bf16[448,512]{1,0:T(8,128)(2,1)S(1)} %get-tuple-element.28.refs_0_), channel_id=1, source_target_pairs={{0,4},{1,5},{2,6},{3,7},{4,0},{5,1},{6,2},{7,3},{8,12},{9,13},{10,... | collective-permute-start | bytes 1376264 | tf_op jit(solution)/shard_map/ppermute | solution.py:13
  22.8 81.0 %collective-permute-start.4 = (bf16[448,512]{1,0:T(8,128)(2,1)S(1)}, bf16[448,512]{1,0:T(8,128)(2,1)}, u32[]{:S(2)}, u32[]{:S(2)}) collective-permute-start(bf16[448,512]{1,0:T(8,128)(2,1)S(1)} %get-tuple-element.28.refs_0_), channel_id=1, source_target_pairs={{0,1},{1,0},{2,3},{3,2},{4,5},{5,4},{6,7},{7,6},{8,9},{9,8},{10,11... | collective-permute-start | bytes 1376264 | tf_op jit(solution)/shard_map/ppermute | solution.py:17
  31.1 72.7 %collective-permute-start.5 = (bf16[448,512]{1,0:T(8,128)(2,1)S(1)}, bf16[448,512]{1,0:T(8,128)(2,1)}, u32[]{:S(2)}, u32[]{:S(2)}) collective-permute-start(bf16[448,512]{1,0:T(8,128)(2,1)S(1)} %collective-permute-done.1.refs_1_), channel_id=1, source_target_pairs={{0,1},{1,0},{2,3},{3,2},{4,5},{5,4},{6,7},{7,6},{8,9},{9,8},{10,11... | collective-permute-start | bytes 1376264 | tf_op jit(solution)/shard_map/ppermute | solution.py:17
  39.6 64.2 %collective-permute-start.6 = (bf16[448,512]{1,0:T(8,128)(2,1)}, bf16[448,512]{1,0:T(8,128)(2,1)}, u32[]{:S(2)}, u32[]{:S(2)}) collective-permute-start(bf16[448,512]{1,0:T(8,128)(2,1)} %collective-permute-done.2.refs_2_), channel_id=1, source_target_pairs={{0,1},{1,0},{2,3},{3,2},{4,5},{5,4},{6,7},{7,6},{8,9},{9,8},{10,11... | collective-permute-start | bytes 1376264 | tf_op jit(solution)/shard_map/ppermute | solution.py:17
  41.5 62.3 %collective-permute-start.7 = (bf16[448,512]{1,0:T(8,128)(2,1)}, bf16[448,512]{1,0:T(8,128)(2,1)}, u32[]{:S(2)}, u32[]{:S(2)}) collective-permute-start(bf16[448,512]{1,0:T(8,128)(2,1)} %collective-permute-done.3.refs_3_), channel_id=1, source_target_pairs={{0,1},{1,0},{2,3},{3,2},{4,5},{5,4},{6,7},{7,6},{8,9},{9,8},{10,11... | collective-permute-start | bytes 1376264 | tf_op jit(solution)/shard_map/ppermute | solution.py:17
  42.1 9.1 %all-to-all-start = ((f32[8,1,448]{2,1,0:T(1,128)}), f32[8,1,448]{2,1,0:T(1,128)S(1)}, u32[]{:S(2)}, u32[]{:S(2)}) async-start(f32[8,1,448]{2,1,0:T(1,128)} %broadcast_in_dim.22), calls=%async_computation | async-start | bytes 32768 | tf_op jit(solution)/shard_map/all_to_all | solution.py:171
  101.8 16.8 %copy-start.9 = (f32[2,256]{1,0:T(2,128)S(1)}, f32[2,256]{1,0:T(2,128)}, u32[]{:S(2)}) copy-start(f32[2,256]{1,0:T(2,128)} %param.14) | copy-start | bytes 6148
  103.2 21.2 %collective-permute-start.8 = (bf16[4096,128]{1,0:T(8,128)(2,1)S(1)}, bf16[4096,128]{1,0:T(8,128)(2,1)S(1)}, u32[]{:S(2)}, u32[]{:S(2)}) collective-permute-start(bf16[4096,128]{1,0:T(8,128)(2,1)S(1)} %slice.95.held_ref), channel_id=1, source_target_pairs={{0,128},{128,0},{1,129},{129,1},{2,130},{130,2},{3,131},{131,3},{4... | collective-permute-start | bytes 3145736 | tf_op jit(solution)/shard_map/ppermute | solution.py:175
  103.8 2.5 %copy-start.1 = (bf16[4096,640]{1,0:T(8,128)(2,1)S(1)}, bf16[4096,640]{1,0:T(8,128)(2,1)}, u32[]{:S(2)}) copy-start(bf16[4096,640]{1,0:T(8,128)(2,1)} %all-gather.3.cloned.1.call-done.refs_9_) | copy-start | bytes 15728644
  114.2 9.9 %all-to-all-start.1 = ((f32[8,2,416]{2,1,0:T(2,128)}), f32[8,2,416]{2,1,0:T(2,128)S(1)}, u32[]{:S(2)}, u32[]{:S(2)}) async-start(f32[8,2,416]{2,1,0:T(2,128)} %broadcast_in_dim.23), calls=%async_computation.1 | async-start | bytes 65536 | tf_op jit(solution)/shard_map/all_to_all | solution.py:171
  125.0 3.7 %collective-permute-start.9 = (bf16[4,416,512]{2,1,0:T(8,128)(2,1)S(1)}, bf16[4,416,512]{2,1,0:T(8,128)(2,1)S(1)}, u32[]{:S(2)}, u32[]{:S(2)}) collective-permute-start(bf16[4,416,512]{2,1,0:T(8,128)(2,1)S(1)} %shares.4), channel_id=1, source_target_pairs={{0,1},{1,0},{2,3},{3,2},{4,5},{5,4},{6,7},{7,6},{8,9},{9,8},{10,11... | collective-permute-start | bytes 5111816 | tf_op jit(solution)/shard_map/ppermute | solution.py:17
  129.4 5.2 %copy-start.5 = (bf16[384,512]{1,0:T(8,128)(2,1)S(1)}, bf16[384,512]{1,0:T(8,128)(2,1)}, u32[]{:S(2)}) copy-start(bf16[384,512]{1,0:T(8,128)(2,1)} %param.8) | copy-start | bytes 1179652
  130.2 14.4 %collective-permute-start.10 = (bf16[416,512]{1,0:T(8,128)(2,1)}, bf16[416,512]{1,0:T(8,128)(2,1)S(1)}, u32[]{:S(2)}, u32[]{:S(2)}) collective-permute-start(bf16[416,512]{1,0:T(8,128)(2,1)} %get-tuple-element.21), channel_id=1, source_target_pairs={{0,4},{1,5},{2,6},{3,7},{4,0},{5,1},{6,2},{7,3},{8,12},{9,13},{10,... | collective-permute-start | bytes 1277960 | tf_op jit(solution)/shard_map/ppermute | solution.py:13
  131.3 21.6 %collective-permute-start.11 = (bf16[416,512]{1,0:T(8,128)(2,1)S(1)}, bf16[416,512]{1,0:T(8,128)(2,1)S(1)}, u32[]{:S(2)}, u32[]{:S(2)}) collective-permute-start(bf16[416,512]{1,0:T(8,128)(2,1)S(1)} %get-tuple-element.23), channel_id=1, source_target_pairs={{0,2},{1,3},{2,4},{3,5},{4,6},{5,7},{6,0},{7,1},{8,10},{9,11},{10,... | collective-permute-start | bytes 1277960 | tf_op jit(solution)/shard_map/ppermute | solution.py:13
  132.3 20.7 %collective-permute-start.12 = (bf16[416,512]{1,0:T(8,128)(2,1)S(1)}, bf16[416,512]{1,0:T(8,128)(2,1)S(1)}, u32[]{:S(2)}, u32[]{:S(2)}) collective-permute-start(bf16[416,512]{1,0:T(8,128)(2,1)S(1)} %get-tuple-element.22), channel_id=1, source_target_pairs={{0,6},{1,7},{2,0},{3,1},{4,2},{5,3},{6,4},{7,5},{8,14},{9,15},{10,... | collective-permute-start | bytes 1277960 | tf_op jit(solution)/shard_map/ppermute | solution.py:13
  153.4 22.9 %copy-start.2 = (f32[416,512]{1,0:T(8,128)}, f32[416,512]{1,0:T(8,128)S(1)}, u32[]{:S(2)}) copy-start(f32[416,512]{1,0:T(8,128)S(1)} %get-tuple-element.20) | copy-start | bytes 2555908
  153.5 22.3 %collective-permute-start.13 = (bf16[416,512]{1,0:T(8,128)(2,1)S(1)}, bf16[416,512]{1,0:T(8,128)(2,1)S(1)}, u32[]{:S(2)}, u32[]{:S(2)}) collective-permute-start(bf16[416,512]{1,0:T(8,128)(2,1)S(1)} %multiply_convert_fusion.1.refs_0_), channel_id=1, source_target_pairs={{0,2},{1,3},{2,4},{3,5},{4,6},{5,7},{6,0},{7,1},{8,10},{9,11},{10,... | collective-permute-start | bytes 1277960 | tf_op jit(solution)/shard_map/ppermute | solution.py:13
  154.1 21.6 %collective-permute-start.14 = (bf16[416,512]{1,0:T(8,128)(2,1)S(1)}, bf16[416,512]{1,0:T(8,128)(2,1)}, u32[]{:S(2)}, u32[]{:S(2)}) collective-permute-start(bf16[416,512]{1,0:T(8,128)(2,1)S(1)} %multiply_convert_fusion.1.refs_0_), channel_id=1, source_target_pairs={{0,6},{1,7},{2,0},{3,1},{4,2},{5,3},{6,4},{7,5},{8,14},{9,15},{10,... | collective-permute-start | bytes 1277960 | tf_op jit(solution)/shard_map/ppermute | solution.py:13
  156.8 19.5 %collective-permute-start.15 = (bf16[416,512]{1,0:T(8,128)(2,1)S(1)}, bf16[416,512]{1,0:T(8,128)(2,1)}, u32[]{:S(2)}, u32[]{:S(2)}) collective-permute-start(bf16[416,512]{1,0:T(8,128)(2,1)S(1)} %multiply_convert_fusion.1.refs_0_), channel_id=1, source_target_pairs={{0,4},{1,5},{2,6},{3,7},{4,0},{5,1},{6,2},{7,3},{8,12},{9,13},{10,... | collective-permute-start | bytes 1277960 | tf_op jit(solution)/shard_map/ppermute | solution.py:13
  156.8 30.0 %collective-permute-start.16 = (bf16[416,512]{1,0:T(8,128)(2,1)S(1)}, bf16[416,512]{1,0:T(8,128)(2,1)}, u32[]{:S(2)}, u32[]{:S(2)}) collective-permute-start(bf16[416,512]{1,0:T(8,128)(2,1)S(1)} %multiply_convert_fusion.1.refs_0_), channel_id=1, source_target_pairs={{0,1},{1,0},{2,3},{3,2},{4,5},{5,4},{6,7},{7,6},{8,9},{9,8},{10,11... | collective-permute-start | bytes 1277960 | tf_op jit(solution)/shard_map/ppermute | solution.py:17
  175.8 11.0 %collective-permute-start.17 = (bf16[416,512]{1,0:T(8,128)(2,1)S(1)}, bf16[416,512]{1,0:T(8,128)(2,1)}, u32[]{:S(2)}, u32[]{:S(2)}) collective-permute-start(bf16[416,512]{1,0:T(8,128)(2,1)S(1)} %collective-permute-done.13.refs_1_), channel_id=1, source_target_pairs={{0,1},{1,0},{2,3},{3,2},{4,5},{5,4},{6,7},{7,6},{8,9},{9,8},{10,11... | collective-permute-start | bytes 1277960 | tf_op jit(solution)/shard_map/ppermute | solution.py:17
  175.8 11.1 %collective-permute-start.18 = (bf16[416,512]{1,0:T(8,128)(2,1)}, bf16[416,512]{1,0:T(8,128)(2,1)}, u32[]{:S(2)}, u32[]{:S(2)}) collective-permute-start(bf16[416,512]{1,0:T(8,128)(2,1)} %collective-permute-done.14.refs_2_), channel_id=1, source_target_pairs={{0,1},{1,0},{2,3},{3,2},{4,5},{5,4},{6,7},{7,6},{8,9},{9,8},{10,11... | collective-permute-start | bytes 1277960 | tf_op jit(solution)/shard_map/ppermute | solution.py:17
  176.3 10.6 %collective-permute-start.19 = (bf16[416,512]{1,0:T(8,128)(2,1)}, bf16[416,512]{1,0:T(8,128)(2,1)}, u32[]{:S(2)}, u32[]{:S(2)}) collective-permute-start(bf16[416,512]{1,0:T(8,128)(2,1)} %collective-permute-done.15.refs_3_), channel_id=1, source_target_pairs={{0,1},{1,0},{2,3},{3,2},{4,5},{5,4},{6,7},{7,6},{8,9},{9,8},{10,11... | collective-permute-start | bytes 1277960 | tf_op jit(solution)/shard_map/ppermute | solution.py:17
  177.0 9.6 %all-to-all-start.2 = ((f32[8,1,416]{2,1,0:T(1,128)}), f32[8,1,416]{2,1,0:T(1,128)S(1)}, u32[]{:S(2)}, u32[]{:S(2)}) async-start(f32[8,1,416]{2,1,0:T(1,128)} %broadcast_in_dim.24), calls=%async_computation.2 | async-start | bytes 32768 | tf_op jit(solution)/shard_map/all_to_all | solution.py:171
  182.6 25.7 %collective-permute-start.20 = (bf16[4096,128]{1,0:T(8,128)(2,1)S(1)}, bf16[4096,128]{1,0:T(8,128)(2,1)S(1)}, u32[]{:S(2)}, u32[]{:S(2)}) collective-permute-start(bf16[4096,128]{1,0:T(8,128)(2,1)S(1)} %slice.99.held_ref), channel_id=1, source_target_pairs={{0,128},{128,0},{1,129},{129,1},{2,130},{130,2},{3,131},{131,3},{4... | collective-permute-start | bytes 3145736 | tf_op jit(solution)/shard_map/ppermute | solution.py:175
  186.8 2.5 %copy-start = (bf16[4096,640]{1,0:T(8,128)(2,1)S(1)}, bf16[4096,640]{1,0:T(8,128)(2,1)}, u32[]{:S(2)}) copy-start(bf16[4096,640]{1,0:T(8,128)(2,1)} %all-gather.5.cloned.1.call-done.refs_9_) | copy-start | bytes 15728644
  208.9 3.5 %collective-permute-start.21 = (bf16[4,384,512]{2,1,0:T(8,128)(2,1)S(1)}, bf16[4,384,512]{2,1,0:T(8,128)(2,1)S(1)}, u32[]{:S(2)}, u32[]{:S(2)}) collective-permute-start(bf16[4,384,512]{2,1,0:T(8,128)(2,1)S(1)} %shares.6), channel_id=1, source_target_pairs={{0,1},{1,0},{2,3},{3,2},{4,5},{5,4},{6,7},{7,6},{8,9},{9,8},{10,11... | collective-permute-start | bytes 4718600 | tf_op jit(solution)/shard_map/ppermute | solution.py:17
  213.0 21.5 %copy-start.3 = (f32[416,512]{1,0:T(8,128)S(1)}, f32[416,512]{1,0:T(8,128)}, u32[]{:S(2)}) copy-start(f32[416,512]{1,0:T(8,128)} %copy-done.2) | copy-start | bytes 2555908
  213.1 13.7 %collective-permute-start.22 = (bf16[384,512]{1,0:T(8,128)(2,1)S(1)}, bf16[384,512]{1,0:T(8,128)(2,1)S(1)}, u32[]{:S(2)}, u32[]{:S(2)}) collective-permute-start(bf16[384,512]{1,0:T(8,128)(2,1)S(1)} %get-tuple-element.24), channel_id=1, source_target_pairs={{0,4},{1,5},{2,6},{3,7},{4,0},{5,1},{6,2},{7,3},{8,12},{9,13},{10,... | collective-permute-start | bytes 1179656 | tf_op jit(solution)/shard_map/ppermute | solution.py:13
  216.3 17.9 %collective-permute-start.23 = (bf16[384,512]{1,0:T(8,128)(2,1)S(1)}, bf16[384,512]{1,0:T(8,128)(2,1)S(1)}, u32[]{:S(2)}, u32[]{:S(2)}) collective-permute-start(bf16[384,512]{1,0:T(8,128)(2,1)S(1)} %get-tuple-element.26), channel_id=1, source_target_pairs={{0,2},{1,3},{2,4},{3,5},{4,6},{5,7},{6,0},{7,1},{8,10},{9,11},{10,... | collective-permute-start | bytes 1179656 | tf_op jit(solution)/shard_map/ppermute | solution.py:13
  216.9 17.6 %collective-permute-start.24 = (bf16[384,512]{1,0:T(8,128)(2,1)S(1)}, bf16[384,512]{1,0:T(8,128)(2,1)S(1)}, u32[]{:S(2)}, u32[]{:S(2)}) collective-permute-start(bf16[384,512]{1,0:T(8,128)(2,1)S(1)} %get-tuple-element.25), channel_id=1, source_target_pairs={{0,6},{1,7},{2,0},{3,1},{4,2},{5,3},{6,4},{7,5},{8,14},{9,15},{10,... | collective-permute-start | bytes 1179656 | tf_op jit(solution)/shard_map/ppermute | solution.py:13
Sparse Core Ops, SparseCore 0:
  9.7 92.0 all-gather.2
  103.6 75.1 all-gather.4
where the time goes:
time: 245 us; the launch traced here: 242 us
  waiting for transfers between devices  147 us (60%)
  starting transfers between devices  39.9 us (16%)
  Pallas kernels  16.1 us (7%)
  between operations  13.9 us (6%)
  local copies, waits for them, and re-layouts  12.9 us (5%)
  blocking collectives  7.82 us (3%)
  other arithmetic  4.39 us (2%)
    ppermute x12, waiting for transfers between devices, shifted(): lax.ppermute(value, axis, [(i, (i + steps) % count) for i in range(count)])  70.8 us
    all_gather x2, waiting for transfers between devices, shards(): taken.append(lax.all_gather(rows, 'sp', axis=0, tiled=True))  50.5 us
    ppermute x12, starting transfers between devices, shifted(): lax.ppermute(value, axis, [(i, (i + steps) % count) for i in range(count)])  19.6 us
    all_to_all x3, waiting for transfers between devices, over_lanes(): return lax.all_to_all(everyone, 'tp', 0, 0, tiled=True).sum(axis=0)  13.3 us
    all_to_all x3, starting transfers between devices, over_lanes(): return lax.all_to_all(everyone, 'tp', 0, 0, tiled=True).sum(axis=0)  12.4 us
    pallas_call x2, Pallas kernels, project(): pl.pallas_call(kernel, out_shape=jax.ShapeDtypeStruct((tokens, width), jn...  8.92 us
    all_to_all x1, blocking collectives, over_lanes(): return lax.all_to_all(everyone, 'tp', 0, 0, tiled=True).sum(axis=0)  7.82 us
    ppermute x10, waiting for transfers between devices, swapped(): lax.ppermute(value, 'tp', [(i, i ^ 1) for i in range(lax.axis_size('tp'))])  6.98 us
  transfers between devices with their start and end apart: 30, of which 17 were waited for; matrix products, arithmetic and copies ran while one was open for 3% of the time, Pallas kernels for 6%

commit v1 on v0

--- a/solution.py
+++ b/solution.py
@@ -35,41 +35,46 @@
     offsets = offsets_of(count)[::-1]
 
     def kernel(*refs):
-        blocks, (inv_ref, w_ref, out_ref, held, arrived) = refs[:count], refs[count:]
+        blocks, (inv_ref, w_ref, out_ref, near, held, near_in, held_in) = refs[:count], refs[count:]
         lane = lax.axis_index("tp")
         other = lane + 1 - 2 * (lane % 2)
         copies = []
         for i in range(count):
             base = lane if i < len(offsets) else other
             at = (base + offsets[i % len(offsets)] + count) % count
+            rows_of = w_ref.at[pl.ds(pl.multiple_of(at * size, size), size), pl.ds(0, 2 * width)]
             copies.append(
-                pltpu.make_async_copy(
-                    w_ref.at[pl.ds(pl.multiple_of(at * size, size), size), pl.ds(0, 2 * width)],
-                    held.at[i],
-                    arrived.at[i],
+                (
+                    pltpu.make_async_copy(blocks[i], near.at[i], near_in.at[i]),
+                    pltpu.make_async_copy(rows_of, held.at[i], held_in.at[i]),
                 )
             )
-            copies[-1].start()
+            for copy in copies[-1]:
+                copy.start()
         total = None
         for i in range(count):
-            copies[i].wait()
-            part = jnp.dot(blocks[i][...], held[i], preferred_element_type=jnp.float32)
+            for copy in copies[i]:
+                copy.wait()
+            part = jnp.dot(near[i], held[i], preferred_element_type=jnp.float32)
             total = part if total is None else total + part
         inv = inv_ref[...]
         value, gate = total[:, :width] * inv, total[:, width:] * inv
         out_ref[...] = (value * jax.nn.sigmoid(gate)).astype(out_ref.dtype)
 
     whole = pl.BlockSpec(memory_space=pltpu.VMEM)
+    apart = pl.BlockSpec(memory_space=pl.ANY)
     return pl.pallas_call(
         kernel,
         out_shape=jax.ShapeDtypeStruct((tokens, width), jnp.bfloat16),
-        in_specs=[whole] * (count + 1) + [pl.BlockSpec(memory_space=pl.ANY)],
+        in_specs=[apart] * count + [whole, apart],
         out_specs=whole,
         scratch_shapes=[
+            pltpu.VMEM((count, tokens, size), jnp.bfloat16),
             pltpu.VMEM((count, size, 2 * width), jnp.bfloat16),
             pltpu.SemaphoreType.DMA((count,)),
+            pltpu.SemaphoreType.DMA((count,)),
         ],
-        compiler_params=pltpu.CompilerParams(vmem_limit_bytes=24 << 20),
+        compiler_params=pltpu.CompilerParams(vmem_limit_bytes=50 << 20),
         cost_estimate=pl.CostEstimate(
             flops=4 * tokens * size * count * width,
             bytes_accessed=4 * size * count * width,
@@ -83,21 +88,17 @@
     total_rows, width = gated.shape
     tokens = total_rows - lead
     reach = taps.shape[0] - 1
-    tile = 32
+    tile = 64 if tokens % 64 == 0 else 32
     lanes = 128
 
     def kernel(gated_ref, taps_ref, out_ref, wide):
         wide[...] = gated_ref[...].astype(jnp.float32)
 
-        @pl.loop(0, tokens // tile)
-        def _(index):
-            start = pl.multiple_of(index * tile, tile)
+        for start in range(0, tokens, tile):
             for lane in range(0, width, lanes):
-                rows = wide[pl.ds(start, tile + lead), pl.ds(lane, lanes)]
                 total = None
                 for k in range(reach + 1):
-                    first = lead - reach + k
-                    window = lax.slice_in_dim(rows, first, first + tile, axis=0)
+                    window = wide[pl.ds(start + lead - reach + k, tile), pl.ds(lane, lanes)]
                     part = taps_ref[pl.ds(k, 1), pl.ds(lane, lanes)] * window
                     total = part if total is None else total + part
                 out_ref[pl.ds(start, tile), pl.ds(lane, lanes)] = total

time: 245 us -> 242 us (0.988)
  local copies, waits for them, and re-layouts: 12.9 us -> 7.99 us
  waiting for transfers between devices: 147 us -> 150 us
    unnamed x22 -> x18, local copies, waits for them, and re-layouts: 5.01 us -> 0.05 us
    ppermute x2, waiting for transfers between devices: 3.94 us -> 7.23 us  [fetched_rows(): lax.ppermute(held, 'grp', [(i, i ^ 1) for i in range(lax.axis_size('grp'))])]
  transfers between devices with their start and end apart: 30 -> 30, of which waited for: 17 -> 20; matrix products, arithmetic and copies ran while one was open for 3% -> 3% of each run, Pallas kernels for 6% -> 5%
where the time goes in v1:
time: 242 us; the launch traced here: 239 us
  waiting for transfers between devices  150 us (62%)
  starting transfers between devices  40.7 us (17%)
  Pallas kernels  14.1 us (6%)
  between operations  13.9 us (6%)
  blocking collectives  8.04 us (3%)
  local copies, waits for them, and re-layouts  7.99 us (3%)
  other arithmetic  4.38 us (2%)
    ppermute x12, waiting for transfers between devices, shifted(): lax.ppermute(value, axis, [(i, (i + steps) % count) for i in range(count)])  69.3 us
    all_gather x2, waiting for transfers between devices, shards(): taken.append(lax.all_gather(rows, 'sp', axis=0, tiled=True))  51.3 us
    ppermute x12, starting transfers between devices, shifted(): lax.ppermute(value, axis, [(i, (i + steps) % count) for i in range(count)])  21.8 us
    all_to_all x3, waiting for transfers between devices, over_lanes(): return lax.all_to_all(everyone, 'tp', 0, 0, tiled=True).sum(axis=0)  13.3 us
    all_to_all x3, starting transfers between devices, over_lanes(): return lax.all_to_all(everyone, 'tp', 0, 0, tiled=True).sum(axis=0)  12.3 us
    pallas_call x2, Pallas kernels, project(): pl.pallas_call(kernel, out_shape=jax.ShapeDtypeStruct((tokens, width), jn...  8.19 us
    all_to_all x1, blocking collectives, over_lanes(): return lax.all_to_all(everyone, 'tp', 0, 0, tiled=True).sum(axis=0)  8.04 us
    ppermute x2, waiting for transfers between devices, fetched_rows(): lax.ppermute(held, 'grp', [(i, i ^ 1) for i in range(lax.axis_size('grp'))])  7.23 us
  transfers between devices with their start and end apart: 30, of which 20 were waited for; matrix products, arithmetic and copies ran while one was open for 3% of the time, Pallas kernels for 5%

profile of v1, /device:TPU:40, one launch (start us, length us, event | category | flops | bytes accessed | tf_op | source)
XLA Modules:
  0.0 239.2 jit_solution(1206886122253057838)
XLA Ops:
  6.6 1.0 fusion.16
  7.6 1.2 slice_bitcast_fusion.6
  8.8 0.8 pad_maximum_fusion
  9.7 0.7 pad_maximum_fusion.1
  10.5 4.7 %collective-permute-start = (bf16[64,512]{1,0:T(8,128)(2,1)S(1)}, bf16[64,512]{1,0:T(8,128)(2,1)S(1)}, u32[]{:S(2)}, u32[]{:S(2)}) collective-permute-start(bf16[64,512]{1,0:T(8,128)(2,1)S(1)} %slice.69), channel_id=1, source_target_pairs={{0,8},{8,16},{16,24},{24,32},{32,40},{40,48},{48,56},{56,64},{64,7... | collective-permute-start | bytes 196616 | tf_op jit(solution)/shard_map/ppermute | solution.py:23
  15.3 1.9 collective-permute-done
  17.1 0.2 multiply_reduce_fusion
  17.4 1.7 collective-permute-start.1
  19.1 1.7 collective-permute-start.2
  20.8 2.0 collective-permute-start.3
  22.8 8.3 %collective-permute-done.1.refs_1_ = bf16[448,512]{1,0:T(8,128)(2,1)S(1)} collective-permute-done((bf16[448,512]{1,0:T(8,128)(2,1)S(1)}, bf16[448,512]{1,0:T(8,128)(2,1)S(1)}, u32[]{:S(2)}, u32[]{:S(2)}) %collective-permute-start.1) | collective-permute-done | bytes 458784 | tf_op jit(solution)/shard_map/ppermute | solution.py:13
  31.1 8.5 %collective-permute-done.2.refs_2_ = bf16[448,512]{1,0:T(8,128)(2,1)} collective-permute-done((bf16[448,512]{1,0:T(8,128)(2,1)S(1)}, bf16[448,512]{1,0:T(8,128)(2,1)}, u32[]{:S(2)}, u32[]{:S(2)}) %collective-permute-start.2) | collective-permute-done | bytes 458784 | tf_op jit(solution)/shard_map/ppermute | solution.py:13
  39.6 1.8 collective-permute-done.3.refs_3_
  41.5 0.6 broadcast_in_dim.22
  42.2 3.7 %all-to-all-start = ((f32[8,1,448]{2,1,0:T(1,128)}), f32[8,1,448]{2,1,0:T(1,128)S(1)}, u32[]{:S(2)}, u32[]{:S(2)}) async-start(f32[8,1,448]{2,1,0:T(1,128)} %broadcast_in_dim.22), calls=%async_computation | async-start | bytes 32768 | tf_op jit(solution)/shard_map/all_to_all | solution.py:172
  45.9 5.3 %all-to-all-done = f32[8,1,448]{2,1,0:T(1,128)S(1)} async-done(((f32[8,1,448]{2,1,0:T(1,128)}), f32[8,1,448]{2,1,0:T(1,128)S(1)}, u32[]{:S(2)}, u32[]{:S(2)}) %all-to-all-start) | async-done | bytes 14368 | tf_op jit(solution)/shard_map/all_to_all | solution.py:172
  51.4 50.4 %all-gather.3.cloned.1.call-done.refs_9_ = bf16[4096,640]{1,0:T(8,128)(2,1)} async-done(((bf16[256,640]{1,0:T(8,128)(2,1)}), bf16[4096,640]{1,0:T(8,128)(2,1)}) %all-gather.3.cloned.1.call-update) | async-done | bytes 5242896 | tf_op jit(solution)/shard_map/all_gather | solution.py:195
  101.8 1.3 slice.95.held_ref
  103.2 0.6 collective-permute-start.8
  103.8 4.2 %project.2.gated_ref = bf16[448,256]{1,0:T(8,128)(2,1)S(1)} custom-call(bf16[448,512]{1,0:T(8,128)(2,1)S(1)} %get-tuple-element.28.refs_0_, bf16[448,512]{1,0:T(8,128)(2,1)S(1)} %collective-permute-done.1.refs_1_, bf16[448,512]{1,0:T(8,128)(2,1)} %collective-permute-done.2.refs_2_, bf16[448,512]{1,0:T(8,128)(2,1)} %collective-permute-done.3.refs_3_, ...), custom_call_target="tpu_custom_call" | custom-call | flops 1879048192 | bytes 4194304 | tf_op jit(solution)/shard_map/project/pallas_call | solution.py:66
  108.0 1.9 depthwise.2
  109.9 0.2 fusion.13
  110.2 0.6 broadcast_in_dim.23
  110.8 4.5 %all-to-all-start.1 = ((f32[8,2,416]{2,1,0:T(2,128)}), f32[8,2,416]{2,1,0:T(2,128)S(1)}, u32[]{:S(2)}, u32[]{:S(2)}) async-start(f32[8,2,416]{2,1,0:T(2,128)} %broadcast_in_dim.23), calls=%async_computation.1 | async-start | bytes 65536 | tf_op jit(solution)/shard_map/all_to_all | solution.py:172
  115.3 5.4 %all-to-all-done.1 = f32[8,2,416]{2,1,0:T(2,128)S(1)} async-done(((f32[8,2,416]{2,1,0:T(2,128)}), f32[8,2,416]{2,1,0:T(2,128)S(1)}, u32[]{:S(2)}, u32[]{:S(2)}) %all-to-all-start.1) | async-done | bytes 26656 | tf_op jit(solution)/shard_map/all_to_all | solution.py:172
  120.8 0.2 multiply_convert_fusion.2.mixed_ref
  121.0 0.6 shares.4
  121.6 0.3 collective-permute-start.9
  122.0 3.6 %collective-permute-done.9.refs_0_ = bf16[4,416,512]{2,1,0:T(8,128)(2,1)S(1)} collective-permute-done((bf16[4,416,512]{2,1,0:T(8,128)(2,1)S(1)}, bf16[4,416,512]{2,1,0:T(8,128)(2,1)S(1)}, u32[]{:S(2)}, u32[]{:S(2)}) %collective-permute-start.9) | collective-permute-done | bytes 1703968 | tf_op jit(solution)/shard_map/ppermute | solution.py:17
  125.5 0.6 shares.5
  126.2 0.9 slice_bitcast_fusion.2
  127.0 2.7 %collective-permute-start.10 = (bf16[416,512]{1,0:T(8,128)(2,1)}, bf16[416,512]{1,0:T(8,128)(2,1)S(1)}, u32[]{:S(2)}, u32[]{:S(2)}) collective-permute-start(bf16[416,512]{1,0:T(8,128)(2,1)} %get-tuple-element.21), channel_id=1, source_target_pairs={{0,4},{1,5},{2,6},{3,7},{4,0},{5,1},{6,2},{7,3},{8,12},{9,13},{10,... | collective-permute-start | bytes 1277960 | tf_op jit(solution)/shard_map/ppermute | solution.py:13
  129.7 0.6 collective-permute-start.11
  130.3 2.7 %collective-permute-start.12 = (bf16[416,512]{1,0:T(8,128)(2,1)S(1)}, bf16[416,512]{1,0:T(8,128)(2,1)S(1)}, u32[]{:S(2)}, u32[]{:S(2)}) collective-permute-start(bf16[416,512]{1,0:T(8,128)(2,1)S(1)} %get-tuple-element.22), channel_id=1, source_target_pairs={{0,6},{1,7},{2,0},{3,1},{4,2},{5,3},{6,4},{7,5},{8,14},{9,15},{10,... | collective-permute-start | bytes 1277960 | tf_op jit(solution)/shard_map/ppermute | solution.py:13
  133.0 8.4 %collective-permute-done.10 = bf16[416,512]{1,0:T(8,128)(2,1)S(1)} collective-permute-done((bf16[416,512]{1,0:T(8,128)(2,1)}, bf16[416,512]{1,0:T(8,128)(2,1)S(1)}, u32[]{:S(2)}, u32[]{:S(2)}) %collective-permute-start.10) | collective-permute-done | bytes 426016 | tf_op jit(solution)/shard_map/ppermute | solution.py:13
  141.5 8.3 %collective-permute-done.11 = bf16[416,512]{1,0:T(8,128)(2,1)S(1)} collective-permute-done((bf16[416,512]{1,0:T(8,128)(2,1)S(1)}, bf16[416,512]{1,0:T(8,128)(2,1)S(1)}, u32[]{:S(2)}, u32[]{:S(2)}) %collective-permute-start.11) | collective-permute-done | bytes 426016 | tf_op jit(solution)/shard_map/ppermute | solution.py:13
  149.7 0.4 multiply_reduce_fusion.1
  150.3 1.3 collective-permute-start.13
  151.6 2.0 collective-permute-start.14
  153.6 0.6 collective-permute-start.15
  154.2 9.5 %collective-permute-done.13.refs_1_ = bf16[416,512]{1,0:T(8,128)(2,1)S(1)} collective-permute-done((bf16[416,512]{1,0:T(8,128)(2,1)S(1)}, bf16[416,512]{1,0:T(8,128)(2,1)S(1)}, u32[]{:S(2)}, u32[]{:S(2)}) %collective-permute-start.13) | collective-permute-done | bytes 426016 | tf_op jit(solution)/shard_map/ppermute | solution.py:13
  163.7 8.2 %collective-permute-done.14.refs_2_ = bf16[416,512]{1,0:T(8,128)(2,1)} collective-permute-done((bf16[416,512]{1,0:T(8,128)(2,1)S(1)}, bf16[416,512]{1,0:T(8,128)(2,1)}, u32[]{:S(2)}, u32[]{:S(2)}) %collective-permute-start.14) | collective-permute-done | bytes 426016 | tf_op jit(solution)/shard_map/ppermute | solution.py:13
  171.9 1.4 collective-permute-done.15.refs_3_
  173.3 0.6 broadcast_in_dim.24
  173.9 4.2 %all-to-all-start.2 = ((f32[8,1,416]{2,1,0:T(1,128)}), f32[8,1,416]{2,1,0:T(1,128)S(1)}, u32[]{:S(2)}, u32[]{:S(2)}) async-start(f32[8,1,416]{2,1,0:T(1,128)} %broadcast_in_dim.24), calls=%async_computation.2 | async-start | bytes 32768 | tf_op jit(solution)/shard_map/all_to_all | solution.py:172
  178.1 0.9 all-gather.5.cloned.1.call-done.refs_9_
  178.9 1.3 slice.99.held_ref
  180.2 0.7 collective-permute-start.20
  180.9 2.5 %all-to-all-done.2 = f32[8,1,416]{2,1,0:T(1,128)S(1)} async-done(((f32[8,1,416]{2,1,0:T(1,128)}), f32[8,1,416]{2,1,0:T(1,128)S(1)}, u32[]{:S(2)}, u32[]{:S(2)}) %all-to-all-start.2) | async-done | bytes 13344 | tf_op jit(solution)/shard_map/all_to_all | solution.py:172
  183.6 4.0 %project.3.gated_ref = bf16[416,256]{1,0:T(8,128)(2,1)S(1)} custom-call(bf16[416,512]{1,0:T(8,128)(2,1)S(1)} %multiply_convert_fusion.1.refs_0_, bf16[416,512]{1,0:T(8,128)(2,1)S(1)} %collective-permute-done.13.refs_1_, bf16[416,512]{1,0:T(8,128)(2,1)} %collective-permute-done.14.refs_2_, bf16[416,512]{1,0:T(8,128)(2,1)} %collective-permute-done.15.refs_3_, ...), custom_call_target="tpu_custom_call" | custom-call | flops 1744830464 | bytes 4194304 | tf_op jit(solution)/shard_map/project/pallas_call | solution.py:66
  187.6 1.6 depthwise.3
  189.5 8.0 %all_to_all.22 = f32[8,2,384]{2,1,0:T(2,128)S(1)} all-to-all(f32[8,2,384]{2,1,0:T(2,128)S(1)} %broadcast_in_dim.25), channel_id=1, replica_groups=mesh['grp'=2,'sp'=16,'tp'=8] {'tp'}, dimensions={0} | all-to-all | bytes 49152 | tf_op jit(solution)/shard_map/all_to_all | solution.py:172
  197.6 0.2 multiply_convert_fusion.3.mixed_ref
  197.8 7.2 %collective-permute-done.20.fetched_ref = bf16[4096,128]{1,0:T(8,128)(2,1)S(1)} collective-permute-done((bf16[4096,128]{1,0:T(8,128)(2,1)S(1)}, bf16[4096,128]{1,0:T(8,128)(2,1)S(1)}, u32[]{:S(2)}, u32[]{:S(2)}) %collective-permute-start.20) | collective-permute-done | bytes 1048608 | tf_op jit(solution)/shard_map/ppermute | solution.py:176
  205.1 0.6 shares.6
  205.8 3.4 %collective-permute-done.21.refs_0_ = bf16[4,384,512]{2,1,0:T(8,128)(2,1)S(1)} collective-permute-done((bf16[4,384,512]{2,1,0:T(8,128)(2,1)S(1)}, bf16[4,384,512]{2,1,0:T(8,128)(2,1)S(1)}, u32[]{:S(2)}, u32[]{:S(2)}) %collective-permute-start.21) | collective-permute-done | bytes 1572896 | tf_op jit(solution)/shard_map/ppermute | solution.py:17
  209.2 0.6 shares.7
  209.9 3.3 %collective-permute-start.22 = (bf16[384,512]{1,0:T(8,128)(2,1)S(1)}, bf16[384,512]{1,0:T(8,128)(2,1)S(1)}, u32[]{:S(2)}, u32[]{:S(2)}) collective-permute-start(bf16[384,512]{1,0:T(8,128)(2,1)S(1)} %get-tuple-element.24), channel_id=1, source_target_pairs={{0,4},{1,5},{2,6},{3,7},{4,0},{5,1},{6,2},{7,3},{8,12},{9,13},{10,... | collective-permute-start | bytes 1179656 | tf_op jit(solution)/shard_map/ppermute | solution.py:13
  213.2 0.6 collective-permute-start.23
  213.7 2.7 %collective-permute-start.24 = (bf16[384,512]{1,0:T(8,128)(2,1)S(1)}, bf16[384,512]{1,0:T(8,128)(2,1)S(1)}, u32[]{:S(2)}, u32[]{:S(2)}) collective-permute-start(bf16[384,512]{1,0:T(8,128)(2,1)S(1)} %get-tuple-element.25), channel_id=1, source_target_pairs={{0,6},{1,7},{2,0},{3,1},{4,2},{5,3},{6,4},{7,5},{8,14},{9,15},{10,... | collective-permute-start | bytes 1179656 | tf_op jit(solution)/shard_map/ppermute | solution.py:13
  216.4 7.2 %collective-permute-done.22 = bf16[384,512]{1,0:T(8,128)(2,1)S(1)} collective-permute-done((bf16[384,512]{1,0:T(8,128)(2,1)S(1)}, bf16[384,512]{1,0:T(8,128)(2,1)S(1)}, u32[]{:S(2)}, u32[]{:S(2)}) %collective-permute-start.22) | collective-permute-done | bytes 393248 | tf_op jit(solution)/shard_map/ppermute | solution.py:13
  223.6 7.6 %collective-permute-done.23 = bf16[384,512]{1,0:T(8,128)(2,1)S(1)} collective-permute-done((bf16[384,512]{1,0:T(8,128)(2,1)S(1)}, bf16[384,512]{1,0:T(8,128)(2,1)S(1)}, u32[]{:S(2)}, u32[]{:S(2)}) %collective-permute-start.23) | collective-permute-done | bytes 393248 | tf_op jit(solution)/shard_map/ppermute | solution.py:13
  231.1 0.2 collective-permute-done.24
  231.3 1.0 fusion.7
  (70 shorter events, 1.5 us)
Async XLA Ops:
  6.5 95.3 %all-gather.3.cloned.1.call-start = ((), (), s32[]{:S(2)}) async-start(), calls=%async_computation.4 | async-start | bytes 5570560 | tf_op jit(solution)/shard_map/all_gather | solution.py:195
  7.6 3.0 %copy-start.2 = (bf16[384,512]{1,0:T(8,128)(2,1)S(1)}, bf16[384,512]{1,0:T(8,128)(2,1)}, u32[]{:S(2)}) copy-start(bf16[384,512]{1,0:T(8,128)(2,1)} %param.8) | copy-start | bytes 1179652
  7.6 7.7 %copy-start.5 = (f32[2,512]{1,0:T(2,128)S(1)}, f32[2,512]{1,0:T(2,128)}, u32[]{:S(2)}) copy-start(f32[2,512]{1,0:T(2,128)} %param.9) | copy-start | bytes 12292
  8.8 32.7 %copy-start.4 = (f32[2,31,256]{2,0,1:T(2,128)S(1)}, f32[2,31,256]{2,0,1:T(2,128)}, u32[]{:S(2)}) copy-start(f32[2,31,256]{2,0,1:T(2,128)} %param.12) | copy-start | bytes 190468
  8.8 37.1 %copy-start.6 = (f32[2,256]{1,0:T(2,128)S(1)}, f32[2,256]{1,0:T(2,128)}, u32[]{:S(2)}) copy-start(f32[2,256]{1,0:T(2,128)} %param.13) | copy-start | bytes 6148
  9.6 169.3 %all-gather.5.cloned.1.call-start = ((), (), s32[]{:S(2)}) async-start(), calls=%async_computation.5 | async-start | bytes 5570560 | tf_op jit(solution)/shard_map/all_gather | solution.py:195
  10.5 6.6 %collective-permute-start = (bf16[64,512]{1,0:T(8,128)(2,1)S(1)}, bf16[64,512]{1,0:T(8,128)(2,1)S(1)}, u32[]{:S(2)}, u32[]{:S(2)}) collective-permute-start(bf16[64,512]{1,0:T(8,128)(2,1)S(1)} %slice.69), channel_id=1, source_target_pairs={{0,8},{8,16},{16,24},{24,32},{32,40},{40,48},{48,56},{56,64},{64,7... | collective-permute-start | bytes 196616 | tf_op jit(solution)/shard_map/ppermute | solution.py:23
  17.4 13.8 %collective-permute-start.1 = (bf16[448,512]{1,0:T(8,128)(2,1)S(1)}, bf16[448,512]{1,0:T(8,128)(2,1)S(1)}, u32[]{:S(2)}, u32[]{:S(2)}) collective-permute-start(bf16[448,512]{1,0:T(8,128)(2,1)S(1)} %get-tuple-element.28.refs_0_), channel_id=1, source_target_pairs={{0,2},{1,3},{2,4},{3,5},{4,6},{5,7},{6,0},{7,1},{8,10},{9,11},{10,... | collective-permute-start | bytes 1376264 | tf_op jit(solution)/shard_map/ppermute | solution.py:13
  19.1 20.5 %collective-permute-start.2 = (bf16[448,512]{1,0:T(8,128)(2,1)S(1)}, bf16[448,512]{1,0:T(8,128)(2,1)}, u32[]{:S(2)}, u32[]{:S(2)}) collective-permute-start(bf16[448,512]{1,0:T(8,128)(2,1)S(1)} %get-tuple-element.28.refs_0_), channel_id=1, source_target_pairs={{0,6},{1,7},{2,0},{3,1},{4,2},{5,3},{6,4},{7,5},{8,14},{9,15},{10,... | collective-permute-start | bytes 1376264 | tf_op jit(solution)/shard_map/ppermute | solution.py:13
  20.8 20.7 %collective-permute-start.3 = (bf16[448,512]{1,0:T(8,128)(2,1)S(1)}, bf16[448,512]{1,0:T(8,128)(2,1)}, u32[]{:S(2)}, u32[]{:S(2)}) collective-permute-start(bf16[448,512]{1,0:T(8,128)(2,1)S(1)} %get-tuple-element.28.refs_0_), channel_id=1, source_target_pairs={{0,4},{1,5},{2,6},{3,7},{4,0},{5,1},{6,2},{7,3},{8,12},{9,13},{10,... | collective-permute-start | bytes 1376264 | tf_op jit(solution)/shard_map/ppermute | solution.py:13
  22.8 81.0 %collective-permute-start.4 = (bf16[448,512]{1,0:T(8,128)(2,1)S(1)}, bf16[448,512]{1,0:T(8,128)(2,1)}, u32[]{:S(2)}, u32[]{:S(2)}) collective-permute-start(bf16[448,512]{1,0:T(8,128)(2,1)S(1)} %get-tuple-element.28.refs_0_), channel_id=1, source_target_pairs={{0,1},{1,0},{2,3},{3,2},{4,5},{5,4},{6,7},{7,6},{8,9},{9,8},{10,11... | collective-permute-start | bytes 1376264 | tf_op jit(solution)/shard_map/ppermute | solution.py:17
  31.1 72.7 %collective-permute-start.5 = (bf16[448,512]{1,0:T(8,128)(2,1)S(1)}, bf16[448,512]{1,0:T(8,128)(2,1)}, u32[]{:S(2)}, u32[]{:S(2)}) collective-permute-start(bf16[448,512]{1,0:T(8,128)(2,1)S(1)} %collective-permute-done.1.refs_1_), channel_id=1, source_target_pairs={{0,1},{1,0},{2,3},{3,2},{4,5},{5,4},{6,7},{7,6},{8,9},{9,8},{10,11... | collective-permute-start | bytes 1376264 | tf_op jit(solution)/shard_map/ppermute | solution.py:17
  39.6 64.2 %collective-permute-start.6 = (bf16[448,512]{1,0:T(8,128)(2,1)}, bf16[448,512]{1,0:T(8,128)(2,1)}, u32[]{:S(2)}, u32[]{:S(2)}) collective-permute-start(bf16[448,512]{1,0:T(8,128)(2,1)} %collective-permute-done.2.refs_2_), channel_id=1, source_target_pairs={{0,1},{1,0},{2,3},{3,2},{4,5},{5,4},{6,7},{7,6},{8,9},{9,8},{10,11... | collective-permute-start | bytes 1376264 | tf_op jit(solution)/shard_map/ppermute | solution.py:17
  41.5 62.3 %collective-permute-start.7 = (bf16[448,512]{1,0:T(8,128)(2,1)}, bf16[448,512]{1,0:T(8,128)(2,1)}, u32[]{:S(2)}, u32[]{:S(2)}) collective-permute-start(bf16[448,512]{1,0:T(8,128)(2,1)} %collective-permute-done.3.refs_3_), channel_id=1, source_target_pairs={{0,1},{1,0},{2,3},{3,2},{4,5},{5,4},{6,7},{7,6},{8,9},{9,8},{10,11... | collective-permute-start | bytes 1376264 | tf_op jit(solution)/shard_map/ppermute | solution.py:17
  42.2 9.1 %all-to-all-start = ((f32[8,1,448]{2,1,0:T(1,128)}), f32[8,1,448]{2,1,0:T(1,128)S(1)}, u32[]{:S(2)}, u32[]{:S(2)}) async-start(f32[8,1,448]{2,1,0:T(1,128)} %broadcast_in_dim.22), calls=%async_computation | async-start | bytes 32768 | tf_op jit(solution)/shard_map/all_to_all | solution.py:172
  103.1 12.1 %copy-start.7 = (f32[2,256]{1,0:T(2,128)S(1)}, f32[2,256]{1,0:T(2,128)}, u32[]{:S(2)}) copy-start(f32[2,256]{1,0:T(2,128)} %param.14) | copy-start | bytes 6148
  103.2 17.8 %collective-permute-start.8 = (bf16[4096,128]{1,0:T(8,128)(2,1)S(1)}, bf16[4096,128]{1,0:T(8,128)(2,1)S(1)}, u32[]{:S(2)}, u32[]{:S(2)}) collective-permute-start(bf16[4096,128]{1,0:T(8,128)(2,1)S(1)} %slice.95.held_ref), channel_id=1, source_target_pairs={{0,128},{128,0},{1,129},{129,1},{2,130},{130,2},{3,131},{131,3},{4... | collective-permute-start | bytes 3145736 | tf_op jit(solution)/shard_map/ppermute | solution.py:176
  110.8 9.9 %all-to-all-start.1 = ((f32[8,2,416]{2,1,0:T(2,128)}), f32[8,2,416]{2,1,0:T(2,128)S(1)}, u32[]{:S(2)}, u32[]{:S(2)}) async-start(f32[8,2,416]{2,1,0:T(2,128)} %broadcast_in_dim.23), calls=%async_computation.1 | async-start | bytes 65536 | tf_op jit(solution)/shard_map/all_to_all | solution.py:172
  121.6 3.9 %collective-permute-start.9 = (bf16[4,416,512]{2,1,0:T(8,128)(2,1)S(1)}, bf16[4,416,512]{2,1,0:T(8,128)(2,1)S(1)}, u32[]{:S(2)}, u32[]{:S(2)}) collective-permute-start(bf16[4,416,512]{2,1,0:T(8,128)(2,1)S(1)} %shares.4), channel_id=1, source_target_pairs={{0,1},{1,0},{2,3},{3,2},{4,5},{5,4},{6,7},{7,6},{8,9},{9,8},{10,11... | collective-permute-start | bytes 5111816 | tf_op jit(solution)/shard_map/ppermute | solution.py:17
  126.2 6.8 %copy-start.3 = (bf16[384,512]{1,0:T(8,128)(2,1)S(1)}, bf16[384,512]{1,0:T(8,128)(2,1)}, u32[]{:S(2)}) copy-start(bf16[384,512]{1,0:T(8,128)(2,1)} %param.8) | copy-start | bytes 1179652
  127.0 14.4 %collective-permute-start.10 = (bf16[416,512]{1,0:T(8,128)(2,1)}, bf16[416,512]{1,0:T(8,128)(2,1)S(1)}, u32[]{:S(2)}, u32[]{:S(2)}) collective-permute-start(bf16[416,512]{1,0:T(8,128)(2,1)} %get-tuple-element.21), channel_id=1, source_target_pairs={{0,4},{1,5},{2,6},{3,7},{4,0},{5,1},{6,2},{7,3},{8,12},{9,13},{10,... | collective-permute-start | bytes 1277960 | tf_op jit(solution)/shard_map/ppermute | solution.py:13
  129.7 20.0 %collective-permute-start.11 = (bf16[416,512]{1,0:T(8,128)(2,1)S(1)}, bf16[416,512]{1,0:T(8,128)(2,1)S(1)}, u32[]{:S(2)}, u32[]{:S(2)}) collective-permute-start(bf16[416,512]{1,0:T(8,128)(2,1)S(1)} %get-tuple-element.23), channel_id=1, source_target_pairs={{0,2},{1,3},{2,4},{3,5},{4,6},{5,7},{6,0},{7,1},{8,10},{9,11},{10,... | collective-permute-start | bytes 1277960 | tf_op jit(solution)/shard_map/ppermute | solution.py:13
  130.3 19.5 %collective-permute-start.12 = (bf16[416,512]{1,0:T(8,128)(2,1)S(1)}, bf16[416,512]{1,0:T(8,128)(2,1)S(1)}, u32[]{:S(2)}, u32[]{:S(2)}) collective-permute-start(bf16[416,512]{1,0:T(8,128)(2,1)S(1)} %get-tuple-element.22), channel_id=1, source_target_pairs={{0,6},{1,7},{2,0},{3,1},{4,2},{5,3},{6,4},{7,5},{8,14},{9,15},{10,... | collective-permute-start | bytes 1277960 | tf_op jit(solution)/shard_map/ppermute | solution.py:13
  150.2 23.1 %copy-start = (f32[416,512]{1,0:T(8,128)}, f32[416,512]{1,0:T(8,128)S(1)}, u32[]{:S(2)}) copy-start(f32[416,512]{1,0:T(8,128)S(1)} %get-tuple-element.20) | copy-start | bytes 2555908
  150.3 13.4 %collective-permute-start.13 = (bf16[416,512]{1,0:T(8,128)(2,1)S(1)}, bf16[416,512]{1,0:T(8,128)(2,1)S(1)}, u32[]{:S(2)}, u32[]{:S(2)}) collective-permute-start(bf16[416,512]{1,0:T(8,128)(2,1)S(1)} %multiply_convert_fusion.1.refs_0_), channel_id=1, source_target_pairs={{0,2},{1,3},{2,4},{3,5},{4,6},{5,7},{6,0},{7,1},{8,10},{9,11},{10,... | collective-permute-start | bytes 1277960 | tf_op jit(solution)/shard_map/ppermute | solution.py:13
  151.6 20.3 %collective-permute-start.14 = (bf16[416,512]{1,0:T(8,128)(2,1)S(1)}, bf16[416,512]{1,0:T(8,128)(2,1)}, u32[]{:S(2)}, u32[]{:S(2)}) collective-permute-start(bf16[416,512]{1,0:T(8,128)(2,1)S(1)} %multiply_convert_fusion.1.refs_0_), channel_id=1, source_target_pairs={{0,6},{1,7},{2,0},{3,1},{4,2},{5,3},{6,4},{7,5},{8,14},{9,15},{10,... | collective-permute-start | bytes 1277960 | tf_op jit(solution)/shard_map/ppermute | solution.py:13
  153.6 19.6 %collective-permute-start.15 = (bf16[416,512]{1,0:T(8,128)(2,1)S(1)}, bf16[416,512]{1,0:T(8,128)(2,1)}, u32[]{:S(2)}, u32[]{:S(2)}) collective-permute-start(bf16[416,512]{1,0:T(8,128)(2,1)S(1)} %multiply_convert_fusion.1.refs_0_), channel_id=1, source_target_pairs={{0,4},{1,5},{2,6},{3,7},{4,0},{5,1},{6,2},{7,3},{8,12},{9,13},{10,... | collective-permute-start | bytes 1277960 | tf_op jit(solution)/shard_map/ppermute | solution.py:13
  154.2 29.4 %collective-permute-start.16 = (bf16[416,512]{1,0:T(8,128)(2,1)S(1)}, bf16[416,512]{1,0:T(8,128)(2,1)}, u32[]{:S(2)}, u32[]{:S(2)}) collective-permute-start(bf16[416,512]{1,0:T(8,128)(2,1)S(1)} %multiply_convert_fusion.1.refs_0_), channel_id=1, source_target_pairs={{0,1},{1,0},{2,3},{3,2},{4,5},{5,4},{6,7},{7,6},{8,9},{9,8},{10,11... | collective-permute-start | bytes 1277960 | tf_op jit(solution)/shard_map/ppermute | solution.py:17
  163.7 19.9 %collective-permute-start.17 = (bf16[416,512]{1,0:T(8,128)(2,1)S(1)}, bf16[416,512]{1,0:T(8,128)(2,1)}, u32[]{:S(2)}, u32[]{:S(2)}) collective-permute-start(bf16[416,512]{1,0:T(8,128)(2,1)S(1)} %collective-permute-done.13.refs_1_), channel_id=1, source_target_pairs={{0,1},{1,0},{2,3},{3,2},{4,5},{5,4},{6,7},{7,6},{8,9},{9,8},{10,11... | collective-permute-start | bytes 1277960 | tf_op jit(solution)/shard_map/ppermute | solution.py:17
  171.9 11.8 %collective-permute-start.18 = (bf16[416,512]{1,0:T(8,128)(2,1)}, bf16[416,512]{1,0:T(8,128)(2,1)}, u32[]{:S(2)}, u32[]{:S(2)}) collective-permute-start(bf16[416,512]{1,0:T(8,128)(2,1)} %collective-permute-done.14.refs_2_), channel_id=1, source_target_pairs={{0,1},{1,0},{2,3},{3,2},{4,5},{5,4},{6,7},{7,6},{8,9},{9,8},{10,11... | collective-permute-start | bytes 1277960 | tf_op jit(solution)/shard_map/ppermute | solution.py:17
  173.3 10.4 %collective-permute-start.19 = (bf16[416,512]{1,0:T(8,128)(2,1)}, bf16[416,512]{1,0:T(8,128)(2,1)}, u32[]{:S(2)}, u32[]{:S(2)}) collective-permute-start(bf16[416,512]{1,0:T(8,128)(2,1)} %collective-permute-done.15.refs_3_), channel_id=1, source_target_pairs={{0,1},{1,0},{2,3},{3,2},{4,5},{5,4},{6,7},{7,6},{8,9},{9,8},{10,11... | collective-permute-start | bytes 1277960 | tf_op jit(solution)/shard_map/ppermute | solution.py:17
  173.9 9.5 %all-to-all-start.2 = ((f32[8,1,416]{2,1,0:T(1,128)}), f32[8,1,416]{2,1,0:T(1,128)S(1)}, u32[]{:S(2)}, u32[]{:S(2)}) async-start(f32[8,1,416]{2,1,0:T(1,128)} %broadcast_in_dim.24), calls=%async_computation.2 | async-start | bytes 32768 | tf_op jit(solution)/shard_map/all_to_all | solution.py:172
  180.2 24.8 %collective-permute-start.20 = (bf16[4096,128]{1,0:T(8,128)(2,1)S(1)}, bf16[4096,128]{1,0:T(8,128)(2,1)S(1)}, u32[]{:S(2)}, u32[]{:S(2)}) collective-permute-start(bf16[4096,128]{1,0:T(8,128)(2,1)S(1)} %slice.99.held_ref), channel_id=1, source_target_pairs={{0,128},{128,0},{1,129},{129,1},{2,130},{130,2},{3,131},{131,3},{4... | collective-permute-start | bytes 3145736 | tf_op jit(solution)/shard_map/ppermute | solution.py:176
  205.6 3.5 %collective-permute-start.21 = (bf16[4,384,512]{2,1,0:T(8,128)(2,1)S(1)}, bf16[4,384,512]{2,1,0:T(8,128)(2,1)S(1)}, u32[]{:S(2)}, u32[]{:S(2)}) collective-permute-start(bf16[4,384,512]{2,1,0:T(8,128)(2,1)S(1)} %shares.6), channel_id=1, source_target_pairs={{0,1},{1,0},{2,3},{3,2},{4,5},{5,4},{6,7},{7,6},{8,9},{9,8},{10,11... | collective-permute-start | bytes 4718600 | tf_op jit(solution)/shard_map/ppermute | solution.py:17
  209.8 21.5 %copy-start.1 = (f32[416,512]{1,0:T(8,128)S(1)}, f32[416,512]{1,0:T(8,128)}, u32[]{:S(2)}) copy-start(f32[416,512]{1,0:T(8,128)} %copy-done) | copy-start | bytes 2555908
  209.9 13.7 %collective-permute-start.22 = (bf16[384,512]{1,0:T(8,128)(2,1)S(1)}, bf16[384,512]{1,0:T(8,128)(2,1)S(1)}, u32[]{:S(2)}, u32[]{:S(2)}) collective-permute-start(bf16[384,512]{1,0:T(8,128)(2,1)S(1)} %get-tuple-element.24), channel_id=1, source_target_pairs={{0,4},{1,5},{2,6},{3,7},{4,0},{5,1},{6,2},{7,3},{8,12},{9,13},{10,... | collective-permute-start | bytes 1179656 | tf_op jit(solution)/shard_map/ppermute | solution.py:13
  213.2 17.9 %collective-permute-start.23 = (bf16[384,512]{1,0:T(8,128)(2,1)S(1)}, bf16[384,512]{1,0:T(8,128)(2,1)S(1)}, u32[]{:S(2)}, u32[]{:S(2)}) collective-permute-start(bf16[384,512]{1,0:T(8,128)(2,1)S(1)} %get-tuple-element.26), channel_id=1, source_target_pairs={{0,2},{1,3},{2,4},{3,5},{4,6},{5,7},{6,0},{7,1},{8,10},{9,11},{10,... | collective-permute-start | bytes 1179656 | tf_op jit(solution)/shard_map/ppermute | solution.py:13
  213.7 17.6 %collective-permute-start.24 = (bf16[384,512]{1,0:T(8,128)(2,1)S(1)}, bf16[384,512]{1,0:T(8,128)(2,1)S(1)}, u32[]{:S(2)}, u32[]{:S(2)}) collective-permute-start(bf16[384,512]{1,0:T(8,128)(2,1)S(1)} %get-tuple-element.25), channel_id=1, source_target_pairs={{0,6},{1,7},{2,0},{3,1},{4,2},{5,3},{6,4},{7,5},{8,14},{9,15},{10,... | collective-permute-start | bytes 1179656 | tf_op jit(solution)/shard_map/ppermute | solution.py:13
Sparse Core Ops, SparseCore 0:
  9.7 92.0 all-gather.2
  103.6 75.2 all-gather.4

commit v2 on v1

--- a/solution.py
+++ b/solution.py
@@ -30,22 +30,24 @@
 
 
 def project(pieces, inv_rms, rows, width):
-    tokens, size = pieces[0].shape
-    count = len(pieces)
+    stacked = not isinstance(pieces, list)
+    count, (tokens, size) = len(pieces), pieces[0].shape
     offsets = offsets_of(count)[::-1]
 
     def kernel(*refs):
-        blocks, (inv_ref, w_ref, out_ref, near, held, near_in, held_in) = refs[:count], refs[count:]
+        *blocks, inv_ref, w_ref, out_ref, near, held, near_in, held_in = refs
         lane = lax.axis_index("tp")
         other = lane + 1 - 2 * (lane % 2)
         copies = []
         for i in range(count):
             base = lane if i < len(offsets) else other
-            at = (base + offsets[i % len(offsets)] + count) % count
-            rows_of = w_ref.at[pl.ds(pl.multiple_of(at * size, size), size), pl.ds(0, 2 * width)]
+            at = i if stacked else (base + offsets[i % len(offsets)] + count) % count
+            block = blocks[0].at[i] if stacked else blocks[i]
+            start = at * size if stacked else pl.multiple_of(at * size, size)
+            rows_of = w_ref.at[pl.ds(start, size), pl.ds(0, 2 * width)]
             copies.append(
                 (
-                    pltpu.make_async_copy(blocks[i], near.at[i], near_in.at[i]),
+                    pltpu.make_async_copy(block, near.at[i], near_in.at[i]),
                     pltpu.make_async_copy(rows_of, held.at[i], held_in.at[i]),
                 )
             )
@@ -61,12 +63,13 @@
         value, gate = total[:, :width] * inv, total[:, width:] * inv
         out_ref[...] = (value * jax.nn.sigmoid(gate)).astype(out_ref.dtype)
 
+    given = [pieces] if stacked else pieces
     whole = pl.BlockSpec(memory_space=pltpu.VMEM)
     apart = pl.BlockSpec(memory_space=pl.ANY)
     return pl.pallas_call(
         kernel,
         out_shape=jax.ShapeDtypeStruct((tokens, width), jnp.bfloat16),
-        in_specs=[apart] * count + [whole, apart],
+        in_specs=[apart] * len(given) + [whole, apart],
         out_specs=whole,
         scratch_shapes=[
             pltpu.VMEM((count, tokens, size), jnp.bfloat16),
@@ -81,7 +84,7 @@
             transcendentals=tokens * width,
         ),
         name="project",
-    )(*pieces, inv_rms, rows)
+    )(*given, inv_rms, rows)
 
 
 def depthwise(gated, taps, lead):
@@ -120,23 +123,23 @@
     )(gated, taps)
 
 
-def shares(mixed, held, fetched, across=None):
+def shares(mixed, held, fetched, offsets, across=None):
     tokens, width = mixed.shape
-    tp = lax.axis_size("tp")
-    offsets = offsets_of(tp)
     count = len(offsets)
-    size = held.shape[0] // tp
-    last = [] if across is None else [jax.ShapeDtypeStruct((tokens, size), jnp.float32)]
-    outs = [jax.ShapeDtypeStruct((count - len(last), tokens, size), jnp.bfloat16)] + last
+    size = held.shape[0] // (2 * count)
+    sent = count if across is None else sum(d != 0 for d in offsets)
+    outs = [jax.ShapeDtypeStruct((sent, tokens, size), jnp.bfloat16)]
+    outs += [jax.ShapeDtypeStruct((tokens, size), jnp.float32)] * (sent < count)
+    given = [] if across is None else [across]
 
     def kernel(mixed_ref, held_ref, fetched_ref, *refs):
-        arrived, (pairs_ref, *own_ref) = refs[: len(refs) - len(outs)], refs[len(refs) - len(outs) :]
-        lane = lax.axis_index("tp")
-        base = lane if arrived else lane + 1 - 2 * (lane % 2)
+        arrived, (pairs_ref, *own_ref) = refs[: len(given)], refs[len(given) :]
+        core = lax.axis_index("tp") % 2
+        side = core if arrived else 1 - core
         odd = lax.axis_index("grp") % 2 == 1
         for i, d in enumerate(offsets):
             for j in range(0, size, width):
-                at = pl.multiple_of((base + d + tp) % tp * size + j, width)
+                at = pl.multiple_of((2 * i + side) * size + j, width)
                 block = held_ref[pl.ds(at, width), :]
                 pair = fetched_ref[pl.ds(at, width), :]
                 block = jnp.concatenate(
@@ -151,7 +154,6 @@
                     pairs_ref[i, :, pl.ds(j, width)] = part.astype(jnp.bfloat16)
 
     whole = pl.BlockSpec(memory_space=pltpu.VMEM)
-    given = [] if across is None else [across]
     return pl.pallas_call(
         kernel,
         out_shape=outs,
@@ -197,15 +199,37 @@
     lead = -(-reach_rows // 32) * 32
 
     def run(layer, current):
-        held = taken[layer][:, 2 * width :]
-        fetched = fetched_rows(held)
+        last = layer == layer_count - 1
+        groups = [offsets[: tp // 4], offsets[tp // 4 :]] if last else [offsets]
+        chip = 2 * (features // tp)
+        held, fetched = [], []
+        for group in groups:
+            held.append(
+                jnp.concatenate(
+                    [
+                        lax.dynamic_slice(
+                            taken[layer],
+                            ((lax.axis_index("tp") // 2 * 2 + d) % tp // 2 * chip, 2 * width),
+                            (chip, half),
+                        )
+                        for d in group
+                    ],
+                    axis=0,
+                )
+            )
+            fetched.append(fetched_rows(held[-1]))
         widened = current.astype(jnp.float32)
         scaled = (widened * in_gain[layer]).astype(jnp.bfloat16)
-        near = [scaled if d == 0 else shifted(scaled, "tp", -d) for d in offsets]
+        if last:
+            near = [scaled if d == 0 else shifted(scaled, "tp", -d) for d in offsets]
+        else:
+            everyone = jnp.broadcast_to(scaled[None], (tp, *scaled.shape))
+            pieces = lax.all_to_all(everyone, "tp", 0, 0, tiled=True)
         squares = over_lanes(jnp.sum(widened * widened, axis=1))
         inv_rms = lax.rsqrt(squares / features + epsilon)[:, None]
-        far = [swapped(piece) for piece in near]
-        gated = project(near[::-1] + far[::-1], inv_rms, taken[layer], width)
+        if last:
+            pieces = near[::-1] + [swapped(piece) for piece in near[::-1]]
+        gated = project(pieces, inv_rms, taken[layer], width)
         conved = depthwise(gated, conv_taps[layer], lead)
         sums = jnp.stack([jnp.sum(conved, axis=1), jnp.sum(conved * conved, axis=1)])
         totals = over_lanes(sums)
@@ -215,11 +239,14 @@
             layer
         ] + norm_shift[layer]
         mixed_out = jax.nn.silu(normed).astype(jnp.bfloat16)
-        across = swapped(shares(mixed_out, held, fetched)[0])
-        pairs, own = shares(mixed_out, held, fetched, across)
-        summed = widened[lead:] + own
-        for piece, d in zip(pairs, offsets):
-            summed += shifted(piece, "tp", d).astype(jnp.float32)
+        summed = widened[lead:]
+        for g, group in enumerate(groups):
+            rows = (mixed_out, held[g], fetched[g], group)
+            across = swapped(shares(*rows)[0])
+            pairs, *own = shares(*rows, across)
+            parts = own + [shifted(p, "tp", d) for p, d in zip(pairs, group)]
+            for part in parts:
+                summed += part.astype(jnp.float32)
         return summed.astype(jnp.bfloat16)
 
     ahead = lead * layer_count

time: 242 us -> 250 us (1.033)
  waiting for transfers between devices: 150 us -> 154 us
    all_gather x2, waiting for transfers between devices: 51.3 us -> 89.8 us  [shards(): taken.append(lax.all_gather(rows, 'sp', axis=0, tiled=True))]
    ppermute x12 -> x9, waiting for transfers between devices: 69.3 us -> 37.1 us  [shifted(): lax.ppermute(value, axis, [(i, (i + steps) % count) for i in range(count)])]
    ppermute x12 -> x9, starting transfers between devices: 21.8 us -> 14.8 us  [shifted(): lax.ppermute(value, axis, [(i, (i + steps) % count) for i in range(count)])]
    all_to_all x0 -> x1, starting transfers between devices: none -> 4.81 us  [run(): pieces = lax.all_to_all(everyone, 'tp', 0, 0, tiled=True)]
    ppermute x10 -> x7, waiting for transfers between devices: 6.98 us -> 3.59 us  [swapped(): lax.ppermute(value, 'tp', [(i, i ^ 1) for i in range(lax.axis_size('tp'))])]
    slice x2 -> x0, local copies, waits for them, and re-layouts: 2.58 us -> none  [run(): held = taken[layer][:, 2 * width:]]
    dynamic_slice x0 -> x2, local copies, waits for them, and re-layouts: none -> 2.57 us  [run(): lax.dynamic_slice(taken[layer], ((lax.axis_index('tp') // 2 * 2 + d) % tp...]
    ppermute x2 -> x3, waiting for transfers between devices: 7.23 us -> 8.28 us  [fetched_rows(): lax.ppermute(held, 'grp', [(i, i ^ 1) for i in range(lax.axis_size('grp'))])]
  transfers between devices with their start and end apart: 30 -> 26, of which waited for: 20 -> 13; matrix products, arithmetic and copies ran while one was open for 3% -> 5% of each run, Pallas kernels for 5% -> 6%
where the time goes in v2:
time: 250 us; the launch traced here: 248 us
  waiting for transfers between devices  154 us (62%)
  starting transfers between devices  40.5 us (16%)
  Pallas kernels  14.3 us (6%)
  between operations  14.1 us (6%)
  local copies, waits for them, and re-layouts  10.1 us (4%)
  blocking collectives  9.74 us (4%)
  other arithmetic  5.54 us (2%)
    all_gather x2, waiting for transfers between devices, shards(): taken.append(lax.all_gather(rows, 'sp', axis=0, tiled=True))  89.8 us
    ppermute x9, waiting for transfers between devices, shifted(): lax.ppermute(value, axis, [(i, (i + steps) % count) for i in range(count)])  37.1 us
    ppermute x9, starting transfers between devices, shifted(): lax.ppermute(value, axis, [(i, (i + steps) % count) for i in range(count)])  14.8 us
    all_to_all x3, waiting for transfers between devices, over_lanes(): return lax.all_to_all(everyone, 'tp', 0, 0, tiled=True).sum(axis=0)  13.3 us
    all_to_all x3, starting transfers between devices, over_lanes(): return lax.all_to_all(everyone, 'tp', 0, 0, tiled=True).sum(axis=0)  12.1 us
    all_to_all x1, blocking collectives, over_lanes(): return lax.all_to_all(everyone, 'tp', 0, 0, tiled=True).sum(axis=0)  9.74 us
    ppermute x3, waiting for transfers between devices, fetched_rows(): lax.ppermute(held, 'grp', [(i, i ^ 1) for i in range(lax.axis_size('grp'))])  8.28 us
    pallas_call x2, Pallas kernels, project(): pl.pallas_call(kernel, out_shape=jax.ShapeDtypeStruct((tokens, width), jn...  7.98 us
  transfers between devices with their start and end apart: 26, of which 13 were waited for; matrix products, arithmetic and copies ran while one was open for 5% of the time, Pallas kernels for 6%

profile of v2, /device:TPU:40, one launch (start us, length us, event | category | flops | bytes accessed | tf_op | source)
XLA Modules:
  0.0 248.3 jit_solution(5577721486553313591)
XLA Ops:
  6.6 1.0 fusion.16
  7.6 1.1 slice_bitcast_fusion.5
  8.8 0.8 pad_maximum_fusion.3
  9.7 0.8 pad_maximum_fusion.4
  10.5 4.7 %collective-permute-start = (bf16[64,512]{1,0:T(8,128)(2,1)S(1)}, bf16[64,512]{1,0:T(8,128)(2,1)S(1)}, u32[]{:S(2)}, u32[]{:S(2)}) collective-permute-start(bf16[64,512]{1,0:T(8,128)(2,1)S(1)} %slice.65), channel_id=1, source_target_pairs={{0,8},{8,16},{16,24},{24,32},{32,40},{40,48},{48,56},{56,64},{64,7... | collective-permute-start | bytes 196616 | tf_op jit(solution)/shard_map/ppermute | solution.py:23
  15.3 1.9 collective-permute-done
  17.1 0.2 multiply_reduce_fusion
  17.4 9.7 %all_to_all.27 = f32[8,1,448]{2,1,0:T(1,128)S(1)} all-to-all(f32[8,1,448]{2,1,0:T(1,128)S(1)} %broadcast_in_dim.25), channel_id=1, replica_groups=mesh['grp'=2,'sp'=16,'tp'=8] {'tp'}, dimensions={0} | all-to-all | bytes 28672 | tf_op jit(solution)/shard_map/all_to_all | solution.py:174
  27.1 2.1 broadcast_in_dim.24
  29.2 4.8 %all-to-all-start = ((bf16[8,448,512]{2,1,0:T(8,128)(2,1)}), bf16[8,448,512]{2,1,0:T(8,128)(2,1)}, u32[]{:S(2)}, u32[]{:S(2)}) async-start(bf16[8,448,512]{2,1,0:T(8,128)(2,1)} %broadcast_in_dim.24), calls=%async_computation | async-start | bytes 7340032 | tf_op jit(solution)/shard_map/all_to_all | solution.py:227
  34.5 67.3 %all-gather.3.cloned.1.call-done.refs_2_ = bf16[4096,640]{1,0:T(8,128)(2,1)} async-done(((bf16[256,640]{1,0:T(8,128)(2,1)}), bf16[4096,640]{1,0:T(8,128)(2,1)}) %all-gather.3.cloned.1.call-update) | async-done | bytes 5242896 | tf_op jit(solution)/shard_map/all_gather | solution.py:197
  101.8 1.3 constant_dynamic-slice_fusion.7
  103.2 0.9 collective-permute-start.1
  104.0 4.0 %project.2.gated_ref = bf16[448,256]{1,0:T(8,128)(2,1)S(1)} custom-call(bf16[8,448,512]{2,1,0:T(8,128)(2,1)} %all-to-all-done.refs_0_, f32[448,1]{1,0:T(8,128)S(1)} %copy.20.refs_1_, bf16[4096,640]{1,0:T(8,128)(2,1)} %all-gather.3.cloned.1.call-done.refs_2_), custom_call_target="tpu_custom_call" | custom-call | flops 1879048192 | bytes 4194304 | tf_op jit(solution)/shard_map/project/pallas_call | solution.py:69
  108.1 1.9 depthwise.2
  110.0 0.2 fusion.13
  110.2 0.6 broadcast_in_dim.26
  110.8 4.2 %all-to-all-start.2 = ((f32[8,2,416]{2,1,0:T(2,128)}), f32[8,2,416]{2,1,0:T(2,128)S(1)}, u32[]{:S(2)}, u32[]{:S(2)}) async-start(f32[8,2,416]{2,1,0:T(2,128)} %broadcast_in_dim.26), calls=%async_computation.2 | async-start | bytes 65536 | tf_op jit(solution)/shard_map/all_to_all | solution.py:174
  115.0 5.4 %all-to-all-done.2 = f32[8,2,416]{2,1,0:T(2,128)S(1)} async-done(((f32[8,2,416]{2,1,0:T(2,128)}), f32[8,2,416]{2,1,0:T(2,128)S(1)}, u32[]{:S(2)}, u32[]{:S(2)}) %all-to-all-start.2) | async-done | bytes 26656 | tf_op jit(solution)/shard_map/all_to_all | solution.py:174
  120.5 0.2 multiply_convert_fusion.2.mixed_ref
  120.8 0.6 shares.6
  121.5 0.1 collective-permute-start.2
  121.6 3.6 %collective-permute-done.2.refs_0_ = bf16[4,416,512]{2,1,0:T(8,128)(2,1)S(1)} collective-permute-done((bf16[4,416,512]{2,1,0:T(8,128)(2,1)S(1)}, bf16[4,416,512]{2,1,0:T(8,128)(2,1)S(1)}, u32[]{:S(2)}, u32[]{:S(2)}) %collective-permute-start.2) | collective-permute-done | bytes 1703968 | tf_op jit(solution)/shard_map/ppermute | solution.py:17
  125.2 0.6 shares.7
  125.8 0.9 slice_bitcast_fusion.2
  126.7 2.5 %collective-permute-start.5 = (bf16[416,512]{1,0:T(8,128)(2,1)}, bf16[416,512]{1,0:T(8,128)(2,1)S(1)}, u32[]{:S(2)}, u32[]{:S(2)}) collective-permute-start(bf16[416,512]{1,0:T(8,128)(2,1)} %get-tuple-element.30), channel_id=1, source_target_pairs={{0,6},{1,7},{2,0},{3,1},{4,2},{5,3},{6,4},{7,5},{8,14},{9,15},{10,... | collective-permute-start | bytes 1277960 | tf_op jit(solution)/shard_map/ppermute | solution.py:13
  129.3 2.3 collective-permute-start.3
  131.7 16.4 %collective-permute-done.5 = bf16[416,512]{1,0:T(8,128)(2,1)S(1)} collective-permute-done((bf16[416,512]{1,0:T(8,128)(2,1)}, bf16[416,512]{1,0:T(8,128)(2,1)S(1)}, u32[]{:S(2)}, u32[]{:S(2)}) %collective-permute-start.5) | collective-permute-done | bytes 426016 | tf_op jit(solution)/shard_map/ppermute | solution.py:13
  148.1 3.1 %collective-permute-done.4 = bf16[416,512]{1,0:T(8,128)(2,1)S(1)} collective-permute-done((bf16[416,512]{1,0:T(8,128)(2,1)S(1)}, bf16[416,512]{1,0:T(8,128)(2,1)S(1)}, u32[]{:S(2)}, u32[]{:S(2)}) %collective-permute-start.4) | collective-permute-done | bytes 426016 | tf_op jit(solution)/shard_map/ppermute | solution.py:13
  151.2 1.4 multiply_reduce_fusion.1
  152.7 0.3 collective-permute-start.6
  153.0 3.2 %collective-permute-start.7 = (bf16[416,512]{1,0:T(8,128)(2,1)S(1)}, bf16[416,512]{1,0:T(8,128)(2,1)S(1)}, u32[]{:S(2)}, u32[]{:S(2)}) collective-permute-start(bf16[416,512]{1,0:T(8,128)(2,1)S(1)} %multiply_convert_fusion.1.refs_0_), channel_id=1, source_target_pairs={{0,6},{1,7},{2,0},{3,1},{4,2},{5,3},{6,4},{7,5},{8,14},{9,15},{10,... | collective-permute-start | bytes 1277960 | tf_op jit(solution)/shard_map/ppermute | solution.py:13
  156.2 22.5 %all-gather.5.cloned.1.call-done.refs_9_ = bf16[4096,640]{1,0:T(8,128)(2,1)} async-done(((bf16[256,640]{1,0:T(8,128)(2,1)}), bf16[4096,640]{1,0:T(8,128)(2,1)}) %all-gather.5.cloned.1.call-update) | async-done | bytes 5242896 | tf_op jit(solution)/shard_map/all_gather | solution.py:197
  178.7 1.3 constant_dynamic-slice_fusion.3
  180.0 0.1 collective-permute-start.9
  180.2 0.6 broadcast_in_dim.27
  180.8 4.4 %all-to-all-start.3 = ((f32[8,1,416]{2,1,0:T(1,128)}), f32[8,1,416]{2,1,0:T(1,128)S(1)}, u32[]{:S(2)}, u32[]{:S(2)}) async-start(f32[8,1,416]{2,1,0:T(1,128)} %broadcast_in_dim.27), calls=%async_computation.3 | async-start | bytes 32768 | tf_op jit(solution)/shard_map/all_to_all | solution.py:174
  185.2 0.5 collective-permute-start.10
  185.7 0.2 collective-permute-start.11
  185.8 0.4 collective-permute-start.12
  186.2 0.8 collective-permute-start.17
  187.0 3.5 %all-to-all-done.3 = f32[8,1,416]{2,1,0:T(1,128)S(1)} async-done(((f32[8,1,416]{2,1,0:T(1,128)}), f32[8,1,416]{2,1,0:T(1,128)S(1)}, u32[]{:S(2)}, u32[]{:S(2)}) %all-to-all-start.3) | async-done | bytes 13344 | tf_op jit(solution)/shard_map/all_to_all | solution.py:174
  190.6 0.1 copy.24.refs_8_
  190.8 4.0 %project.3.gated_ref = bf16[416,256]{1,0:T(8,128)(2,1)S(1)} custom-call(bf16[416,512]{1,0:T(8,128)(2,1)S(1)} %multiply_convert_fusion.1.refs_0_, bf16[416,512]{1,0:T(8,128)(2,1)S(1)} %collective-permute-done.6.refs_1_, bf16[416,512]{1,0:T(8,128)(2,1)S(1)} %collective-permute-done.7.refs_2_, bf16[416,512]{1,0:T(8,128)(2,1)S(1)} %collective-permute-done.8.refs_3_, ...), custom_call_target="tpu_custom_call" | custom-call | flops 1744830464 | bytes 4194304 | tf_op jit(solution)/shard_map/project/pallas_call | solution.py:69
  194.7 1.6 depthwise.3
  196.4 0.2 fusion.14
  196.6 0.6 broadcast_in_dim.28
  197.2 3.5 %all-to-all-start.4 = ((f32[8,2,384]{2,1,0:T(2,128)}), f32[8,2,384]{2,1,0:T(2,128)S(1)}, u32[]{:S(2)}, u32[]{:S(2)}) async-start(f32[8,2,384]{2,1,0:T(2,128)} %broadcast_in_dim.28), calls=%async_computation.4 | async-start | bytes 49152 | tf_op jit(solution)/shard_map/all_to_all | solution.py:174
  200.8 0.8 collective-permute-start.13
  201.6 4.3 %all-to-all-done.4 = f32[8,2,384]{2,1,0:T(2,128)S(1)} async-done(((f32[8,2,384]{2,1,0:T(2,128)}), f32[8,2,384]{2,1,0:T(2,128)S(1)}, u32[]{:S(2)}, u32[]{:S(2)}) %all-to-all-start.4) | async-done | bytes 24608 | tf_op jit(solution)/shard_map/all_to_all | solution.py:174
  206.0 0.2 multiply_convert_fusion.3.mixed_ref
  206.2 0.4 shares.10
  206.6 0.1 collective-permute-start.18
  206.8 8.2 %collective-permute-done.13.fetched_ref = bf16[2048,128]{1,0:T(8,128)(2,1)S(1)} collective-permute-done((bf16[2048,128]{1,0:T(8,128)(2,1)S(1)}, bf16[2048,128]{1,0:T(8,128)(2,1)S(1)}, u32[]{:S(2)}, u32[]{:S(2)}) %collective-permute-start.13) | collective-permute-done | bytes 524320 | tf_op jit(solution)/shard_map/ppermute | solution.py:178
  215.0 0.4 shares.8
  215.3 0.1 collective-permute-start.14
  215.5 0.4 shares.11
  215.9 3.1 %collective-permute-start.19 = (bf16[384,512]{1,0:T(8,128)(2,1)S(1)}, bf16[384,512]{1,0:T(8,128)(2,1)S(1)}, u32[]{:S(2)}, u32[]{:S(2)}) collective-permute-start(bf16[384,512]{1,0:T(8,128)(2,1)S(1)} %bitcast.43), channel_id=1, source_target_pairs={{0,6},{1,7},{2,0},{3,1},{4,2},{5,3},{6,4},{7,5},{8,14},{9,15},{10,... | collective-permute-start | bytes 1179656 | tf_op jit(solution)/shard_map/ppermute | solution.py:13
  219.0 0.4 shares.9
  219.4 0.5 collective-permute-start.16
  220.0 2.8 %collective-permute-start.15 = (bf16[384,512]{1,0:T(8,128)(2,1)S(1)}, bf16[384,512]{1,0:T(8,128)(2,1)S(1)}, u32[]{:S(2)}, u32[]{:S(2)}) collective-permute-start(bf16[384,512]{1,0:T(8,128)(2,1)S(1)} %get-tuple-element.32), channel_id=1, source_target_pairs={{0,4},{1,5},{2,6},{3,7},{4,0},{5,1},{6,2},{7,3},{8,12},{9,13},{10,... | collective-permute-start | bytes 1179656 | tf_op jit(solution)/shard_map/ppermute | solution.py:13
  222.7 13.7 %collective-permute-done.19 = bf16[384,512]{1,0:T(8,128)(2,1)S(1)} collective-permute-done((bf16[384,512]{1,0:T(8,128)(2,1)S(1)}, bf16[384,512]{1,0:T(8,128)(2,1)S(1)}, u32[]{:S(2)}, u32[]{:S(2)}) %collective-permute-start.19) | collective-permute-done | bytes 393248 | tf_op jit(solution)/shard_map/ppermute | solution.py:13
  236.4 4.0 %collective-permute-done.16 = bf16[384,512]{1,0:T(8,128)(2,1)S(1)} collective-permute-done((bf16[384,512]{1,0:T(8,128)(2,1)S(1)}, bf16[384,512]{1,0:T(8,128)(2,1)S(1)}, u32[]{:S(2)}, u32[]{:S(2)}) %collective-permute-start.16) | collective-permute-done | bytes 393248 | tf_op jit(solution)/shard_map/ppermute | solution.py:13
  240.4 1.0 fusion.7
  (66 shorter events, 1.2 us)
Async XLA Ops:
  6.5 4.0 %copy-start.2 = (bf16[384,512]{1,0:T(8,128)(2,1)S(1)}, bf16[384,512]{1,0:T(8,128)(2,1)}, u32[]{:S(2)}) copy-start(bf16[384,512]{1,0:T(8,128)(2,1)} %param.8) | copy-start | bytes 1179652
  6.5 8.7 %copy-start.4 = (f32[2,512]{1,0:T(2,128)S(1)}, f32[2,512]{1,0:T(2,128)}, u32[]{:S(2)}) copy-start(f32[2,512]{1,0:T(2,128)} %param.9) | copy-start | bytes 12292
  6.6 95.2 %all-gather.3.cloned.1.call-start = ((), (), s32[]{:S(2)}) async-start(), calls=%async_computation.5 | async-start | bytes 5570560 | tf_op jit(solution)/shard_map/all_gather | solution.py:197
  9.6 169.2 %all-gather.5.cloned.1.call-start = ((), (), s32[]{:S(2)}) async-start(), calls=%async_computation.6 | async-start | bytes 5570560 | tf_op jit(solution)/shard_map/all_gather | solution.py:197
  10.5 6.6 %collective-permute-start = (bf16[64,512]{1,0:T(8,128)(2,1)S(1)}, bf16[64,512]{1,0:T(8,128)(2,1)S(1)}, u32[]{:S(2)}, u32[]{:S(2)}) collective-permute-start(bf16[64,512]{1,0:T(8,128)(2,1)S(1)} %slice.65), channel_id=1, source_target_pairs={{0,8},{8,16},{16,24},{24,32},{32,40},{40,48},{48,56},{56,64},{64,7... | collective-permute-start | bytes 196616 | tf_op jit(solution)/shard_map/ppermute | solution.py:23
  29.2 5.0 %copy-start.3 = (f32[2,31,256]{2,0,1:T(2,128)S(1)}, f32[2,31,256]{2,0,1:T(2,128)}, u32[]{:S(2)}) copy-start(f32[2,31,256]{2,0,1:T(2,128)} %param.12) | copy-start | bytes 190468
  29.2 5.1 %copy-start.5 = (f32[2,256]{1,0:T(2,128)S(1)}, f32[2,256]{1,0:T(2,128)}, u32[]{:S(2)}) copy-start(f32[2,256]{1,0:T(2,128)} %param.14) | copy-start | bytes 6148
  29.2 74.8 %all-to-all-start = ((bf16[8,448,512]{2,1,0:T(8,128)(2,1)}), bf16[8,448,512]{2,1,0:T(8,128)(2,1)}, u32[]{:S(2)}, u32[]{:S(2)}) async-start(bf16[8,448,512]{2,1,0:T(8,128)(2,1)} %broadcast_in_dim.24), calls=%async_computation | async-start | bytes 7340032 | tf_op jit(solution)/shard_map/all_to_all | solution.py:227
  103.2 11.9 %copy-start.6 = (f32[2,256]{1,0:T(2,128)S(1)}, f32[2,256]{1,0:T(2,128)}, u32[]{:S(2)}) copy-start(f32[2,256]{1,0:T(2,128)} %param.13) | copy-start | bytes 6148
  103.2 17.7 %collective-permute-start.1 = (bf16[4096,128]{1,0:T(8,128)(2,1)S(1)}, bf16[4096,128]{1,0:T(8,128)(2,1)S(1)}, u32[]{:S(2)}, u32[]{:S(2)}) collective-permute-start(bf16[4096,128]{1,0:T(8,128)(2,1)S(1)} %pad_maximum_fusion.held_ref), channel_id=1, source_target_pairs={{0,128},{128,0},{1,129},{129,1},{2,130},{130,2},{3,131},{131,3},{4... | collective-permute-start | bytes 3145736 | tf_op jit(solution)/shard_map/ppermute | solution.py:178
  110.8 9.6 %all-to-all-start.2 = ((f32[8,2,416]{2,1,0:T(2,128)}), f32[8,2,416]{2,1,0:T(2,128)S(1)}, u32[]{:S(2)}, u32[]{:S(2)}) async-start(f32[8,2,416]{2,1,0:T(2,128)} %broadcast_in_dim.26), calls=%async_computation.2 | async-start | bytes 65536 | tf_op jit(solution)/shard_map/all_to_all | solution.py:174
  121.5 3.7 %collective-permute-start.2 = (bf16[4,416,512]{2,1,0:T(8,128)(2,1)S(1)}, bf16[4,416,512]{2,1,0:T(8,128)(2,1)S(1)}, u32[]{:S(2)}, u32[]{:S(2)}) collective-permute-start(bf16[4,416,512]{2,1,0:T(8,128)(2,1)S(1)} %shares.6), channel_id=1, source_target_pairs={{0,1},{1,0},{2,3},{3,2},{4,5},{5,4},{6,7},{7,6},{8,9},{9,8},{10,11... | collective-permute-start | bytes 5111816 | tf_op jit(solution)/shard_map/ppermute | solution.py:17
  126.7 21.4 %collective-permute-start.5 = (bf16[416,512]{1,0:T(8,128)(2,1)}, bf16[416,512]{1,0:T(8,128)(2,1)S(1)}, u32[]{:S(2)}, u32[]{:S(2)}) collective-permute-start(bf16[416,512]{1,0:T(8,128)(2,1)} %get-tuple-element.30), channel_id=1, source_target_pairs={{0,6},{1,7},{2,0},{3,1},{4,2},{5,3},{6,4},{7,5},{8,14},{9,15},{10,... | collective-permute-start | bytes 1277960 | tf_op jit(solution)/shard_map/ppermute | solution.py:13
  129.3 21.9 %collective-permute-start.4 = (bf16[416,512]{1,0:T(8,128)(2,1)S(1)}, bf16[416,512]{1,0:T(8,128)(2,1)S(1)}, u32[]{:S(2)}, u32[]{:S(2)}) collective-permute-start(bf16[416,512]{1,0:T(8,128)(2,1)S(1)} %get-tuple-element.31), channel_id=1, source_target_pairs={{0,2},{1,3},{2,4},{3,5},{4,6},{5,7},{6,0},{7,1},{8,10},{9,11},{10,... | collective-permute-start | bytes 1277960 | tf_op jit(solution)/shard_map/ppermute | solution.py:13
  129.3 21.9 %collective-permute-start.3 = (bf16[416,512]{1,0:T(8,128)(2,1)S(1)}, bf16[416,512]{1,0:T(8,128)(2,1)}, u32[]{:S(2)}, u32[]{:S(2)}) collective-permute-start(bf16[416,512]{1,0:T(8,128)(2,1)S(1)} %get-tuple-element.29), channel_id=1, source_target_pairs={{0,4},{1,5},{2,6},{3,7},{4,0},{5,1},{6,2},{7,3},{8,12},{9,13},{10,... | collective-permute-start | bytes 1277960 | tf_op jit(solution)/shard_map/ppermute | solution.py:13
  152.6 3.6 %copy-start = (f32[416,512]{1,0:T(8,128)}, f32[416,512]{1,0:T(8,128)S(1)}, u32[]{:S(2)}) copy-start(f32[416,512]{1,0:T(8,128)S(1)} %get-tuple-element.20) | copy-start | bytes 2555908
  152.7 32.5 %collective-permute-start.6 = (bf16[416,512]{1,0:T(8,128)(2,1)S(1)}, bf16[416,512]{1,0:T(8,128)(2,1)S(1)}, u32[]{:S(2)}, u32[]{:S(2)}) collective-permute-start(bf16[416,512]{1,0:T(8,128)(2,1)S(1)} %multiply_convert_fusion.1.refs_0_), channel_id=1, source_target_pairs={{0,2},{1,3},{2,4},{3,5},{4,6},{5,7},{6,0},{7,1},{8,10},{9,11},{10,... | collective-permute-start | bytes 1277960 | tf_op jit(solution)/shard_map/ppermute | solution.py:13
  153.0 32.6 %collective-permute-start.7 = (bf16[416,512]{1,0:T(8,128)(2,1)S(1)}, bf16[416,512]{1,0:T(8,128)(2,1)S(1)}, u32[]{:S(2)}, u32[]{:S(2)}) collective-permute-start(bf16[416,512]{1,0:T(8,128)(2,1)S(1)} %multiply_convert_fusion.1.refs_0_), channel_id=1, source_target_pairs={{0,6},{1,7},{2,0},{3,1},{4,2},{5,3},{6,4},{7,5},{8,14},{9,15},{10,... | collective-permute-start | bytes 1277960 | tf_op jit(solution)/shard_map/ppermute | solution.py:13
  156.2 29.6 %collective-permute-start.8 = (bf16[416,512]{1,0:T(8,128)(2,1)S(1)}, bf16[416,512]{1,0:T(8,128)(2,1)S(1)}, u32[]{:S(2)}, u32[]{:S(2)}) collective-permute-start(bf16[416,512]{1,0:T(8,128)(2,1)S(1)} %multiply_convert_fusion.1.refs_0_), channel_id=1, source_target_pairs={{0,4},{1,5},{2,6},{3,7},{4,0},{5,1},{6,2},{7,3},{8,12},{9,13},{10,... | collective-permute-start | bytes 1277960 | tf_op jit(solution)/shard_map/ppermute | solution.py:13
  180.0 10.7 %collective-permute-start.9 = (bf16[416,512]{1,0:T(8,128)(2,1)S(1)}, bf16[416,512]{1,0:T(8,128)(2,1)}, u32[]{:S(2)}, u32[]{:S(2)}) collective-permute-start(bf16[416,512]{1,0:T(8,128)(2,1)S(1)} %multiply_convert_fusion.1.refs_0_), channel_id=1, source_target_pairs={{0,1},{1,0},{2,3},{3,2},{4,5},{5,4},{6,7},{7,6},{8,9},{9,8},{10,11... | collective-permute-start | bytes 1277960 | tf_op jit(solution)/shard_map/ppermute | solution.py:17
  180.8 9.7 %all-to-all-start.3 = ((f32[8,1,416]{2,1,0:T(1,128)}), f32[8,1,416]{2,1,0:T(1,128)S(1)}, u32[]{:S(2)}, u32[]{:S(2)}) async-start(f32[8,1,416]{2,1,0:T(1,128)} %broadcast_in_dim.27), calls=%async_computation.3 | async-start | bytes 32768 | tf_op jit(solution)/shard_map/all_to_all | solution.py:174
  185.2 5.6 %collective-permute-start.10 = (bf16[416,512]{1,0:T(8,128)(2,1)S(1)}, bf16[416,512]{1,0:T(8,128)(2,1)}, u32[]{:S(2)}, u32[]{:S(2)}) collective-permute-start(bf16[416,512]{1,0:T(8,128)(2,1)S(1)} %collective-permute-done.6.refs_1_), channel_id=1, source_target_pairs={{0,1},{1,0},{2,3},{3,2},{4,5},{5,4},{6,7},{7,6},{8,9},{9,8},{10,11... | collective-permute-start | bytes 1277960 | tf_op jit(solution)/shard_map/ppermute | solution.py:17
  185.7 5.1 %collective-permute-start.11 = (bf16[416,512]{1,0:T(8,128)(2,1)S(1)}, bf16[416,512]{1,0:T(8,128)(2,1)}, u32[]{:S(2)}, u32[]{:S(2)}) collective-permute-start(bf16[416,512]{1,0:T(8,128)(2,1)S(1)} %collective-permute-done.7.refs_2_), channel_id=1, source_target_pairs={{0,1},{1,0},{2,3},{3,2},{4,5},{5,4},{6,7},{7,6},{8,9},{9,8},{10,11... | collective-permute-start | bytes 1277960 | tf_op jit(solution)/shard_map/ppermute | solution.py:17
  185.8 4.9 %collective-permute-start.12 = (bf16[416,512]{1,0:T(8,128)(2,1)S(1)}, bf16[416,512]{1,0:T(8,128)(2,1)}, u32[]{:S(2)}, u32[]{:S(2)}) collective-permute-start(bf16[416,512]{1,0:T(8,128)(2,1)S(1)} %collective-permute-done.8.refs_3_), channel_id=1, source_target_pairs={{0,1},{1,0},{2,3},{3,2},{4,5},{5,4},{6,7},{7,6},{8,9},{9,8},{10,11... | collective-permute-start | bytes 1277960 | tf_op jit(solution)/shard_map/ppermute | solution.py:17
  186.2 20.0 %collective-permute-start.17 = (bf16[2048,128]{1,0:T(8,128)(2,1)S(1)}, bf16[2048,128]{1,0:T(8,128)(2,1)S(1)}, u32[]{:S(2)}, u32[]{:S(2)}) collective-permute-start(bf16[2048,128]{1,0:T(8,128)(2,1)S(1)} %pad_maximum_fusion.2.held_ref), channel_id=1, source_target_pairs={{0,128},{128,0},{1,129},{129,1},{2,130},{130,2},{3,131},{131,3},{4... | collective-permute-start | bytes 1572872 | tf_op jit(solution)/shard_map/ppermute | solution.py:178
  197.2 8.7 %all-to-all-start.4 = ((f32[8,2,384]{2,1,0:T(2,128)}), f32[8,2,384]{2,1,0:T(2,128)S(1)}, u32[]{:S(2)}, u32[]{:S(2)}) async-start(f32[8,2,384]{2,1,0:T(2,128)} %broadcast_in_dim.28), calls=%async_computation.4 | async-start | bytes 49152 | tf_op jit(solution)/shard_map/all_to_all | solution.py:174
  200.8 14.2 %collective-permute-start.13 = (bf16[2048,128]{1,0:T(8,128)(2,1)S(1)}, bf16[2048,128]{1,0:T(8,128)(2,1)S(1)}, u32[]{:S(2)}, u32[]{:S(2)}) collective-permute-start(bf16[2048,128]{1,0:T(8,128)(2,1)S(1)} %pad_maximum_fusion.1.held_ref), channel_id=1, source_target_pairs={{0,128},{128,0},{1,129},{129,1},{2,130},{130,2},{3,131},{131,3},{4... | collective-permute-start | bytes 1572872 | tf_op jit(solution)/shard_map/ppermute | solution.py:178
  206.6 8.9 %collective-permute-start.18 = (bf16[2,384,512]{2,1,0:T(8,128)(2,1)S(1)}, bf16[2,384,512]{2,1,0:T(8,128)(2,1)S(1)}, u32[]{:S(2)}, u32[]{:S(2)}) collective-permute-start(bf16[2,384,512]{2,1,0:T(8,128)(2,1)S(1)} %shares.10), channel_id=1, source_target_pairs={{0,1},{1,0},{2,3},{3,2},{4,5},{5,4},{6,7},{7,6},{8,9},{9,8},{10,11... | collective-permute-start | bytes 2359304 | tf_op jit(solution)/shard_map/ppermute | solution.py:17
  215.3 3.7 %collective-permute-start.14 = (bf16[2,384,512]{2,1,0:T(8,128)(2,1)S(1)}, bf16[2,384,512]{2,1,0:T(8,128)(2,1)S(1)}, u32[]{:S(2)}, u32[]{:S(2)}) collective-permute-start(bf16[2,384,512]{2,1,0:T(8,128)(2,1)S(1)} %shares.8), channel_id=1, source_target_pairs={{0,1},{1,0},{2,3},{3,2},{4,5},{5,4},{6,7},{7,6},{8,9},{9,8},{10,11... | collective-permute-start | bytes 2359304 | tf_op jit(solution)/shard_map/ppermute | solution.py:17
  215.9 24.5 %copy-start.1 = (f32[416,512]{1,0:T(8,128)S(1)}, f32[416,512]{1,0:T(8,128)}, u32[]{:S(2)}) copy-start(f32[416,512]{1,0:T(8,128)} %copy-done) | copy-start | bytes 2555908
  215.9 20.5 %collective-permute-start.19 = (bf16[384,512]{1,0:T(8,128)(2,1)S(1)}, bf16[384,512]{1,0:T(8,128)(2,1)S(1)}, u32[]{:S(2)}, u32[]{:S(2)}) collective-permute-start(bf16[384,512]{1,0:T(8,128)(2,1)S(1)} %bitcast.43), channel_id=1, source_target_pairs={{0,6},{1,7},{2,0},{3,1},{4,2},{5,3},{6,4},{7,5},{8,14},{9,15},{10,... | collective-permute-start | bytes 1179656 | tf_op jit(solution)/shard_map/ppermute | solution.py:13
  219.4 21.0 %collective-permute-start.16 = (bf16[384,512]{1,0:T(8,128)(2,1)S(1)}, bf16[384,512]{1,0:T(8,128)(2,1)S(1)}, u32[]{:S(2)}, u32[]{:S(2)}) collective-permute-start(bf16[384,512]{1,0:T(8,128)(2,1)S(1)} %get-tuple-element.33), channel_id=1, source_target_pairs={{0,2},{1,3},{2,4},{3,5},{4,6},{5,7},{6,0},{7,1},{8,10},{9,11},{10,... | collective-permute-start | bytes 1179656 | tf_op jit(solution)/shard_map/ppermute | solution.py:13
  220.0 20.4 %collective-permute-start.15 = (bf16[384,512]{1,0:T(8,128)(2,1)S(1)}, bf16[384,512]{1,0:T(8,128)(2,1)S(1)}, u32[]{:S(2)}, u32[]{:S(2)}) collective-permute-start(bf16[384,512]{1,0:T(8,128)(2,1)S(1)} %get-tuple-element.32), channel_id=1, source_target_pairs={{0,4},{1,5},{2,6},{3,7},{4,0},{5,1},{6,2},{7,3},{8,12},{9,13},{10,... | collective-permute-start | bytes 1179656 | tf_op jit(solution)/shard_map/ppermute | solution.py:13
Sparse Core Ops, SparseCore 0:
  9.7 92.0 all-gather.2
  103.6 75.0 all-gather.4

commit v3 on v2

--- a/solution.py
+++ b/solution.py
@@ -123,17 +123,21 @@
     )(gated, taps)
 
 
-def shares(mixed, held, fetched, offsets, across=None):
+def shares(mixed, held, fetched, offsets, across=None, parts=1):
     tokens, width = mixed.shape
     count = len(offsets)
     size = held.shape[0] // (2 * count)
-    sent = count if across is None else sum(d != 0 for d in offsets)
-    outs = [jax.ShapeDtypeStruct((sent, tokens, size), jnp.bfloat16)]
-    outs += [jax.ShapeDtypeStruct((tokens, size), jnp.float32)] * (sent < count)
+    piece = size // parts
+    if across is None:
+        outs = [jax.ShapeDtypeStruct((count, tokens, size), jnp.bfloat16)]
+    else:
+        sent = parts * sum(d != 0 for d in offsets)
+        outs = [jax.ShapeDtypeStruct((tokens, piece), jnp.bfloat16)] * sent
+        outs += [jax.ShapeDtypeStruct((tokens, size), jnp.float32)] * (0 in offsets)
     given = [] if across is None else [across]
 
     def kernel(mixed_ref, held_ref, fetched_ref, *refs):
-        arrived, (pairs_ref, *own_ref) = refs[: len(given)], refs[len(given) :]
+        arrived, out_refs = refs[: len(given)], refs[len(given) :]
         core = lax.axis_index("tp") % 2
         side = core if arrived else 1 - core
         odd = lax.axis_index("grp") % 2 == 1
@@ -149,9 +153,12 @@
                 if arrived:
                     part += arrived[0][i, :, pl.ds(j, width)].astype(jnp.float32)
                 if arrived and d == 0:
-                    own_ref[0][:, pl.ds(j, width)] = part
+                    out_refs[-1][:, pl.ds(j, width)] = part
+                elif arrived:
+                    into = out_refs[i * parts + j // piece]
+                    into[:, pl.ds(j % piece, width)] = part.astype(jnp.bfloat16)
                 else:
-                    pairs_ref[i, :, pl.ds(j, width)] = part.astype(jnp.bfloat16)
+                    out_refs[0][i, :, pl.ds(j, width)] = part.astype(jnp.bfloat16)
 
     whole = pl.BlockSpec(memory_space=pltpu.VMEM)
     return pl.pallas_call(
@@ -167,6 +174,10 @@
         ),
         name="shares",
     )(mixed, held, fetched, *given)
+
+
+def joined(a, b):
+    return (a.astype(jnp.float32) + b.astype(jnp.float32)).astype(jnp.bfloat16)
 
 
 def over_lanes(part):
@@ -232,21 +243,33 @@
         gated = project(pieces, inv_rms, taken[layer], width)
         conved = depthwise(gated, conv_taps[layer], lead)
         sums = jnp.stack([jnp.sum(conved, axis=1), jnp.sum(conved * conved, axis=1)])
-        totals = over_lanes(sums)
-        row_mean = totals[0] / channels
-        spread = totals[1] / channels - row_mean * row_mean
+        stats = over_lanes(sums)
+        row_mean = stats[0] / channels
+        spread = stats[1] / channels - row_mean * row_mean
         normed = (conved - row_mean[:, None]) * lax.rsqrt(spread + epsilon)[:, None] * norm_gain[
             layer
         ] + norm_shift[layer]
         mixed_out = jax.nn.silu(normed).astype(jnp.bfloat16)
-        summed = widened[lead:]
+        totals = [widened[lead:]]
         for g, group in enumerate(groups):
             rows = (mixed_out, held[g], fetched[g], group)
             across = swapped(shares(*rows)[0])
-            pairs, *own = shares(*rows, across)
-            parts = own + [shifted(p, "tp", d) for p, d in zip(pairs, group)]
-            for part in parts:
-                summed += part.astype(jnp.float32)
+            pairs = list(shares(*rows, across, 2 if last else 1))
+            if 0 in group:
+                totals.append(pairs.pop())
+            if not last:
+                totals += [shifted(p, "tp", d) for p, d in zip(pairs, group)]
+            elif g == 0:
+                far_up, far_down, up, up_free = pairs
+                far_up, far_down = shifted(far_up, "tp", 2), shifted(far_down, "tp", -2)
+                up_free = shifted(up_free, "tp", 2)
+            else:
+                down_free, down = pairs
+                up = shifted(joined(up, far_up), "tp", 2)
+                down = jnp.concatenate([down_free, joined(down, far_down)], axis=1)
+                totals.append(shifted(down, "tp", -2))
+                totals.append(jnp.concatenate([up, up_free], axis=1))
+        summed = sum(part.astype(jnp.float32) for part in totals)
         return summed.astype(jnp.bfloat16)
 
     ahead = lead * layer_count

time: 250 us -> 249 us (level)
    ppermute x9 -> x11, waiting for transfers between devices: 37.1 us -> 32.6 us  [shifted(): lax.ppermute(value, axis, [(i, (i + steps) % count) for i in range(count)])]
    ppermute x9 -> x11, starting transfers between devices: 14.8 us -> 16.4 us  [shifted(): lax.ppermute(value, axis, [(i, (i + steps) % count) for i in range(count)])]
  transfers between devices with their start and end apart: 26 -> 28, of which waited for: 13 -> 14; matrix products, arithmetic and copies ran while one was open for 5% -> 4% of each run, Pallas kernels for 6% -> 6%
where the time goes in v3:
time: 249 us
  waiting for transfers between devices  153 us (61%)
  starting transfers between devices  42.3 us (17%)
  Pallas kernels  15 us (6%)
  between operations  14.1 us (6%)
  blocking collectives  9.74 us (4%)
  local copies, waits for them, and re-layouts  9.13 us (4%)
  other arithmetic  5.63 us (2%)
    all_gather x2, waiting for transfers between devices, shards(): taken.append(lax.all_gather(rows, 'sp', axis=0, tiled=True))  91.2 us
    ppermute x11, waiting for transfers between devices, shifted(): lax.ppermute(value, axis, [(i, (i + steps) % count) for i in range(count)])  32.6 us
    ppermute x11, starting transfers between devices, shifted(): lax.ppermute(value, axis, [(i, (i + steps) % count) for i in range(count)])  16.4 us
    all_to_all x3, waiting for transfers between devices, over_lanes(): return lax.all_to_all(everyone, 'tp', 0, 0, tiled=True).sum(axis=0)  13.1 us
    all_to_all x3, starting transfers between devices, over_lanes(): return lax.all_to_all(everyone, 'tp', 0, 0, tiled=True).sum(axis=0)  11.9 us
    all_to_all x1, blocking collectives, over_lanes(): return lax.all_to_all(everyone, 'tp', 0, 0, tiled=True).sum(axis=0)  9.74 us
    ppermute x3, waiting for transfers between devices, fetched_rows(): lax.ppermute(held, 'grp', [(i, i ^ 1) for i in range(lax.axis_size('grp'))])  8.75 us
    pallas_call x2, Pallas kernels, project(): pl.pallas_call(kernel, out_shape=jax.ShapeDtypeStruct((tokens, width), jn...  7.98 us
  transfers between devices with their start and end apart: 28, of which 14 were waited for; matrix products, arithmetic and copies ran while one was open for 4% of the time, Pallas kernels for 6%

profile of v3, /device:TPU:40, one launch (start us, length us, event | category | flops | bytes accessed | tf_op | source)
XLA Modules:
  0.0 248.5 jit_solution(12720135553492969094)
XLA Ops:
  6.6 1.0 fusion.15
  7.6 1.1 slice_bitcast_fusion
  8.8 0.8 pad_maximum_fusion.4
  9.7 0.8 pad_maximum_fusion.5
  10.5 4.7 %collective-permute-start = (bf16[64,512]{1,0:T(8,128)(2,1)S(1)}, bf16[64,512]{1,0:T(8,128)(2,1)S(1)}, u32[]{:S(2)}, u32[]{:S(2)}) collective-permute-start(bf16[64,512]{1,0:T(8,128)(2,1)S(1)} %slice.65), channel_id=1, source_target_pairs={{0,8},{8,16},{16,24},{24,32},{32,40},{40,48},{48,56},{56,64},{64,7... | collective-permute-start | bytes 196616 | tf_op jit(solution)/shard_map/ppermute | solution.py:23
  15.3 1.9 collective-permute-done
  17.1 0.2 multiply_reduce_fusion
  17.4 9.7 %all_to_all.27 = f32[8,1,448]{2,1,0:T(1,128)S(1)} all-to-all(f32[8,1,448]{2,1,0:T(1,128)S(1)} %broadcast_in_dim.25), channel_id=1, replica_groups=mesh['grp'=2,'sp'=16,'tp'=8] {'tp'}, dimensions={0} | all-to-all | bytes 28672 | tf_op jit(solution)/shard_map/all_to_all | solution.py:185
  27.1 2.1 broadcast_in_dim.24
  29.2 4.8 %all-to-all-start = ((bf16[8,448,512]{2,1,0:T(8,128)(2,1)}), bf16[8,448,512]{2,1,0:T(8,128)(2,1)}, u32[]{:S(2)}, u32[]{:S(2)}) async-start(bf16[8,448,512]{2,1,0:T(8,128)(2,1)} %broadcast_in_dim.24), calls=%async_computation | async-start | bytes 7340032 | tf_op jit(solution)/shard_map/all_to_all | solution.py:238
  34.5 67.5 %all-gather.3.cloned.1.call-done.refs_2_ = bf16[4096,640]{1,0:T(8,128)(2,1)} async-done(((bf16[256,640]{1,0:T(8,128)(2,1)}), bf16[4096,640]{1,0:T(8,128)(2,1)}) %all-gather.3.cloned.1.call-update) | async-done | bytes 5242896 | tf_op jit(solution)/shard_map/all_gather | solution.py:208
  102.0 1.3 constant_dynamic-slice_fusion.7
  103.4 0.7 collective-permute-start.1
  104.0 4.0 %project.2.gated_ref = bf16[448,256]{1,0:T(8,128)(2,1)S(1)} custom-call(bf16[8,448,512]{2,1,0:T(8,128)(2,1)} %all-to-all-done.refs_0_, f32[448,1]{1,0:T(8,128)S(1)} %copy.20.refs_1_, bf16[4096,640]{1,0:T(8,128)(2,1)} %all-gather.3.cloned.1.call-done.refs_2_), custom_call_target="tpu_custom_call" | custom-call | flops 1879048192 | bytes 4194304 | tf_op jit(solution)/shard_map/project/pallas_call | solution.py:69
  108.1 1.9 depthwise.2
  110.0 0.2 fusion.12
  110.2 0.6 broadcast_in_dim.26
  110.8 4.2 %all-to-all-start.2 = ((f32[8,2,416]{2,1,0:T(2,128)}), f32[8,2,416]{2,1,0:T(2,128)S(1)}, u32[]{:S(2)}, u32[]{:S(2)}) async-start(f32[8,2,416]{2,1,0:T(2,128)} %broadcast_in_dim.26), calls=%async_computation.2 | async-start | bytes 65536 | tf_op jit(solution)/shard_map/all_to_all | solution.py:185
  115.1 5.4 %all-to-all-done.2 = f32[8,2,416]{2,1,0:T(2,128)S(1)} async-done(((f32[8,2,416]{2,1,0:T(2,128)}), f32[8,2,416]{2,1,0:T(2,128)S(1)}, u32[]{:S(2)}, u32[]{:S(2)}) %all-to-all-start.2) | async-done | bytes 26656 | tf_op jit(solution)/shard_map/all_to_all | solution.py:185
  120.5 0.2 multiply_convert_fusion.2.mixed_ref
  120.8 0.6 shares.6
  121.6 3.6 %collective-permute-done.2.refs_0_ = bf16[4,416,512]{2,1,0:T(8,128)(2,1)S(1)} collective-permute-done((bf16[4,416,512]{2,1,0:T(8,128)(2,1)S(1)}, bf16[4,416,512]{2,1,0:T(8,128)(2,1)S(1)}, u32[]{:S(2)}, u32[]{:S(2)}) %collective-permute-start.2) | collective-permute-done | bytes 1703968 | tf_op jit(solution)/shard_map/ppermute | solution.py:17
  125.1 1.3 shares.7
  126.4 2.5 collective-permute-start.5
  128.9 2.5 %collective-permute-start.3 = (bf16[416,512]{1,0:T(8,128)(2,1)S(1)}, bf16[416,512]{1,0:T(8,128)(2,1)S(1)}, u32[]{:S(2)}, u32[]{:S(2)}) collective-permute-start(bf16[416,512]{1,0:T(8,128)(2,1)S(1)} %get-tuple-element.17), channel_id=1, source_target_pairs={{0,4},{1,5},{2,6},{3,7},{4,0},{5,1},{6,2},{7,3},{8,12},{9,13},{10,... | collective-permute-start | bytes 1277960 | tf_op jit(solution)/shard_map/ppermute | solution.py:13
  131.4 1.1 maximum_convert_fusion
  132.5 15.3 %collective-permute-done.5 = bf16[416,512]{1,0:T(8,128)(2,1)S(1)} collective-permute-done((bf16[416,512]{1,0:T(8,128)(2,1)}, bf16[416,512]{1,0:T(8,128)(2,1)S(1)}, u32[]{:S(2)}, u32[]{:S(2)}) %collective-permute-start.5) | collective-permute-done | bytes 426016 | tf_op jit(solution)/shard_map/ppermute | solution.py:13
  147.8 3.3 %collective-permute-done.4 = bf16[416,512]{1,0:T(8,128)(2,1)S(1)} collective-permute-done((bf16[416,512]{1,0:T(8,128)(2,1)}, bf16[416,512]{1,0:T(8,128)(2,1)S(1)}, u32[]{:S(2)}, u32[]{:S(2)}) %collective-permute-start.4) | collective-permute-done | bytes 426016 | tf_op jit(solution)/shard_map/ppermute | solution.py:13
  151.0 0.4 multiply_reduce_fusion.1
  151.6 0.3 collective-permute-start.6
  151.9 3.2 %collective-permute-start.7 = (bf16[416,512]{1,0:T(8,128)(2,1)S(1)}, bf16[416,512]{1,0:T(8,128)(2,1)S(1)}, u32[]{:S(2)}, u32[]{:S(2)}) collective-permute-start(bf16[416,512]{1,0:T(8,128)(2,1)S(1)} %multiply_convert_fusion.1.refs_0_), channel_id=1, source_target_pairs={{0,6},{1,7},{2,0},{3,1},{4,2},{5,3},{6,4},{7,5},{8,14},{9,15},{10,... | collective-permute-start | bytes 1277960 | tf_op jit(solution)/shard_map/ppermute | solution.py:13
  155.1 23.8 %all-gather.5.cloned.1.call-done.refs_9_ = bf16[4096,640]{1,0:T(8,128)(2,1)} async-done(((bf16[256,640]{1,0:T(8,128)(2,1)}), bf16[4096,640]{1,0:T(8,128)(2,1)}) %all-gather.5.cloned.1.call-update) | async-done | bytes 5242896 | tf_op jit(solution)/shard_map/all_gather | solution.py:208
  178.9 1.3 constant_dynamic-slice_fusion.1
  180.2 0.1 collective-permute-start.9
  180.3 0.6 broadcast_in_dim.27
  180.9 4.2 %all-to-all-start.3 = ((f32[8,1,416]{2,1,0:T(1,128)}), f32[8,1,416]{2,1,0:T(1,128)S(1)}, u32[]{:S(2)}, u32[]{:S(2)}) async-start(f32[8,1,416]{2,1,0:T(1,128)} %broadcast_in_dim.27), calls=%async_computation.3 | async-start | bytes 32768 | tf_op jit(solution)/shard_map/all_to_all | solution.py:185
  185.1 0.5 collective-permute-start.10
  185.6 0.2 collective-permute-start.11
  185.8 0.4 collective-permute-start.12
  186.2 0.8 collective-permute-start.13
  187.0 3.4 %all-to-all-done.3 = f32[8,1,416]{2,1,0:T(1,128)S(1)} async-done(((f32[8,1,416]{2,1,0:T(1,128)}), f32[8,1,416]{2,1,0:T(1,128)S(1)}, u32[]{:S(2)}, u32[]{:S(2)}) %all-to-all-start.3) | async-done | bytes 13344 | tf_op jit(solution)/shard_map/all_to_all | solution.py:185
  190.5 0.1 copy.24.refs_8_
  190.7 4.0 %project.3.gated_ref = bf16[416,256]{1,0:T(8,128)(2,1)S(1)} custom-call(bf16[416,512]{1,0:T(8,128)(2,1)S(1)} %multiply_convert_fusion.1.refs_0_, bf16[416,512]{1,0:T(8,128)(2,1)S(1)} %collective-permute-done.6.refs_1_, bf16[416,512]{1,0:T(8,128)(2,1)S(1)} %collective-permute-done.7.refs_2_, bf16[416,512]{1,0:T(8,128)(2,1)S(1)} %collective-permute-done.8.refs_3_, ...), custom_call_target="tpu_custom_call" | custom-call | flops 1744830464 | bytes 4194304 | tf_op jit(solution)/shard_map/project/pallas_call | solution.py:69
  194.7 1.6 depthwise.3
  196.3 0.2 fusion.13
  196.5 0.6 broadcast_in_dim.28
  197.1 3.5 %all-to-all-start.4 = ((f32[8,2,384]{2,1,0:T(2,128)}), f32[8,2,384]{2,1,0:T(2,128)S(1)}, u32[]{:S(2)}, u32[]{:S(2)}) async-start(f32[8,2,384]{2,1,0:T(2,128)} %broadcast_in_dim.28), calls=%async_computation.4 | async-start | bytes 49152 | tf_op jit(solution)/shard_map/all_to_all | solution.py:185
  200.7 0.8 collective-permute-start.15
  201.6 4.3 %all-to-all-done.4 = f32[8,2,384]{2,1,0:T(2,128)S(1)} async-done(((f32[8,2,384]{2,1,0:T(2,128)}), f32[8,2,384]{2,1,0:T(2,128)S(1)}, u32[]{:S(2)}, u32[]{:S(2)}) %all-to-all-start.4) | async-done | bytes 24608 | tf_op jit(solution)/shard_map/all_to_all | solution.py:185
  205.9 0.2 multiply_convert_fusion.3.mixed_ref
  206.1 8.7 %collective-permute-done.15.fetched_ref = bf16[2048,128]{1,0:T(8,128)(2,1)S(1)} collective-permute-done((bf16[2048,128]{1,0:T(8,128)(2,1)S(1)}, bf16[2048,128]{1,0:T(8,128)(2,1)S(1)}, u32[]{:S(2)}, u32[]{:S(2)}) %collective-permute-start.15) | collective-permute-done | bytes 524320 | tf_op jit(solution)/shard_map/ppermute | solution.py:189
  214.9 0.4 shares.10
  215.4 0.4 shares.8
  215.8 0.6 collective-permute-start.14
  216.4 1.3 collective-permute-done.16.refs_0_
  217.7 0.4 shares.11
  218.1 3.3 %collective-permute-start.17 = (bf16[384,256]{1,0:T(8,128)(2,1)S(1)}, bf16[384,256]{1,0:T(8,128)(2,1)S(1)}, u32[]{:S(2)}, u32[]{:S(2)}) collective-permute-start(bf16[384,256]{1,0:T(8,128)(2,1)S(1)} %get-tuple-element.23), channel_id=1, source_target_pairs={{0,6},{1,7},{2,0},{3,1},{4,2},{5,3},{6,4},{7,5},{8,14},{9,15},{10,... | collective-permute-start | bytes 589832 | tf_op jit(solution)/shard_map/ppermute | solution.py:13
  221.4 0.7 collective-permute-start.19
  222.1 0.4 shares.9
  222.5 3.3 %collective-permute-done.17 = bf16[384,256]{1,0:T(8,128)(2,1)S(1)} collective-permute-done((bf16[384,256]{1,0:T(8,128)(2,1)S(1)}, bf16[384,256]{1,0:T(8,128)(2,1)S(1)}, u32[]{:S(2)}, u32[]{:S(2)}) %collective-permute-start.17) | collective-permute-done | bytes 196640 | tf_op jit(solution)/shard_map/ppermute | solution.py:13
  225.9 3.8 %collective-permute-start.18 = (bf16[384,512]{1,0:T(8,128)(2,1)S(1)}, bf16[384,512]{1,0:T(8,128)(2,1)S(1)}, u32[]{:S(2)}, u32[]{:S(2)}) collective-permute-start(bf16[384,512]{1,0:T(8,128)(2,1)S(1)} %pad_maximum_fusion.3), channel_id=1, source_target_pairs={{0,6},{1,7},{2,0},{3,1},{4,2},{5,3},{6,4},{7,5},{8,14},{9,15},{10,... | collective-permute-start | bytes 1179656 | tf_op jit(solution)/shard_map/ppermute | solution.py:13
  229.7 3.7 %collective-permute-done.19 = bf16[384,256]{1,0:T(8,128)(2,1)S(1)} collective-permute-done((bf16[384,256]{1,0:T(8,128)(2,1)S(1)}, bf16[384,256]{1,0:T(8,128)(2,1)S(1)}, u32[]{:S(2)}, u32[]{:S(2)}) %collective-permute-start.19) | collective-permute-done | bytes 196640 | tf_op jit(solution)/shard_map/ppermute | solution.py:13
  233.7 7.0 %collective-permute-done.20 = bf16[384,256]{1,0:T(8,128)(2,1)S(1)} collective-permute-done((bf16[384,256]{1,0:T(8,128)(2,1)S(1)}, bf16[384,256]{1,0:T(8,128)(2,1)S(1)}, u32[]{:S(2)}, u32[]{:S(2)}) %collective-permute-start.20) | collective-permute-done | bytes 196640 | tf_op jit(solution)/shard_map/ppermute | solution.py:13
  240.7 1.0 fusion.6
  (71 shorter events, 1.5 us)
Async XLA Ops:
  6.5 4.0 %copy-start.2 = (bf16[384,512]{1,0:T(8,128)(2,1)S(1)}, bf16[384,512]{1,0:T(8,128)(2,1)}, u32[]{:S(2)}) copy-start(bf16[384,512]{1,0:T(8,128)(2,1)} %param.8) | copy-start | bytes 1179652
  6.5 8.7 %copy-start.4 = (f32[2,512]{1,0:T(2,128)S(1)}, f32[2,512]{1,0:T(2,128)}, u32[]{:S(2)}) copy-start(f32[2,512]{1,0:T(2,128)} %param.9) | copy-start | bytes 12292
  6.6 95.4 %all-gather.3.cloned.1.call-start = ((), (), s32[]{:S(2)}) async-start(), calls=%async_computation.5 | async-start | bytes 5570560 | tf_op jit(solution)/shard_map/all_gather | solution.py:208
  9.6 169.3 %all-gather.5.cloned.1.call-start = ((), (), s32[]{:S(2)}) async-start(), calls=%async_computation.6 | async-start | bytes 5570560 | tf_op jit(solution)/shard_map/all_gather | solution.py:208
  10.5 6.6 %collective-permute-start = (bf16[64,512]{1,0:T(8,128)(2,1)S(1)}, bf16[64,512]{1,0:T(8,128)(2,1)S(1)}, u32[]{:S(2)}, u32[]{:S(2)}) collective-permute-start(bf16[64,512]{1,0:T(8,128)(2,1)S(1)} %slice.65), channel_id=1, source_target_pairs={{0,8},{8,16},{16,24},{24,32},{32,40},{40,48},{48,56},{56,64},{64,7... | collective-permute-start | bytes 196616 | tf_op jit(solution)/shard_map/ppermute | solution.py:23
  29.2 5.0 %copy-start.3 = (f32[2,31,256]{2,0,1:T(2,128)S(1)}, f32[2,31,256]{2,0,1:T(2,128)}, u32[]{:S(2)}) copy-start(f32[2,31,256]{2,0,1:T(2,128)} %param.12) | copy-start | bytes 190468
  29.2 5.1 %copy-start.5 = (f32[2,256]{1,0:T(2,128)S(1)}, f32[2,256]{1,0:T(2,128)}, u32[]{:S(2)}) copy-start(f32[2,256]{1,0:T(2,128)} %param.14) | copy-start | bytes 6148
  29.2 74.8 %all-to-all-start = ((bf16[8,448,512]{2,1,0:T(8,128)(2,1)}), bf16[8,448,512]{2,1,0:T(8,128)(2,1)}, u32[]{:S(2)}, u32[]{:S(2)}) async-start(bf16[8,448,512]{2,1,0:T(8,128)(2,1)} %broadcast_in_dim.24), calls=%async_computation | async-start | bytes 7340032 | tf_op jit(solution)/shard_map/all_to_all | solution.py:238
  103.3 11.7 %copy-start.6 = (f32[2,256]{1,0:T(2,128)S(1)}, f32[2,256]{1,0:T(2,128)}, u32[]{:S(2)}) copy-start(f32[2,256]{1,0:T(2,128)} %param.13) | copy-start | bytes 6148
  103.4 17.4 %collective-permute-start.1 = (bf16[4096,128]{1,0:T(8,128)(2,1)S(1)}, bf16[4096,128]{1,0:T(8,128)(2,1)S(1)}, u32[]{:S(2)}, u32[]{:S(2)}) collective-permute-start(bf16[4096,128]{1,0:T(8,128)(2,1)S(1)} %pad_maximum_fusion.held_ref), channel_id=1, source_target_pairs={{0,128},{128,0},{1,129},{129,1},{2,130},{130,2},{3,131},{131,3},{4... | collective-permute-start | bytes 3145736 | tf_op jit(solution)/shard_map/ppermute | solution.py:189
  110.8 9.6 %all-to-all-start.2 = ((f32[8,2,416]{2,1,0:T(2,128)}), f32[8,2,416]{2,1,0:T(2,128)S(1)}, u32[]{:S(2)}, u32[]{:S(2)}) async-start(f32[8,2,416]{2,1,0:T(2,128)} %broadcast_in_dim.26), calls=%async_computation.2 | async-start | bytes 65536 | tf_op jit(solution)/shard_map/all_to_all | solution.py:185
  121.4 3.7 %collective-permute-start.2 = (bf16[4,416,512]{2,1,0:T(8,128)(2,1)S(1)}, bf16[4,416,512]{2,1,0:T(8,128)(2,1)S(1)}, u32[]{:S(2)}, u32[]{:S(2)}) collective-permute-start(bf16[4,416,512]{2,1,0:T(8,128)(2,1)S(1)} %shares.6), channel_id=1, source_target_pairs={{0,1},{1,0},{2,3},{3,2},{4,5},{5,4},{6,7},{7,6},{8,9},{9,8},{10,11... | collective-permute-start | bytes 5111816 | tf_op jit(solution)/shard_map/ppermute | solution.py:17
  126.4 21.3 %collective-permute-start.5 = (bf16[416,512]{1,0:T(8,128)(2,1)}, bf16[416,512]{1,0:T(8,128)(2,1)S(1)}, u32[]{:S(2)}, u32[]{:S(2)}) collective-permute-start(bf16[416,512]{1,0:T(8,128)(2,1)} %get-tuple-element.19), channel_id=1, source_target_pairs={{0,6},{1,7},{2,0},{3,1},{4,2},{5,3},{6,4},{7,5},{8,14},{9,15},{10,... | collective-permute-start | bytes 1277960 | tf_op jit(solution)/shard_map/ppermute | solution.py:13
  128.9 22.1 %collective-permute-start.4 = (bf16[416,512]{1,0:T(8,128)(2,1)}, bf16[416,512]{1,0:T(8,128)(2,1)S(1)}, u32[]{:S(2)}, u32[]{:S(2)}) collective-permute-start(bf16[416,512]{1,0:T(8,128)(2,1)} %get-tuple-element.18), channel_id=1, source_target_pairs={{0,2},{1,3},{2,4},{3,5},{4,6},{5,7},{6,0},{7,1},{8,10},{9,11},{10,... | collective-permute-start | bytes 1277960 | tf_op jit(solution)/shard_map/ppermute | solution.py:13
  128.9 22.1 %collective-permute-start.3 = (bf16[416,512]{1,0:T(8,128)(2,1)S(1)}, bf16[416,512]{1,0:T(8,128)(2,1)S(1)}, u32[]{:S(2)}, u32[]{:S(2)}) collective-permute-start(bf16[416,512]{1,0:T(8,128)(2,1)S(1)} %get-tuple-element.17), channel_id=1, source_target_pairs={{0,4},{1,5},{2,6},{3,7},{4,0},{5,1},{6,2},{7,3},{8,12},{9,13},{10,... | collective-permute-start | bytes 1277960 | tf_op jit(solution)/shard_map/ppermute | solution.py:13
  151.5 3.6 %copy-start = (f32[416,512]{1,0:T(8,128)}, f32[416,512]{1,0:T(8,128)S(1)}, u32[]{:S(2)}) copy-start(f32[416,512]{1,0:T(8,128)S(1)} %get-tuple-element.34) | copy-start | bytes 2555908
  151.6 33.5 %collective-permute-start.6 = (bf16[416,512]{1,0:T(8,128)(2,1)S(1)}, bf16[416,512]{1,0:T(8,128)(2,1)S(1)}, u32[]{:S(2)}, u32[]{:S(2)}) collective-permute-start(bf16[416,512]{1,0:T(8,128)(2,1)S(1)} %multiply_convert_fusion.1.refs_0_), channel_id=1, source_target_pairs={{0,2},{1,3},{2,4},{3,5},{4,6},{5,7},{6,0},{7,1},{8,10},{9,11},{10,... | collective-permute-start | bytes 1277960 | tf_op jit(solution)/shard_map/ppermute | solution.py:13
  151.9 33.7 %collective-permute-start.7 = (bf16[416,512]{1,0:T(8,128)(2,1)S(1)}, bf16[416,512]{1,0:T(8,128)(2,1)S(1)}, u32[]{:S(2)}, u32[]{:S(2)}) collective-permute-start(bf16[416,512]{1,0:T(8,128)(2,1)S(1)} %multiply_convert_fusion.1.refs_0_), channel_id=1, source_target_pairs={{0,6},{1,7},{2,0},{3,1},{4,2},{5,3},{6,4},{7,5},{8,14},{9,15},{10,... | collective-permute-start | bytes 1277960 | tf_op jit(solution)/shard_map/ppermute | solution.py:13
  155.1 30.7 %collective-permute-start.8 = (bf16[416,512]{1,0:T(8,128)(2,1)S(1)}, bf16[416,512]{1,0:T(8,128)(2,1)S(1)}, u32[]{:S(2)}, u32[]{:S(2)}) collective-permute-start(bf16[416,512]{1,0:T(8,128)(2,1)S(1)} %multiply_convert_fusion.1.refs_0_), channel_id=1, source_target_pairs={{0,4},{1,5},{2,6},{3,7},{4,0},{5,1},{6,2},{7,3},{8,12},{9,13},{10,... | collective-permute-start | bytes 1277960 | tf_op jit(solution)/shard_map/ppermute | solution.py:13
  180.2 10.5 %collective-permute-start.9 = (bf16[416,512]{1,0:T(8,128)(2,1)S(1)}, bf16[416,512]{1,0:T(8,128)(2,1)}, u32[]{:S(2)}, u32[]{:S(2)}) collective-permute-start(bf16[416,512]{1,0:T(8,128)(2,1)S(1)} %multiply_convert_fusion.1.refs_0_), channel_id=1, source_target_pairs={{0,1},{1,0},{2,3},{3,2},{4,5},{5,4},{6,7},{7,6},{8,9},{9,8},{10,11... | collective-permute-start | bytes 1277960 | tf_op jit(solution)/shard_map/ppermute | solution.py:17
  180.9 9.5 %all-to-all-start.3 = ((f32[8,1,416]{2,1,0:T(1,128)}), f32[8,1,416]{2,1,0:T(1,128)S(1)}, u32[]{:S(2)}, u32[]{:S(2)}) async-start(f32[8,1,416]{2,1,0:T(1,128)} %broadcast_in_dim.27), calls=%async_computation.3 | async-start | bytes 32768 | tf_op jit(solution)/shard_map/all_to_all | solution.py:185
  185.1 5.6 %collective-permute-start.10 = (bf16[416,512]{1,0:T(8,128)(2,1)S(1)}, bf16[416,512]{1,0:T(8,128)(2,1)}, u32[]{:S(2)}, u32[]{:S(2)}) collective-permute-start(bf16[416,512]{1,0:T(8,128)(2,1)S(1)} %collective-permute-done.6.refs_1_), channel_id=1, source_target_pairs={{0,1},{1,0},{2,3},{3,2},{4,5},{5,4},{6,7},{7,6},{8,9},{9,8},{10,11... | collective-permute-start | bytes 1277960 | tf_op jit(solution)/shard_map/ppermute | solution.py:17
  185.6 5.1 %collective-permute-start.11 = (bf16[416,512]{1,0:T(8,128)(2,1)S(1)}, bf16[416,512]{1,0:T(8,128)(2,1)}, u32[]{:S(2)}, u32[]{:S(2)}) collective-permute-start(bf16[416,512]{1,0:T(8,128)(2,1)S(1)} %collective-permute-done.7.refs_2_), channel_id=1, source_target_pairs={{0,1},{1,0},{2,3},{3,2},{4,5},{5,4},{6,7},{7,6},{8,9},{9,8},{10,11... | collective-permute-start | bytes 1277960 | tf_op jit(solution)/shard_map/ppermute | solution.py:17
  185.8 4.9 %collective-permute-start.12 = (bf16[416,512]{1,0:T(8,128)(2,1)S(1)}, bf16[416,512]{1,0:T(8,128)(2,1)}, u32[]{:S(2)}, u32[]{:S(2)}) collective-permute-start(bf16[416,512]{1,0:T(8,128)(2,1)S(1)} %collective-permute-done.8.refs_3_), channel_id=1, source_target_pairs={{0,1},{1,0},{2,3},{3,2},{4,5},{5,4},{6,7},{7,6},{8,9},{9,8},{10,11... | collective-permute-start | bytes 1277960 | tf_op jit(solution)/shard_map/ppermute | solution.py:17
  186.2 29.3 %collective-permute-start.13 = (bf16[2048,128]{1,0:T(8,128)(2,1)S(1)}, bf16[2048,128]{1,0:T(8,128)(2,1)S(1)}, u32[]{:S(2)}, u32[]{:S(2)}) collective-permute-start(bf16[2048,128]{1,0:T(8,128)(2,1)S(1)} %pad_maximum_fusion.1.held_ref), channel_id=1, source_target_pairs={{0,128},{128,0},{1,129},{129,1},{2,130},{130,2},{3,131},{131,3},{4... | collective-permute-start | bytes 1572872 | tf_op jit(solution)/shard_map/ppermute | solution.py:189
  197.1 8.7 %all-to-all-start.4 = ((f32[8,2,384]{2,1,0:T(2,128)}), f32[8,2,384]{2,1,0:T(2,128)S(1)}, u32[]{:S(2)}, u32[]{:S(2)}) async-start(f32[8,2,384]{2,1,0:T(2,128)} %broadcast_in_dim.28), calls=%async_computation.4 | async-start | bytes 49152 | tf_op jit(solution)/shard_map/all_to_all | solution.py:185
  200.7 14.2 %collective-permute-start.15 = (bf16[2048,128]{1,0:T(8,128)(2,1)S(1)}, bf16[2048,128]{1,0:T(8,128)(2,1)S(1)}, u32[]{:S(2)}, u32[]{:S(2)}) collective-permute-start(bf16[2048,128]{1,0:T(8,128)(2,1)S(1)} %pad_maximum_fusion.2.held_ref), channel_id=1, source_target_pairs={{0,128},{128,0},{1,129},{129,1},{2,130},{130,2},{3,131},{131,3},{4... | collective-permute-start | bytes 1572872 | tf_op jit(solution)/shard_map/ppermute | solution.py:189
  215.3 2.4 collective-permute-start.16
  215.8 6.3 %collective-permute-start.14 = (bf16[2,384,512]{2,1,0:T(8,128)(2,1)S(1)}, bf16[2,384,512]{2,1,0:T(8,128)(2,1)S(1)}, u32[]{:S(2)}, u32[]{:S(2)}) collective-permute-start(bf16[2,384,512]{2,1,0:T(8,128)(2,1)S(1)} %shares.8), channel_id=1, source_target_pairs={{0,1},{1,0},{2,3},{3,2},{4,5},{5,4},{6,7},{7,6},{8,9},{9,8},{10,11... | collective-permute-start | bytes 2359304 | tf_op jit(solution)/shard_map/ppermute | solution.py:17
  218.1 22.6 %copy-start.1 = (f32[416,512]{1,0:T(8,128)S(1)}, f32[416,512]{1,0:T(8,128)}, u32[]{:S(2)}) copy-start(f32[416,512]{1,0:T(8,128)} %copy-done) | copy-start | bytes 2555908
  218.1 7.8 %collective-permute-start.17 = (bf16[384,256]{1,0:T(8,128)(2,1)S(1)}, bf16[384,256]{1,0:T(8,128)(2,1)S(1)}, u32[]{:S(2)}, u32[]{:S(2)}) collective-permute-start(bf16[384,256]{1,0:T(8,128)(2,1)S(1)} %get-tuple-element.23), channel_id=1, source_target_pairs={{0,6},{1,7},{2,0},{3,1},{4,2},{5,3},{6,4},{7,5},{8,14},{9,15},{10,... | collective-permute-start | bytes 589832 | tf_op jit(solution)/shard_map/ppermute | solution.py:13
  221.4 12.3 %collective-permute-start.21 = (bf16[384,256]{1,0:T(8,128)(2,1)S(1)}, bf16[384,256]{1,0:T(8,128)(2,1)S(1)}, u32[]{:S(2)}, u32[]{:S(2)}) collective-permute-start(bf16[384,256]{1,0:T(8,128)(2,1)S(1)} %get-tuple-element.26), channel_id=1, source_target_pairs={{0,2},{1,3},{2,4},{3,5},{4,6},{5,7},{6,0},{7,1},{8,10},{9,11},{10,... | collective-permute-start | bytes 589832 | tf_op jit(solution)/shard_map/ppermute | solution.py:13
  221.4 12.1 %collective-permute-start.19 = (bf16[384,256]{1,0:T(8,128)(2,1)S(1)}, bf16[384,256]{1,0:T(8,128)(2,1)S(1)}, u32[]{:S(2)}, u32[]{:S(2)}) collective-permute-start(bf16[384,256]{1,0:T(8,128)(2,1)S(1)} %get-tuple-element.25), channel_id=1, source_target_pairs={{0,2},{1,3},{2,4},{3,5},{4,6},{5,7},{6,0},{7,1},{8,10},{9,11},{10,... | collective-permute-start | bytes 589832 | tf_op jit(solution)/shard_map/ppermute | solution.py:13
  225.9 14.7 %collective-permute-start.18 = (bf16[384,512]{1,0:T(8,128)(2,1)S(1)}, bf16[384,512]{1,0:T(8,128)(2,1)S(1)}, u32[]{:S(2)}, u32[]{:S(2)}) collective-permute-start(bf16[384,512]{1,0:T(8,128)(2,1)S(1)} %pad_maximum_fusion.3), channel_id=1, source_target_pairs={{0,6},{1,7},{2,0},{3,1},{4,2},{5,3},{6,4},{7,5},{8,14},{9,15},{10,... | collective-permute-start | bytes 1179656 | tf_op jit(solution)/shard_map/ppermute | solution.py:13
  233.5 7.1 %collective-permute-start.20 = (bf16[384,256]{1,0:T(8,128)(2,1)S(1)}, bf16[384,256]{1,0:T(8,128)(2,1)S(1)}, u32[]{:S(2)}, u32[]{:S(2)}) collective-permute-start(bf16[384,256]{1,0:T(8,128)(2,1)S(1)} %add_convert_fusion), channel_id=1, source_target_pairs={{0,2},{1,3},{2,4},{3,5},{4,6},{5,7},{6,0},{7,1},{8,10},{9,11},{10,... | collective-permute-start | bytes 589832 | tf_op jit(solution)/shard_map/ppermute | solution.py:13
Sparse Core Ops, SparseCore 0:
  9.7 92.2 all-gather.2
  103.8 75.0 all-gather.4

commit v4 on v3

--- a/solution.py
+++ b/solution.py
@@ -87,6 +87,36 @@
     )(*given, inv_rms, rows)
 
 
+def packed(layer, w_value, w_gate, w_out):
+    depth, width = w_value.shape[1:]
+    columns = w_out.shape[2]
+    half = columns // 2
+
+    def kernel(value_ref, gate_ref, out_ref, rows_ref):
+        odd = lax.axis_index("grp") % 2 == 1
+        rows_ref[:, pl.ds(0, width)] = value_ref[...]
+        rows_ref[:, pl.ds(width, width)] = gate_ref[...]
+        rows_ref[:, pl.ds(2 * width, half)] = jnp.where(
+            odd, out_ref[:, pl.ds(half, half)], out_ref[:, pl.ds(0, half)]
+        )
+
+    def at(*shape):
+        return pl.BlockSpec((None, *shape), lambda i: (layer, 0, 0))
+
+    return pl.pallas_call(
+        kernel,
+        out_shape=jax.ShapeDtypeStruct((depth, 2 * width + half), w_value.dtype),
+        grid=(1,),
+        in_specs=[at(depth, width), at(depth, width), at(depth, columns)],
+        out_specs=pl.BlockSpec((depth, 2 * width + half), lambda i: (0, 0)),
+        compiler_params=pltpu.CompilerParams(vmem_limit_bytes=63 << 20),
+        cost_estimate=pl.CostEstimate(
+            flops=depth * width, bytes_accessed=10 * depth * width, transcendentals=0
+        ),
+        name="packed",
+    )(w_value, w_gate, w_out)
+
+
 def depthwise(gated, taps, lead):
     total_rows, width = gated.shape
     tokens = total_rows - lead
@@ -200,11 +230,9 @@
     offsets = offsets_of(tp)
 
     half = w_out.shape[2] // 2
-    mine = lax.axis_index("grp") % 2 * half
     taken = []
     for layer in range(layer_count):
-        part = lax.dynamic_slice_in_dim(w_out[layer], mine, half, 1)
-        rows = jnp.concatenate([w_value[layer], w_gate[layer], part], axis=1)
+        rows = packed(layer, w_value, w_gate, w_out)
         taken.append(lax.all_gather(rows, "sp", axis=0, tiled=True))
 
     lead = -(-reach_rows // 32) * 32
@@ -212,6 +240,17 @@
     def run(layer, current):
         last = layer == layer_count - 1
         groups = [offsets[: tp // 4], offsets[tp // 4 :]] if last else [offsets]
+        widened = current.astype(jnp.float32)
+        scaled = (widened * in_gain[layer]).astype(jnp.bfloat16)
+        if last:
+            near = [scaled if d == 0 else shifted(scaled, "tp", -d) for d in offsets]
+        else:
+            everyone = jnp.broadcast_to(scaled[None], (tp, *scaled.shape))
+            pieces = lax.all_to_all(everyone, "tp", 0, 0, tiled=True)
+        squares = over_lanes(jnp.sum(widened * widened, axis=1))
+        inv_rms = lax.rsqrt(squares / features + epsilon)
+        lane, inv_rms = lax.optimization_barrier((lax.axis_index("tp") // 2 * 2, inv_rms))
+        inv_rms = inv_rms[:, None]
         chip = 2 * (features // tp)
         held, fetched = [], []
         for group in groups:
@@ -220,7 +259,7 @@
                     [
                         lax.dynamic_slice(
                             taken[layer],
-                            ((lax.axis_index("tp") // 2 * 2 + d) % tp // 2 * chip, 2 * width),
+                            ((lane + d) % tp // 2 * chip, 2 * width),
                             (chip, half),
                         )
                         for d in group
@@ -229,15 +268,6 @@
                 )
             )
             fetched.append(fetched_rows(held[-1]))
-        widened = current.astype(jnp.float32)
-        scaled = (widened * in_gain[layer]).astype(jnp.bfloat16)
-        if last:
-            near = [scaled if d == 0 else shifted(scaled, "tp", -d) for d in offsets]
-        else:
-            everyone = jnp.broadcast_to(scaled[None], (tp, *scaled.shape))
-            pieces = lax.all_to_all(everyone, "tp", 0, 0, tiled=True)
-        squares = over_lanes(jnp.sum(widened * widened, axis=1))
-        inv_rms = lax.rsqrt(squares / features + epsilon)[:, None]
         if last:
             pieces = near[::-1] + [swapped(piece) for piece in near[::-1]]
         gated = project(pieces, inv_rms, taken[layer], width)

time: 249 us -> 240 us (0.964)
  waiting for transfers between devices: 153 us -> 140 us
  Pallas kernels: 15 us -> 18.6 us
    all_gather x2, waiting for transfers between devices: 91.2 us -> 71.4 us  [shards(): taken.append(lax.all_gather(rows, 'sp', axis=0, tiled=True))]
    all_to_all x3, waiting for transfers between devices: 13.1 us -> 20.3 us  [over_lanes(): return lax.all_to_all(everyone, 'tp', 0, 0, tiled=True).sum(axis=0)]
    pallas_call x0 -> x2, Pallas kernels: none -> 3.64 us  [packed(): pl.pallas_call(kernel, out_shape=jax.ShapeDtypeStruct((depth, 2 * width +...]
  transfers between devices with their start and end apart: 28 -> 28, of which waited for: 14 -> 14; matrix products, arithmetic and copies ran while one was open for 4% -> 4% of each run, Pallas kernels for 6% -> 7%
where the time goes in v4:
time: 240 us; the launch traced here: 239 us
  waiting for transfers between devices  140 us (58%)
  starting transfers between devices  44.6 us (19%)
  Pallas kernels  18.6 us (8%)
  between operations  14.1 us (6%)
  blocking collectives  9.74 us (4%)
  local copies, waits for them, and re-layouts  7.84 us (3%)
  other arithmetic  4.11 us (2%)
    all_gather x2, waiting for transfers between devices, shards(): taken.append(lax.all_gather(rows, 'sp', axis=0, tiled=True))  71.4 us
    ppermute x11, waiting for transfers between devices, shifted(): lax.ppermute(value, axis, [(i, (i + steps) % count) for i in range(count)])  32.8 us
    all_to_all x3, waiting for transfers between devices, over_lanes(): return lax.all_to_all(everyone, 'tp', 0, 0, tiled=True).sum(axis=0)  20.3 us
    ppermute x11, starting transfers between devices, shifted(): lax.ppermute(value, axis, [(i, (i + steps) % count) for i in range(count)])  16.4 us
    all_to_all x3, starting transfers between devices, over_lanes(): return lax.all_to_all(everyone, 'tp', 0, 0, tiled=True).sum(axis=0)  13.7 us
    all_to_all x1, blocking collectives, over_lanes(): return lax.all_to_all(everyone, 'tp', 0, 0, tiled=True).sum(axis=0)  9.74 us
    ppermute x3, waiting for transfers between devices, fetched_rows(): lax.ppermute(held, 'grp', [(i, i ^ 1) for i in range(lax.axis_size('grp'))])  8.81 us
    pallas_call x2, Pallas kernels, project(): pl.pallas_call(kernel, out_shape=jax.ShapeDtypeStruct((tokens, width), jn...  7.98 us
  transfers between devices with their start and end apart: 28, of which 14 were waited for; matrix products, arithmetic and copies ran while one was open for 4% of the time, Pallas kernels for 7%

profile of v4, /device:TPU:40, one launch (start us, length us, event | category | flops | bytes accessed | tf_op | source)
XLA Modules:
  0.0 239.1 jit_solution(2022363662946784691)
XLA Ops:
  6.6 1.8 packed.2
  8.5 1.8 packed.3
  10.4 4.7 %collective-permute-start = (bf16[64,512]{1,0:T(8,128)(2,1)S(1)}, bf16[64,512]{1,0:T(8,128)(2,1)S(1)}, u32[]{:S(2)}, u32[]{:S(2)}) collective-permute-start(bf16[64,512]{1,0:T(8,128)(2,1)S(1)} %slice.47), channel_id=1, source_target_pairs={{0,8},{8,16},{16,24},{24,32},{32,40},{40,48},{48,56},{56,64},{64,7... | collective-permute-start | bytes 196616 | tf_op jit(solution)/shard_map/ppermute | solution.py:23
  15.2 1.9 collective-permute-done
  17.0 0.2 multiply_reduce_fusion
  17.2 9.7 %all_to_all.27 = f32[8,1,448]{2,1,0:T(1,128)S(1)} all-to-all(f32[8,1,448]{2,1,0:T(1,128)S(1)} %broadcast_in_dim.29), channel_id=1, replica_groups=mesh['grp'=2,'sp'=16,'tp'=8] {'tp'}, dimensions={0} | all-to-all | bytes 28672 | tf_op jit(solution)/shard_map/all_to_all | solution.py:215
  27.0 2.1 broadcast_in_dim.28
  29.1 4.8 %all-to-all-start = ((bf16[8,448,512]{2,1,0:T(8,128)(2,1)}), bf16[8,448,512]{2,1,0:T(8,128)(2,1)}, u32[]{:S(2)}, u32[]{:S(2)}) async-start(bf16[8,448,512]{2,1,0:T(8,128)(2,1)} %broadcast_in_dim.28), calls=%async_computation | async-start | bytes 7340032 | tf_op jit(solution)/shard_map/all_to_all | solution.py:249
  34.4 66.8 %all-gather.3.cloned.1.call-done.refs_2_ = bf16[4096,640]{1,0:T(8,128)(2,1)} async-done(((bf16[256,640]{1,0:T(8,128)(2,1)}), bf16[4096,640]{1,0:T(8,128)(2,1)}) %all-gather.3.cloned.1.call-update) | async-done | bytes 5242896 | tf_op jit(solution)/shard_map/all_gather | solution.py:236
  101.2 1.3 constant_dynamic-slice_fusion.7
  102.6 0.6 collective-permute-start.1
  103.2 4.0 %project.2.gated_ref = bf16[448,256]{1,0:T(8,128)(2,1)S(1)} custom-call(bf16[8,448,512]{2,1,0:T(8,128)(2,1)} %all-to-all-done.refs_0_, f32[448,1]{1,0:T(8,128)S(1)} %copy.20.refs_1_, bf16[4096,640]{1,0:T(8,128)(2,1)} %all-gather.3.cloned.1.call-done.refs_2_), custom_call_target="tpu_custom_call" | custom-call | flops 1879048192 | bytes 4194304 | tf_op jit(solution)/shard_map/project/pallas_call | solution.py:69
  107.2 1.9 depthwise.2
  109.1 0.2 fusion.12
  109.4 0.6 broadcast_in_dim.31
  110.0 4.5 %all-to-all-start.2 = ((f32[8,2,416]{2,1,0:T(2,128)}), f32[8,2,416]{2,1,0:T(2,128)S(1)}, u32[]{:S(2)}, u32[]{:S(2)}) async-start(f32[8,2,416]{2,1,0:T(2,128)} %broadcast_in_dim.31), calls=%async_computation.2 | async-start | bytes 65536 | tf_op jit(solution)/shard_map/all_to_all | solution.py:215
  114.5 5.4 %all-to-all-done.2 = f32[8,2,416]{2,1,0:T(2,128)S(1)} async-done(((f32[8,2,416]{2,1,0:T(2,128)}), f32[8,2,416]{2,1,0:T(2,128)S(1)}, u32[]{:S(2)}, u32[]{:S(2)}) %all-to-all-start.2) | async-done | bytes 26656 | tf_op jit(solution)/shard_map/all_to_all | solution.py:215
  120.0 0.2 multiply_convert_fusion.2.mixed_ref
  120.2 0.6 shares.6
  120.8 0.1 collective-permute-start.2
  121.0 3.6 %collective-permute-done.2.refs_0_ = bf16[4,416,512]{2,1,0:T(8,128)(2,1)S(1)} collective-permute-done((bf16[4,416,512]{2,1,0:T(8,128)(2,1)S(1)}, bf16[4,416,512]{2,1,0:T(8,128)(2,1)S(1)}, u32[]{:S(2)}, u32[]{:S(2)}) %collective-permute-start.2) | collective-permute-done | bytes 1703968 | tf_op jit(solution)/shard_map/ppermute | solution.py:17
  124.6 1.3 shares.7
  125.9 2.8 %collective-permute-start.5 = (bf16[416,512]{1,0:T(8,128)(2,1)}, bf16[416,512]{1,0:T(8,128)(2,1)S(1)}, u32[]{:S(2)}, u32[]{:S(2)}) collective-permute-start(bf16[416,512]{1,0:T(8,128)(2,1)} %get-tuple-element.25), channel_id=1, source_target_pairs={{0,6},{1,7},{2,0},{3,1},{4,2},{5,3},{6,4},{7,5},{8,14},{9,15},{10,... | collective-permute-start | bytes 1277960 | tf_op jit(solution)/shard_map/ppermute | solution.py:13
  128.6 2.2 collective-permute-start.3
  130.9 1.1 maximum_convert_fusion
  132.0 15.5 %collective-permute-done.5 = bf16[416,512]{1,0:T(8,128)(2,1)S(1)} collective-permute-done((bf16[416,512]{1,0:T(8,128)(2,1)}, bf16[416,512]{1,0:T(8,128)(2,1)S(1)}, u32[]{:S(2)}, u32[]{:S(2)}) %collective-permute-start.5) | collective-permute-done | bytes 426016 | tf_op jit(solution)/shard_map/ppermute | solution.py:13
  147.5 3.3 %collective-permute-done.4 = bf16[416,512]{1,0:T(8,128)(2,1)S(1)} collective-permute-done((bf16[416,512]{1,0:T(8,128)(2,1)}, bf16[416,512]{1,0:T(8,128)(2,1)S(1)}, u32[]{:S(2)}, u32[]{:S(2)}) %collective-permute-start.4) | collective-permute-done | bytes 426016 | tf_op jit(solution)/shard_map/ppermute | solution.py:13
  150.8 0.4 multiply_reduce_fusion.1
  151.2 0.9 copy-done
  152.2 0.3 collective-permute-start.6
  152.5 3.2 %collective-permute-start.7 = (bf16[416,512]{1,0:T(8,128)(2,1)S(1)}, bf16[416,512]{1,0:T(8,128)(2,1)S(1)}, u32[]{:S(2)}, u32[]{:S(2)}) collective-permute-start(bf16[416,512]{1,0:T(8,128)(2,1)S(1)} %multiply_convert_fusion.1.refs_0_), channel_id=1, source_target_pairs={{0,6},{1,7},{2,0},{3,1},{4,2},{5,3},{6,4},{7,5},{8,14},{9,15},{10,... | collective-permute-start | bytes 1277960 | tf_op jit(solution)/shard_map/ppermute | solution.py:13
  155.7 0.6 broadcast_in_dim.32
  156.3 4.8 %all-to-all-start.3 = ((f32[8,1,416]{2,1,0:T(1,128)}), f32[8,1,416]{2,1,0:T(1,128)S(1)}, u32[]{:S(2)}, u32[]{:S(2)}) async-start(f32[8,1,416]{2,1,0:T(1,128)} %broadcast_in_dim.32), calls=%async_computation.3 | async-start | bytes 32768 | tf_op jit(solution)/shard_map/all_to_all | solution.py:215
  161.2 0.5 collective-permute-start.9
  161.7 11.1 %all-to-all-done.3 = f32[8,1,416]{2,1,0:T(1,128)S(1)} async-done(((f32[8,1,416]{2,1,0:T(1,128)}), f32[8,1,416]{2,1,0:T(1,128)S(1)}, u32[]{:S(2)}, u32[]{:S(2)}) %all-to-all-start.3) | async-done | bytes 13344 | tf_op jit(solution)/shard_map/all_to_all | solution.py:215
  172.8 0.3 collective-permute-start.10
  173.1 0.3 collective-permute-start.11
  173.4 0.2 collective-permute-start.12
  173.6 0.1 copy.24.refs_8_
  173.8 4.6 %all-gather.5.cloned.1.call-done.refs_9_ = bf16[4096,640]{1,0:T(8,128)(2,1)} async-done(((bf16[256,640]{1,0:T(8,128)(2,1)}), bf16[4096,640]{1,0:T(8,128)(2,1)}) %all-gather.5.cloned.1.call-update) | async-done | bytes 5242896 | tf_op jit(solution)/shard_map/all_gather | solution.py:236
  178.3 1.3 constant_dynamic-slice_fusion.1
  179.7 0.6 collective-permute-start.13
  180.3 4.0 %project.3.gated_ref = bf16[416,256]{1,0:T(8,128)(2,1)S(1)} custom-call(bf16[416,512]{1,0:T(8,128)(2,1)S(1)} %multiply_convert_fusion.1.refs_0_, bf16[416,512]{1,0:T(8,128)(2,1)S(1)} %collective-permute-done.6.refs_1_, bf16[416,512]{1,0:T(8,128)(2,1)S(1)} %collective-permute-done.7.refs_2_, bf16[416,512]{1,0:T(8,128)(2,1)S(1)} %collective-permute-done.8.refs_3_, ...), custom_call_target="tpu_custom_call" | custom-call | flops 1744830464 | bytes 4194304 | tf_op jit(solution)/shard_map/project/pallas_call | solution.py:69
  184.2 1.6 depthwise.3
  185.9 0.2 fusion.13
  186.1 0.6 broadcast_in_dim.34
  186.7 4.4 %all-to-all-start.4 = ((f32[8,2,384]{2,1,0:T(2,128)}), f32[8,2,384]{2,1,0:T(2,128)S(1)}, u32[]{:S(2)}, u32[]{:S(2)}) async-start(f32[8,2,384]{2,1,0:T(2,128)} %broadcast_in_dim.34), calls=%async_computation.4 | async-start | bytes 49152 | tf_op jit(solution)/shard_map/all_to_all | solution.py:215
  191.1 1.6 collective-permute-start.15
  192.7 3.8 %all-to-all-done.4 = f32[8,2,384]{2,1,0:T(2,128)S(1)} async-done(((f32[8,2,384]{2,1,0:T(2,128)}), f32[8,2,384]{2,1,0:T(2,128)S(1)}, u32[]{:S(2)}, u32[]{:S(2)}) %all-to-all-start.4) | async-done | bytes 24608 | tf_op jit(solution)/shard_map/all_to_all | solution.py:215
  196.5 0.2 multiply_convert_fusion.3.mixed_ref
  196.8 8.8 %collective-permute-done.15.fetched_ref = bf16[2048,128]{1,0:T(8,128)(2,1)S(1)} collective-permute-done((bf16[2048,128]{1,0:T(8,128)(2,1)S(1)}, bf16[2048,128]{1,0:T(8,128)(2,1)S(1)}, u32[]{:S(2)}, u32[]{:S(2)}) %collective-permute-start.15) | collective-permute-done | bytes 524320 | tf_op jit(solution)/shard_map/ppermute | solution.py:219
  205.6 0.4 shares.10
  206.1 0.4 shares.8
  206.5 0.6 collective-permute-start.14
  207.1 1.3 collective-permute-done.16.refs_0_
  208.4 0.4 shares.11
  208.8 3.2 %collective-permute-start.17 = (bf16[384,256]{1,0:T(8,128)(2,1)S(1)}, bf16[384,256]{1,0:T(8,128)(2,1)S(1)}, u32[]{:S(2)}, u32[]{:S(2)}) collective-permute-start(bf16[384,256]{1,0:T(8,128)(2,1)S(1)} %get-tuple-element.31), channel_id=1, source_target_pairs={{0,6},{1,7},{2,0},{3,1},{4,2},{5,3},{6,4},{7,5},{8,14},{9,15},{10,... | collective-permute-start | bytes 589832 | tf_op jit(solution)/shard_map/ppermute | solution.py:13
  211.9 0.8 collective-permute-start.19
  212.8 0.4 shares.9
  213.2 3.3 %collective-permute-done.17 = bf16[384,256]{1,0:T(8,128)(2,1)S(1)} collective-permute-done((bf16[384,256]{1,0:T(8,128)(2,1)S(1)}, bf16[384,256]{1,0:T(8,128)(2,1)S(1)}, u32[]{:S(2)}, u32[]{:S(2)}) %collective-permute-start.17) | collective-permute-done | bytes 196640 | tf_op jit(solution)/shard_map/ppermute | solution.py:13
  216.5 3.8 %collective-permute-start.18 = (bf16[384,512]{1,0:T(8,128)(2,1)S(1)}, bf16[384,512]{1,0:T(8,128)(2,1)S(1)}, u32[]{:S(2)}, u32[]{:S(2)}) collective-permute-start(bf16[384,512]{1,0:T(8,128)(2,1)S(1)} %pad_maximum_fusion.3), channel_id=1, source_target_pairs={{0,6},{1,7},{2,0},{3,1},{4,2},{5,3},{6,4},{7,5},{8,14},{9,15},{10,... | collective-permute-start | bytes 1179656 | tf_op jit(solution)/shard_map/ppermute | solution.py:13
  220.3 3.7 %collective-permute-done.19 = bf16[384,256]{1,0:T(8,128)(2,1)S(1)} collective-permute-done((bf16[384,256]{1,0:T(8,128)(2,1)S(1)}, bf16[384,256]{1,0:T(8,128)(2,1)S(1)}, u32[]{:S(2)}, u32[]{:S(2)}) %collective-permute-start.19) | collective-permute-done | bytes 196640 | tf_op jit(solution)/shard_map/ppermute | solution.py:13
  224.2 7.0 %collective-permute-done.20 = bf16[384,256]{1,0:T(8,128)(2,1)S(1)} collective-permute-done((bf16[384,256]{1,0:T(8,128)(2,1)S(1)}, bf16[384,256]{1,0:T(8,128)(2,1)S(1)}, u32[]{:S(2)}, u32[]{:S(2)}) %collective-permute-start.20) | collective-permute-done | bytes 196640 | tf_op jit(solution)/shard_map/ppermute | solution.py:13
  231.2 1.0 fusion.6
  (67 shorter events, 1.3 us)
Async XLA Ops:
  6.5 3.8 %copy-start.2 = (bf16[384,512]{1,0:T(8,128)(2,1)S(1)}, bf16[384,512]{1,0:T(8,128)(2,1)}, u32[]{:S(2)}) copy-start(bf16[384,512]{1,0:T(8,128)(2,1)} %param.8) | copy-start | bytes 1179652
  6.5 8.6 %copy-start.4 = (f32[2,512]{1,0:T(2,128)S(1)}, f32[2,512]{1,0:T(2,128)}, u32[]{:S(2)}) copy-start(f32[2,512]{1,0:T(2,128)} %param.9) | copy-start | bytes 12292
  6.6 94.7 %all-gather.3.cloned.1.call-start = ((), (), s32[]{:S(2)}) async-start(), calls=%async_computation.5 | async-start | bytes 5570560 | tf_op jit(solution)/shard_map/all_gather | solution.py:236
  8.5 169.9 %all-gather.5.cloned.1.call-start = ((), (), s32[]{:S(2)}) async-start(), calls=%async_computation.6 | async-start | bytes 5570560 | tf_op jit(solution)/shard_map/all_gather | solution.py:236
  10.4 6.6 %collective-permute-start = (bf16[64,512]{1,0:T(8,128)(2,1)S(1)}, bf16[64,512]{1,0:T(8,128)(2,1)S(1)}, u32[]{:S(2)}, u32[]{:S(2)}) collective-permute-start(bf16[64,512]{1,0:T(8,128)(2,1)S(1)} %slice.47), channel_id=1, source_target_pairs={{0,8},{8,16},{16,24},{24,32},{32,40},{40,48},{48,56},{56,64},{64,7... | collective-permute-start | bytes 196616 | tf_op jit(solution)/shard_map/ppermute | solution.py:23
  29.1 4.8 %copy-start.3 = (f32[2,31,256]{2,0,1:T(2,128)S(1)}, f32[2,31,256]{2,0,1:T(2,128)}, u32[]{:S(2)}) copy-start(f32[2,31,256]{2,0,1:T(2,128)} %param.12) | copy-start | bytes 190468
  29.1 4.9 %copy-start.5 = (f32[2,256]{1,0:T(2,128)S(1)}, f32[2,256]{1,0:T(2,128)}, u32[]{:S(2)}) copy-start(f32[2,256]{1,0:T(2,128)} %param.14) | copy-start | bytes 6148
  29.1 74.1 %all-to-all-start = ((bf16[8,448,512]{2,1,0:T(8,128)(2,1)}), bf16[8,448,512]{2,1,0:T(8,128)(2,1)}, u32[]{:S(2)}, u32[]{:S(2)}) async-start(bf16[8,448,512]{2,1,0:T(8,128)(2,1)} %broadcast_in_dim.28), calls=%async_computation | async-start | bytes 7340032 | tf_op jit(solution)/shard_map/all_to_all | solution.py:249
  102.6 11.9 %copy-start.6 = (f32[2,256]{1,0:T(2,128)S(1)}, f32[2,256]{1,0:T(2,128)}, u32[]{:S(2)}) copy-start(f32[2,256]{1,0:T(2,128)} %param.13) | copy-start | bytes 6148
  102.6 17.6 %collective-permute-start.1 = (bf16[4096,128]{1,0:T(8,128)(2,1)S(1)}, bf16[4096,128]{1,0:T(8,128)(2,1)S(1)}, u32[]{:S(2)}, u32[]{:S(2)}) collective-permute-start(bf16[4096,128]{1,0:T(8,128)(2,1)S(1)} %pad_maximum_fusion.held_ref), channel_id=1, source_target_pairs={{0,128},{128,0},{1,129},{129,1},{2,130},{130,2},{3,131},{131,3},{4... | collective-permute-start | bytes 3145736 | tf_op jit(solution)/shard_map/ppermute | solution.py:219
  110.0 9.9 %all-to-all-start.2 = ((f32[8,2,416]{2,1,0:T(2,128)}), f32[8,2,416]{2,1,0:T(2,128)S(1)}, u32[]{:S(2)}, u32[]{:S(2)}) async-start(f32[8,2,416]{2,1,0:T(2,128)} %broadcast_in_dim.31), calls=%async_computation.2 | async-start | bytes 65536 | tf_op jit(solution)/shard_map/all_to_all | solution.py:215
  120.8 3.7 %collective-permute-start.2 = (bf16[4,416,512]{2,1,0:T(8,128)(2,1)S(1)}, bf16[4,416,512]{2,1,0:T(8,128)(2,1)S(1)}, u32[]{:S(2)}, u32[]{:S(2)}) collective-permute-start(bf16[4,416,512]{2,1,0:T(8,128)(2,1)S(1)} %shares.6), channel_id=1, source_target_pairs={{0,1},{1,0},{2,3},{3,2},{4,5},{5,4},{6,7},{7,6},{8,9},{9,8},{10,11... | collective-permute-start | bytes 5111816 | tf_op jit(solution)/shard_map/ppermute | solution.py:17
  125.9 21.6 %collective-permute-start.5 = (bf16[416,512]{1,0:T(8,128)(2,1)}, bf16[416,512]{1,0:T(8,128)(2,1)S(1)}, u32[]{:S(2)}, u32[]{:S(2)}) collective-permute-start(bf16[416,512]{1,0:T(8,128)(2,1)} %get-tuple-element.25), channel_id=1, source_target_pairs={{0,6},{1,7},{2,0},{3,1},{4,2},{5,3},{6,4},{7,5},{8,14},{9,15},{10,... | collective-permute-start | bytes 1277960 | tf_op jit(solution)/shard_map/ppermute | solution.py:13
  128.6 22.1 %collective-permute-start.4 = (bf16[416,512]{1,0:T(8,128)(2,1)}, bf16[416,512]{1,0:T(8,128)(2,1)S(1)}, u32[]{:S(2)}, u32[]{:S(2)}) collective-permute-start(bf16[416,512]{1,0:T(8,128)(2,1)} %get-tuple-element.24), channel_id=1, source_target_pairs={{0,2},{1,3},{2,4},{3,5},{4,6},{5,7},{6,0},{7,1},{8,10},{9,11},{10,... | collective-permute-start | bytes 1277960 | tf_op jit(solution)/shard_map/ppermute | solution.py:13
  128.6 22.1 %collective-permute-start.3 = (bf16[416,512]{1,0:T(8,128)(2,1)S(1)}, bf16[416,512]{1,0:T(8,128)(2,1)S(1)}, u32[]{:S(2)}, u32[]{:S(2)}) collective-permute-start(bf16[416,512]{1,0:T(8,128)(2,1)S(1)} %get-tuple-element.23), channel_id=1, source_target_pairs={{0,4},{1,5},{2,6},{3,7},{4,0},{5,1},{6,2},{7,3},{8,12},{9,13},{10,... | collective-permute-start | bytes 1277960 | tf_op jit(solution)/shard_map/ppermute | solution.py:13
  151.2 0.9 copy-start
  152.2 20.6 %collective-permute-start.6 = (bf16[416,512]{1,0:T(8,128)(2,1)S(1)}, bf16[416,512]{1,0:T(8,128)(2,1)S(1)}, u32[]{:S(2)}, u32[]{:S(2)}) collective-permute-start(bf16[416,512]{1,0:T(8,128)(2,1)S(1)} %multiply_convert_fusion.1.refs_0_), channel_id=1, source_target_pairs={{0,2},{1,3},{2,4},{3,5},{4,6},{5,7},{6,0},{7,1},{8,10},{9,11},{10,... | collective-permute-start | bytes 1277960 | tf_op jit(solution)/shard_map/ppermute | solution.py:13
  152.5 20.6 %collective-permute-start.7 = (bf16[416,512]{1,0:T(8,128)(2,1)S(1)}, bf16[416,512]{1,0:T(8,128)(2,1)S(1)}, u32[]{:S(2)}, u32[]{:S(2)}) collective-permute-start(bf16[416,512]{1,0:T(8,128)(2,1)S(1)} %multiply_convert_fusion.1.refs_0_), channel_id=1, source_target_pairs={{0,6},{1,7},{2,0},{3,1},{4,2},{5,3},{6,4},{7,5},{8,14},{9,15},{10,... | collective-permute-start | bytes 1277960 | tf_op jit(solution)/shard_map/ppermute | solution.py:13
  155.7 17.7 %collective-permute-start.8 = (bf16[416,512]{1,0:T(8,128)(2,1)S(1)}, bf16[416,512]{1,0:T(8,128)(2,1)S(1)}, u32[]{:S(2)}, u32[]{:S(2)}) collective-permute-start(bf16[416,512]{1,0:T(8,128)(2,1)S(1)} %multiply_convert_fusion.1.refs_0_), channel_id=1, source_target_pairs={{0,4},{1,5},{2,6},{3,7},{4,0},{5,1},{6,2},{7,3},{8,12},{9,13},{10,... | collective-permute-start | bytes 1277960 | tf_op jit(solution)/shard_map/ppermute | solution.py:13
  156.3 16.4 %all-to-all-start.3 = ((f32[8,1,416]{2,1,0:T(1,128)}), f32[8,1,416]{2,1,0:T(1,128)S(1)}, u32[]{:S(2)}, u32[]{:S(2)}) async-start(f32[8,1,416]{2,1,0:T(1,128)} %broadcast_in_dim.32), calls=%async_computation.3 | async-start | bytes 32768 | tf_op jit(solution)/shard_map/all_to_all | solution.py:215
  161.2 19.1 %collective-permute-start.9 = (bf16[416,512]{1,0:T(8,128)(2,1)S(1)}, bf16[416,512]{1,0:T(8,128)(2,1)}, u32[]{:S(2)}, u32[]{:S(2)}) collective-permute-start(bf16[416,512]{1,0:T(8,128)(2,1)S(1)} %multiply_convert_fusion.1.refs_0_), channel_id=1, source_target_pairs={{0,1},{1,0},{2,3},{3,2},{4,5},{5,4},{6,7},{7,6},{8,9},{9,8},{10,11... | collective-permute-start | bytes 1277960 | tf_op jit(solution)/shard_map/ppermute | solution.py:17
  172.8 7.5 %collective-permute-start.10 = (bf16[416,512]{1,0:T(8,128)(2,1)S(1)}, bf16[416,512]{1,0:T(8,128)(2,1)}, u32[]{:S(2)}, u32[]{:S(2)}) collective-permute-start(bf16[416,512]{1,0:T(8,128)(2,1)S(1)} %collective-permute-done.6.refs_1_), channel_id=1, source_target_pairs={{0,1},{1,0},{2,3},{3,2},{4,5},{5,4},{6,7},{7,6},{8,9},{9,8},{10,11... | collective-permute-start | bytes 1277960 | tf_op jit(solution)/shard_map/ppermute | solution.py:17
  173.1 7.2 %collective-permute-start.11 = (bf16[416,512]{1,0:T(8,128)(2,1)S(1)}, bf16[416,512]{1,0:T(8,128)(2,1)}, u32[]{:S(2)}, u32[]{:S(2)}) collective-permute-start(bf16[416,512]{1,0:T(8,128)(2,1)S(1)} %collective-permute-done.7.refs_2_), channel_id=1, source_target_pairs={{0,1},{1,0},{2,3},{3,2},{4,5},{5,4},{6,7},{7,6},{8,9},{9,8},{10,11... | collective-permute-start | bytes 1277960 | tf_op jit(solution)/shard_map/ppermute | solution.py:17
  173.4 6.9 %collective-permute-start.12 = (bf16[416,512]{1,0:T(8,128)(2,1)S(1)}, bf16[416,512]{1,0:T(8,128)(2,1)}, u32[]{:S(2)}, u32[]{:S(2)}) collective-permute-start(bf16[416,512]{1,0:T(8,128)(2,1)S(1)} %collective-permute-done.8.refs_3_), channel_id=1, source_target_pairs={{0,1},{1,0},{2,3},{3,2},{4,5},{5,4},{6,7},{7,6},{8,9},{9,8},{10,11... | collective-permute-start | bytes 1277960 | tf_op jit(solution)/shard_map/ppermute | solution.py:17
  179.7 26.4 %collective-permute-start.13 = (bf16[2048,128]{1,0:T(8,128)(2,1)S(1)}, bf16[2048,128]{1,0:T(8,128)(2,1)S(1)}, u32[]{:S(2)}, u32[]{:S(2)}) collective-permute-start(bf16[2048,128]{1,0:T(8,128)(2,1)S(1)} %pad_maximum_fusion.1.held_ref), channel_id=1, source_target_pairs={{0,128},{128,0},{1,129},{129,1},{2,130},{130,2},{3,131},{131,3},{4... | collective-permute-start | bytes 1572872 | tf_op jit(solution)/shard_map/ppermute | solution.py:219
  186.7 9.8 %all-to-all-start.4 = ((f32[8,2,384]{2,1,0:T(2,128)}), f32[8,2,384]{2,1,0:T(2,128)S(1)}, u32[]{:S(2)}, u32[]{:S(2)}) async-start(f32[8,2,384]{2,1,0:T(2,128)} %broadcast_in_dim.34), calls=%async_computation.4 | async-start | bytes 49152 | tf_op jit(solution)/shard_map/all_to_all | solution.py:215
  191.1 14.5 %collective-permute-start.15 = (bf16[2048,128]{1,0:T(8,128)(2,1)S(1)}, bf16[2048,128]{1,0:T(8,128)(2,1)S(1)}, u32[]{:S(2)}, u32[]{:S(2)}) collective-permute-start(bf16[2048,128]{1,0:T(8,128)(2,1)S(1)} %pad_maximum_fusion.2.held_ref), channel_id=1, source_target_pairs={{0,128},{128,0},{1,129},{129,1},{2,130},{130,2},{3,131},{131,3},{4... | collective-permute-start | bytes 1572872 | tf_op jit(solution)/shard_map/ppermute | solution.py:219
  206.0 2.4 %collective-permute-start.16 = (bf16[2,384,512]{2,1,0:T(8,128)(2,1)S(1)}, bf16[2,384,512]{2,1,0:T(8,128)(2,1)S(1)}, u32[]{:S(2)}, u32[]{:S(2)}) collective-permute-start(bf16[2,384,512]{2,1,0:T(8,128)(2,1)S(1)} %shares.10), channel_id=1, source_target_pairs={{0,1},{1,0},{2,3},{3,2},{4,5},{5,4},{6,7},{7,6},{8,9},{9,8},{10,11... | collective-permute-start | bytes 2359304 | tf_op jit(solution)/shard_map/ppermute | solution.py:17
  206.5 6.2 %collective-permute-start.14 = (bf16[2,384,512]{2,1,0:T(8,128)(2,1)S(1)}, bf16[2,384,512]{2,1,0:T(8,128)(2,1)S(1)}, u32[]{:S(2)}, u32[]{:S(2)}) collective-permute-start(bf16[2,384,512]{2,1,0:T(8,128)(2,1)S(1)} %shares.8), channel_id=1, source_target_pairs={{0,1},{1,0},{2,3},{3,2},{4,5},{5,4},{6,7},{7,6},{8,9},{9,8},{10,11... | collective-permute-start | bytes 2359304 | tf_op jit(solution)/shard_map/ppermute | solution.py:17
  208.8 22.5 %copy-start.1 = (f32[416,512]{1,0:T(8,128)S(1)}, f32[416,512]{1,0:T(8,128)}, u32[]{:S(2)}) copy-start(f32[416,512]{1,0:T(8,128)} %copy-done) | copy-start | bytes 2555908
  208.8 7.6 %collective-permute-start.17 = (bf16[384,256]{1,0:T(8,128)(2,1)S(1)}, bf16[384,256]{1,0:T(8,128)(2,1)S(1)}, u32[]{:S(2)}, u32[]{:S(2)}) collective-permute-start(bf16[384,256]{1,0:T(8,128)(2,1)S(1)} %get-tuple-element.31), channel_id=1, source_target_pairs={{0,6},{1,7},{2,0},{3,1},{4,2},{5,3},{6,4},{7,5},{8,14},{9,15},{10,... | collective-permute-start | bytes 589832 | tf_op jit(solution)/shard_map/ppermute | solution.py:13
  211.9 12.3 %collective-permute-start.21 = (bf16[384,256]{1,0:T(8,128)(2,1)S(1)}, bf16[384,256]{1,0:T(8,128)(2,1)S(1)}, u32[]{:S(2)}, u32[]{:S(2)}) collective-permute-start(bf16[384,256]{1,0:T(8,128)(2,1)S(1)} %get-tuple-element.34), channel_id=1, source_target_pairs={{0,2},{1,3},{2,4},{3,5},{4,6},{5,7},{6,0},{7,1},{8,10},{9,11},{10,... | collective-permute-start | bytes 589832 | tf_op jit(solution)/shard_map/ppermute | solution.py:13
  211.9 12.1 %collective-permute-start.19 = (bf16[384,256]{1,0:T(8,128)(2,1)S(1)}, bf16[384,256]{1,0:T(8,128)(2,1)S(1)}, u32[]{:S(2)}, u32[]{:S(2)}) collective-permute-start(bf16[384,256]{1,0:T(8,128)(2,1)S(1)} %get-tuple-element.33), channel_id=1, source_target_pairs={{0,2},{1,3},{2,4},{3,5},{4,6},{5,7},{6,0},{7,1},{8,10},{9,11},{10,... | collective-permute-start | bytes 589832 | tf_op jit(solution)/shard_map/ppermute | solution.py:13
  216.5 14.7 %collective-permute-start.18 = (bf16[384,512]{1,0:T(8,128)(2,1)S(1)}, bf16[384,512]{1,0:T(8,128)(2,1)S(1)}, u32[]{:S(2)}, u32[]{:S(2)}) collective-permute-start(bf16[384,512]{1,0:T(8,128)(2,1)S(1)} %pad_maximum_fusion.3), channel_id=1, source_target_pairs={{0,6},{1,7},{2,0},{3,1},{4,2},{5,3},{6,4},{7,5},{8,14},{9,15},{10,... | collective-permute-start | bytes 1179656 | tf_op jit(solution)/shard_map/ppermute | solution.py:13
  224.1 7.1 %collective-permute-start.20 = (bf16[384,256]{1,0:T(8,128)(2,1)S(1)}, bf16[384,256]{1,0:T(8,128)(2,1)S(1)}, u32[]{:S(2)}, u32[]{:S(2)}) collective-permute-start(bf16[384,256]{1,0:T(8,128)(2,1)S(1)} %add_convert_fusion), channel_id=1, source_target_pairs={{0,2},{1,3},{2,4},{3,5},{4,6},{5,7},{6,0},{7,1},{8,10},{9,11},{10,... | collective-permute-start | bytes 589832 | tf_op jit(solution)/shard_map/ppermute | solution.py:13
Sparse Core Ops, SparseCore 0:
  9.2 92.0 all-gather.2
  103.0 75.2 all-gather.4
